TPU v7x, 32 devices: a whole 2x2x4 slice. The times are simulated.
32 devices in a mesh: dp: 4 (over y, x), kv: 4 (over z), tp: 2 (over core).
Axes of the slice: x: 2, y: 2, z: 4, core: 2. Of those that a mesh axis runs over, the one named last changes fastest.
Arguments:
- tokens: bfloat16 [256, 2048], P('dp', ('kv', 'tp')), parts along dimension 0, may hold values from -64 to 64, as said below
- lengths: int32 [32], P(('dp', 'kv', 'tp')), parts along dimension 0, may hold values from 1 to 8, 28 in all
- state: float32 [32, 16, 128, 128], P(('dp', 'kv', 'tp')), parts along dimension 0, may hold values from -1.8 to 1.8
- gain_first: float32 [2048], replicated, may hold values from 0.1 to 1.9
- first_gate: bfloat16 [2048, 5632], P(None, 'kv'), may hold values from -0.125 to 0.125
- first_up: bfloat16 [2048, 5632], P(None, 'kv'), may hold values from -0.125 to 0.125
- first_down: bfloat16 [5632, 2048], P('kv'), may hold values from -0.109375 to 0.109375
- gain_mix: float32 [2048], replicated, may hold values from 0.1 to 1.9
- query_weight: bfloat16 [2048, 2048], P(None, ('kv', 'tp')), may hold values from -0.125 to 0.125
- key_weight: bfloat16 [2048, 2048], P(None, ('kv', 'tp')), may hold values from -0.125 to 0.125
- value_weight: bfloat16 [2048, 2048], P(None, ('kv', 'tp')), may hold values from -0.125 to 0.125
- gating_weight: bfloat16 [2048, 2048], P(None, ('kv', 'tp')), may hold values from -0.125 to 0.125
- write_weight: bfloat16 [2048, 16], replicated, may hold values from -0.125 to 0.125
- forget_weight: bfloat16 [2048, 16], replicated, may hold values from -0.125 to 0.125
- forget_rate: float32 [16], replicated, may hold values from -4 to 1.5
- out_weight: bfloat16 [2048, 2048], P(None, ('kv', 'tp')), may hold values from -0.125 to 0.125
- gain_second: float32 [2048], replicated, may hold values from 0.1 to 1.9
- second_gate: bfloat16 [2048, 5632], P(None, 'kv'), may hold values from -0.125 to 0.125
- second_up: bfloat16 [2048, 5632], P(None, 'kv'), may hold values from -0.125 to 0.125
- second_down: bfloat16 [5632, 2048], P('kv'), may hold values from -0.109375 to 0.109375
Outputs:
- mixed_out: bfloat16 [256, 2048], P('dp', ('kv', 'tp')), parts along dimension 0
- new_state: float32 [32, 16, 128, 128], P(('dp', 'kv', 'tp')), parts along dimension 0
There are 4 independent parts, one for each index of `dp`. A program takes and returns all parts, laid end to end along the dimension named above; an argument that names none is the same for every part. Nothing has to cross between parts.
Inputs may be any that keep to these rules, and one draw needn't show every extreme that they name: Activations of the new tokens. `lengths`: the live new tokens of each sequence; within each independent group of 8 sequences (one part along dp) they sum to seven halves of 8, rounded down, and some sequence of each group has all 8 live.
All inputs are finite; a program needn't handle non-finite values.
Results may differ from a plain program's by a relative error of at most 0.0058.
Values may be sent and summed in bfloat16 or wider, within the bound.
A program may use at most 128 MiB of HBM per device.

v0:
```python
import functools
import math

import jax
import jax.numpy as jnp
from jax import lax
from jax.experimental import pallas as pl
from jax.experimental.pallas import tpu as pltpu
from jax.sharding import PartitionSpec as P

HEADS = 16
HEAD = 128
BLK = 8


EPSILON = 1e-06


def fold_step(gain, gate_cols, up_cols, portion):
    values = portion.astype(jnp.float32)
    scaled = (values * gain).astype(jnp.bfloat16)
    gate_acc = jnp.dot(scaled, gate_cols, preferred_element_type=jnp.float32)
    up_acc = jnp.dot(scaled, up_cols, preferred_element_type=jnp.float32)
    squares = jnp.sum(values * values, axis=1)
    return (gate_acc, up_acc, squares)


def finish_units(gate_acc, up_acc, squares, channels, down_rows):
    row_scale = lax.rsqrt(squares / channels + EPSILON)[:, None]
    hidden = (jax.nn.silu(gate_acc * row_scale) * (up_acc * row_scale)).astype(jnp.bfloat16)
    return jnp.dot(hidden, down_rows, preferred_element_type=jnp.float32)


def feed_forward(hidden_in, gain, w_gate, w_up, w_down):
    channels = gain.shape[0]
    paired = lax.all_to_all(hidden_in, "tp", split_axis=0, concat_axis=1, tiled=True)
    gate_acc, up_acc, squares = fold_step(
        gain, w_gate, w_up, lax.all_gather(paired, "kv", axis=1, tiled=True)
    )
    ffn_term = finish_units(gate_acc, up_acc, squares, channels, w_down)
    partial_value = lax.psum_scatter(ffn_term, "kv", scatter_dimension=1, tiled=True)
    summed = lax.all_to_all(partial_value, "tp", split_axis=1, concat_axis=0, tiled=True)
    return (hidden_in.astype(jnp.float32) + 0.5 * summed).astype(jnp.bfloat16)


def delta_block(query, key_in, value, gating, write_pre, forget_pre, rates, live, state):
    seq_count, block_len, head_count, head_size = query.shape
    precise = lax.Precision.HIGHEST
    query_unit = (
        query
        * lax.rsqrt(jnp.sum(query * query, axis=-1, keepdims=True) + EPSILON)
        / math.sqrt(head_size)
    )
    key_unit = key_in * lax.rsqrt(jnp.sum(key_in * key_in, axis=-1, keepdims=True) + EPSILON)
    live_rows = live[:, :, None]
    write_gate = jax.nn.sigmoid(write_pre) * live_rows
    forget = -jnp.exp(rates)[None, None, :] * jax.nn.softplus(forget_pre) * live_rows
    cumulative = jnp.cumsum(forget, axis=1)
    cum_heads = jnp.transpose(cumulative, (0, 2, 1))
    positions = jnp.arange(block_len)
    causal = positions[:, None] >= positions[None, :]
    strict = positions[:, None] > positions[None, :]
    differ = jnp.minimum(cum_heads[:, :, :, None] - cum_heads[:, :, None, :], 0.0)
    decay_mat = jnp.where(causal, jnp.exp(differ), 0.0)
    key_dots = jnp.einsum("sthd,suhd->shtu", key_unit, key_unit, precision=precise)
    write_heads = jnp.transpose(write_gate, (0, 2, 1))
    strict_part = jnp.where(strict, write_heads[:, :, :, None] * decay_mat * key_dots, 0.0)
    identity = jnp.eye(block_len, dtype=jnp.float32)
    squared = jnp.einsum("shtu,shuv->shtv", strict_part, strict_part, precision=precise)
    fourth = jnp.einsum("shtu,shuv->shtv", squared, squared, precision=precise)
    inverse = jnp.einsum(
        "shtu,shuv->shtv", identity - strict_part, identity + squared, precision=precise
    )
    inverse = jnp.einsum("shtu,shuv->shtv", inverse, identity + fourth, precision=precise)
    growth = jnp.exp(cumulative)
    target = jnp.einsum(
        "shtu,suhv->sthv", inverse, write_gate[..., None] * value, precision=precise
    )
    key_mix = jnp.einsum(
        "shtu,suhk->sthk", inverse, (write_gate * growth)[..., None] * key_unit, precision=precise
    )
    update = target - jnp.einsum("sthk,shkv->sthv", key_mix, state, precision=precise)
    scores = jnp.einsum("sthd,suhd->shtu", query_unit, key_unit, precision=precise) * decay_mat
    attend = jnp.einsum("sthk,shkv->sthv", query_unit * growth[..., None], state, precision=precise)
    attend = attend + jnp.einsum("shtu,suhv->sthv", scores, update, precision=precise)
    final_cum = cumulative[:, -1:, :]
    fading = jnp.exp(final_cum - cumulative)
    new_state = jnp.exp(final_cum[:, 0, :])[:, :, None, None] * state
    new_state = new_state + jnp.einsum(
        "sthk,sthv->shkv", key_unit * fading[..., None], update, precision=precise
    )
    normed = attend * lax.rsqrt(jnp.mean(attend * attend, axis=-1, keepdims=True) + EPSILON)
    normed = normed * jax.nn.silu(gating) * live[:, :, None, None]
    mixed_heads = normed.reshape(seq_count * block_len, head_count * head_size).astype(jnp.bfloat16)
    return (mixed_heads, new_state)


def per_device(
    tokens,
    lengths,
    state,
    gain_first,
    first_gate,
    first_up,
    first_down,
    gain_mix,
    query_weight,
    key_weight,
    value_weight,
    gating_weight,
    write_weight,
    forget_weight,
    forget_rate,
    out_weight,
    gain_second,
    second_gate,
    second_up,
    second_down,
):
    after_first = feed_forward(tokens, gain_first, first_gate, first_up, first_down)
    seq_count = lengths.shape[0]
    own_count = seq_count * BLK
    whole_rows = lax.all_gather(after_first, ("kv", "tp"), axis=1, tiled=True)
    scaled_all = (whole_rows.astype(jnp.float32) * gain_mix).astype(jnp.bfloat16)
    stacked = jnp.stack(
        [
            jnp.dot(scaled_all, matrix, preferred_element_type=jnp.float32)
            for matrix in (query_weight, key_weight, value_weight, gating_weight)
        ]
    )
    owned = lax.all_to_all(
        stacked.astype(jnp.bfloat16), ("kv", "tp"), split_axis=1, concat_axis=2, tiled=True
    ).astype(stacked.dtype)
    row_start = lax.axis_index(("kv", "tp")) * own_count
    own_values = lax.dynamic_slice_in_dim(whole_rows, row_start, own_count, 0).astype(jnp.float32)
    own_scaled = lax.dynamic_slice_in_dim(scaled_all, row_start, own_count, 0)
    mix_scale = lax.rsqrt(jnp.mean(own_values * own_values, axis=1, keepdims=True) + EPSILON)
    query = (owned[0] * mix_scale).reshape(seq_count, BLK, HEADS, HEAD)
    key_in = (owned[1] * mix_scale).reshape(seq_count, BLK, HEADS, HEAD)
    value = (owned[2] * mix_scale).reshape(seq_count, BLK, HEADS, HEAD)
    gating = (owned[3] * mix_scale).reshape(seq_count, BLK, HEADS, HEAD)
    write_pre = (
        jnp.dot(own_scaled, write_weight, preferred_element_type=jnp.float32) * mix_scale
    ).reshape(seq_count, BLK, HEADS)
    forget_pre = (
        jnp.dot(own_scaled, forget_weight, preferred_element_type=jnp.float32) * mix_scale
    ).reshape(seq_count, BLK, HEADS)
    positions = jnp.arange(BLK, dtype=jnp.int32)
    live = (positions[None, :] < lengths[:, None]).astype(jnp.float32)
    mixed_heads, new_state = delta_block(
        query, key_in, value, gating, write_pre, forget_pre, forget_rate, live, state
    )
    half_cols = mixed_heads.shape[1] // 2
    portion = lax.all_gather(mixed_heads, ("kv", "tp"), axis=0, tiled=True)
    first_half = jnp.dot(
        portion[:, :half_cols], out_weight[:half_cols], preferred_element_type=jnp.float32
    ).astype(jnp.bfloat16)
    second_half = jnp.dot(
        portion[:, half_cols:], out_weight[half_cols:], preferred_element_type=jnp.float32
    ).astype(jnp.bfloat16)
    first_half, second_half = lax.optimization_barrier((first_half, second_half))
    mixed_sum = first_half.astype(jnp.float32) + second_half.astype(jnp.float32)
    after_mix = (after_first.astype(jnp.float32) + mixed_sum).astype(jnp.bfloat16)
    mixed_out = feed_forward(after_mix, gain_second, second_gate, second_up, second_down)
    return (mixed_out, new_state)


F32 = jnp.float32
BF16 = jnp.bfloat16
MESH = pl.DeviceIdType.MESH
VMEM_LIMIT = 60 * 1024 * 1024


def fused_kernel(
    kv_size,
    channels,
    tokens_hbm,
    lengths_ref,
    gains1_hbm,
    gains_mix_hbm,
    gains2_hbm,
    rates_hbm,
    state_hbm,
    gate1_hbm,
    up1_hbm,
    down1_hbm,
    query_hbm,
    key_hbm,
    value_hbm,
    gating_hbm,
    write_hbm,
    forget_hbm,
    out_hbm,
    gate2_hbm,
    up2_hbm,
    down2_hbm,
    mixed_out_ref,
    new_state_hbm,
    gate1,
    up1,
    down1,
    gate2,
    up2,
    down2,
    proj,
    out_w,
    small_w,
    state,
    state_high,
    state_low,
    gains1_ref,
    gains_mix_ref,
    gains2_ref,
    rates_ref,
    state_out,
    gate_acc,
    up_acc,
    proj_acc,
    small_acc,
    gathers,
    heads_all,
    pair_send,
    pair_recv,
    red_send,
    red_recv,
    part_send,
    part_recv,
    load_sems,
    gather_send_sems,
    gather_recv_sems,
    pair_send_sems,
    pair_recv_sems,
    red_send_sems,
    red_recv_sems,
    part_send_sems,
    part_recv_sems,
    store_sem,
):
    kv = lax.axis_index("kv")
    tp = lax.axis_index("tp")
    devices = 2 * kv_size
    me = kv * 2 + tp
    rows, cols = tokens_hbm.shape
    take = gate1.shape[1]
    hidden_local = gate1_hbm.shape[1]
    lead = hidden_local - take
    overlap = 2 * take - hidden_local
    first_col = pl.multiple_of(tp * lead, 128)

    def load(index, src, dst):
        return pltpu.make_async_copy(src, dst, load_sems.at[index])

    cut = pl.ds(first_col, take)
    loads = {
        "gate1": load(0, gate1_hbm.at[:, cut], gate1),
        "up1": load(1, up1_hbm.at[:, cut], up1),
        "down1": load(2, down1_hbm.at[cut, :], down1),
        "query": load(3, query_hbm, proj.at[:, 0:cols]),
        "key": load(4, key_hbm, proj.at[:, cols : 2 * cols]),
        "value": load(5, value_hbm, proj.at[:, 2 * cols : 3 * cols]),
        "gating": load(6, gating_hbm, proj.at[:, 3 * cols : 4 * cols]),
        "write": load(7, write_hbm, small_w.at[0:HEADS]),
        "forget": load(8, forget_hbm, small_w.at[HEADS : 2 * HEADS]),
        "state": load(9, state_hbm.at[0], state),
        "out": load(10, out_hbm, out_w),
        "gate2": load(11, gate2_hbm.at[:, cut], gate2),
        "up2": load(12, up2_hbm.at[:, cut], up2),
        "down2": load(13, down2_hbm.at[cut, :], down2),
        "tokens": load(14, tokens_hbm, gathers.at[0, me]),
        "gains1": load(15, gains1_hbm, gains1_ref),
        "gains_mix": load(16, gains_mix_hbm, gains_mix_ref),
        "gains2": load(17, gains2_hbm, gains2_ref),
        "rates": load(18, rates_hbm, rates_ref),
    }
    small = ("tokens", "gains1", "gains_mix", "gains2", "rates")
    for name in small + ("gate1", "up1", "down1"):
        loads[name].start()

    def remote(src, dst, send_sem, recv_sem, to_kv, to_tp):
        return pltpu.make_async_remote_copy(
            src_ref=src,
            dst_ref=dst,
            send_sem=send_sem,
            recv_sem=recv_sem,
            device_id={"kv": to_kv, "tp": to_tp},
            device_id_type=MESH,
        )

    barrier = pltpu.get_barrier_semaphore()
    for off in range(1, devices):
        peer = lax.rem(me + off, devices)
        pl.semaphore_signal(
            barrier,
            inc=1,
            device_id={"kv": peer // 2, "tp": lax.rem(peer, 2)},
            device_id_type=MESH,
        )
    pl.semaphore_wait(barrier, devices - 1)

    sent = []

    def swapped(off):
        chip, bit = kv, 1
        while bit < kv_size:
            if off & bit:
                chip = chip + bit - 2 * bit * lax.rem(kv // bit, 2)
            bit *= 2
        return chip

    def gather_start(phase, buf):
        copies = {}
        for off in list(range(kv_size - 1, 0, -1)) + [0]:
            copies[off] = remote(
                buf.at[me],
                buf.at[me],
                gather_send_sems.at[phase, off],
                gather_recv_sems.at[phase, off],
                swapped(off),
                1 - tp,
            )
            copies[off].start()
        return copies

    def gather_finish(phase, buf, copies, use=lambda slot, first: None):
        use(me, True)
        copies[0].wait_recv()
        use(kv * 2 + 1 - tp, False)
        forwards = {}
        for off in range(1, kv_size):
            copies[off].wait_recv()
            slot = swapped(off) * 2 + 1 - tp
            forwards[off] = remote(
                buf.at[slot],
                buf.at[slot],
                gather_send_sems.at[phase, kv_size - 1 + off],
                gather_recv_sems.at[phase, kv_size - 1 + off],
                kv,
                1 - tp,
            )
            forwards[off].start()
        for off in range(1, kv_size):
            use(swapped(off) * 2 + 1 - tp, False)
        for off in range(1, kv_size):
            forwards[off].wait_recv()
            use(swapped(off) * 2 + tp, False)
        sent.extend(copies.values())
        sent.extend(forwards.values())

    def multiply(buf, gain_ref, products):
        squares = [jnp.zeros((rows, 1), F32)]

        def use(slot, first):
            at = pl.ds(pl.multiple_of(slot * cols, cols), cols)
            values = buf[slot].astype(F32)
            squares[0] = squares[0] + jnp.sum(values * values, axis=1, keepdims=True)
            scaled = (values * gain_ref[:, at]).astype(BF16)
            for acc, weight, across in products:
                if across:
                    term = lax.dot_general(
                        scaled,
                        weight[:, at],
                        (((1,), (1,)), ((), ())),
                        preferred_element_type=F32,
                    )
                else:
                    term = jnp.dot(scaled, weight[at, :], preferred_element_type=F32)
                if first:
                    acc[...] = term
                else:
                    acc[...] += term

        return squares, use

    def inverse_rms(squares):
        return lax.rsqrt(squares[0] / channels + EPSILON)

    def half_step(phase, at, buf, copies, gain_ref, names, gate_w, up_w, down_w):
        loads[names[0]].wait()
        loads[names[1]].wait()
        squares, use = multiply(buf, gain_ref, ((gate_acc, gate_w, False), (up_acc, up_w, False)))
        gather_finish(at, buf, copies, use)
        row_scale = inverse_rms(squares)
        gate = gate_acc[...] * row_scale
        up = up_acc[...] * row_scale
        column = lax.broadcasted_iota(jnp.int32, (rows, take), 1)
        hidden = jnp.where(column >= tp * overlap, jax.nn.silu(gate) * up, 0.0).astype(BF16)
        loads[names[2]].wait()

        def columns_of(chip, core):
            at = pl.multiple_of((chip * 2 + core) * cols, cols)
            return jnp.dot(hidden, down_w[:, pl.ds(at, cols)], preferred_element_type=F32)

        order = list(range(kv_size - 1, -1, -1))
        pair_copies = []
        for off in order:
            pair_send[phase, off] = columns_of(swapped(off), tp if off else 1 - tp)
            copy = remote(
                pair_send.at[phase, off],
                pair_recv.at[phase, off],
                pair_send_sems.at[phase, off],
                pair_recv_sems.at[phase, off],
                kv,
                1 - tp,
            )
            copy.start()
            pair_copies.append(copy)
        red_copies = []
        total = None
        for position, off in enumerate(order):
            term = columns_of(swapped(off), 1 - tp if off else tp)
            pair_copies[position].wait_recv()
            term = term + pair_recv[phase, off]
            if off == 0:
                total = term
                continue
            red_send[phase, off] = term.astype(BF16)
            copy = remote(
                red_send.at[phase, off],
                red_recv.at[phase, off],
                red_send_sems.at[phase, off],
                red_recv_sems.at[phase, off],
                swapped(off),
                1 - tp,
            )
            copy.start()
            red_copies.append(copy)
        for copy in red_copies[::-1]:
            copy.wait_recv()
        for off in range(1, kv_size):
            total = total + red_recv[phase, off].astype(F32)
        sent.extend(pair_copies + red_copies)
        return total

    for name in small:
        loads[name].wait()
    copies = gather_start(0, gathers.at[0])
    for name in ("query", "key", "value", "gating", "write", "forget", "state", "out"):
        loads[name].start()
    for name in ("gate2", "up2", "down2"):
        loads[name].start()
    total = half_step(
        0, 0, gathers.at[0], copies, gains1_ref, ("gate1", "up1", "down1"), gate1, up1, down1
    )
    after_first = (gathers[0, me].astype(F32) + 0.5 * total).astype(BF16)
    gathers[1, me] = after_first
    copies = gather_start(1, gathers.at[1])

    loads["state"].wait()
    for head in range(HEADS):
        high = state[head].astype(BF16)
        state_high[head] = high
        state_low[head] = (state[head] - high.astype(F32)).astype(BF16)
    for name in ("query", "key", "value", "gating", "write", "forget"):
        loads[name].wait()
    squares, use = multiply(
        gathers.at[1], gains_mix_ref, ((proj_acc, proj, False), (small_acc, small_w, True))
    )
    gather_finish(1, gathers.at[1], copies, use)
    mix_scale = inverse_rms(squares)
    part_send[...] = (proj_acc[...] * mix_scale).reshape(devices, BLK, 4 * cols).astype(BF16)
    part_copies = []
    for off in range(1, devices):
        peer = lax.rem(me + off, devices)
        copy = remote(
            part_send.at[peer],
            part_recv.at[me],
            part_send_sems.at[off],
            part_recv_sems.at[off],
            peer // 2,
            lax.rem(peer, 2),
        )
        copy.start()
        part_copies.append(copy)
    part_recv[me] = part_send[me]
    small_acc[...] = small_acc[...] * mix_scale
    own = pl.ds(pl.multiple_of(me * BLK, BLK), BLK)
    write_pre = small_acc[own, 0:HEADS]
    forget_pre = small_acc[own, HEADS : 2 * HEADS]

    size = HEADS * BLK
    row = lax.broadcasted_iota(jnp.int32, (size, size), 0)
    col = lax.broadcasted_iota(jnp.int32, (size, size), 1)
    same = (row // BLK) == (col // BLK)
    causal = same & (row >= col)
    strict = same & (row > col)
    diagonal = row == col
    identity = jnp.where(diagonal, 1.0, 0.0)
    head_row = lax.broadcasted_iota(jnp.int32, (size, HEADS), 0) // BLK
    head_col = lax.broadcasted_iota(jnp.int32, (size, HEADS), 1)
    pick = head_row == head_col

    def as_column(block):
        return jnp.sum(jnp.where(pick, block, 0.0), axis=1, keepdims=True)

    def to_row(column):
        return jnp.sum(jnp.where(diagonal, column, 0.0), axis=0, keepdims=True)

    token_at = lax.rem(lax.broadcasted_iota(jnp.int32, (size, 1), 0), BLK)
    live = jnp.where(token_at < lengths_ref[0], 1.0, 0.0)
    write_col = as_column(jnp.concatenate([write_pre] * HEADS, axis=0))
    forget_col = as_column(jnp.concatenate([forget_pre] * HEADS, axis=0))
    rate_col = as_column(jnp.broadcast_to(rates_ref[...], (size, HEADS)))
    write_gate = jax.nn.sigmoid(write_col) * live
    softplus = jnp.maximum(forget_col, 0.0) + jnp.log1p(jnp.exp(-jnp.abs(forget_col)))
    forget = -jnp.exp(rate_col) * softplus * live
    forget_row = to_row(forget)
    cumulative = jnp.sum(jnp.where(causal, forget_row, 0.0), axis=1, keepdims=True)
    final = jnp.sum(jnp.where(same, forget_row, 0.0), axis=1, keepdims=True)
    decay = jnp.where(causal, jnp.exp(jnp.minimum(cumulative - to_row(cumulative), 0.0)), 0.0)
    growth = jnp.exp(cumulative)
    fading = jnp.exp(final - cumulative)
    shrink = jnp.exp(final)

    for copy in part_copies:
        copy.wait_recv()

    def by_head(index):
        pieces = []
        for j in range(devices):
            block = part_recv[j, :, index * cols : (index + 1) * cols].astype(F32)
            for at in range(0, cols, HEAD):
                pieces.append(block[:, at : at + HEAD])
        return jnp.concatenate(pieces, axis=0)

    def cut_terms(a):
        high = a.astype(BF16).astype(F32)
        return high, a - high

    def dot(a, b, across=False):
        high_a, low_a = cut_terms(a)
        high_b, low_b = cut_terms(b)
        axis = 1 if across else 0
        left = jnp.concatenate([high_a, high_a, low_a], axis=1).astype(BF16)
        right = jnp.concatenate([high_b, low_b, high_b], axis=axis).astype(BF16)
        return lax.dot_general(
            left, right, (((1,), (axis,)), ((), ())), preferred_element_type=F32
        )

    query, key_in, value, gating = (by_head(index) for index in range(4))
    query_unit = (
        query
        * lax.rsqrt(jnp.sum(query * query, axis=1, keepdims=True) + EPSILON)
        * (1.0 / math.sqrt(HEAD))
    )
    key_unit = key_in * lax.rsqrt(jnp.sum(key_in * key_in, axis=1, keepdims=True) + EPSILON)
    products = dot(jnp.concatenate([key_unit, query_unit], axis=0), key_unit, True)
    lower = products[:size]
    lower = jnp.where(strict, write_gate * decay * lower, 0.0)
    squared = dot(lower, lower)
    fourth = dot(squared, squared)
    inverse = dot(identity - lower, identity + squared)
    inverse = dot(inverse, identity + fourth)
    key_grown = (write_gate * growth) * key_unit
    query_grown = query_unit * growth
    scores = products[size:] * decay

    key_terms, query_terms = [], []
    for head in range(HEADS):
        at = slice(head * BLK, (head + 1) * BLK)
        high, low = cut_terms(jnp.concatenate([key_grown[at], query_grown[at]], axis=0))
        both = jnp.concatenate([high, low], axis=0).astype(BF16)
        result = jnp.dot(both, state_high[head], preferred_element_type=F32)
        result = result[: 2 * BLK] + result[2 * BLK :]
        result = result + jnp.dot(
            both[: 2 * BLK], state_low[head], preferred_element_type=F32
        )
        key_terms.append(result[:BLK])
        query_terms.append(result[BLK:])
    update = dot(inverse, write_gate * value - jnp.concatenate(key_terms, axis=0))
    attend = jnp.concatenate(query_terms, axis=0) + dot(scores, update)
    normed = attend * lax.rsqrt(jnp.mean(attend * attend, axis=1, keepdims=True) + EPSILON)
    normed = normed * jax.nn.silu(gating) * live
    heads_all[me] = jnp.concatenate(
        [normed[head * BLK : (head + 1) * BLK] for head in range(HEADS)], axis=1
    ).astype(BF16)
    copies = gather_start(2, heads_all)
    faded = key_unit * fading
    for head in range(HEADS):
        at = slice(head * BLK, (head + 1) * BLK)
        key_high, key_low = cut_terms(faded[at])
        value_high, value_low = cut_terms(update[at])
        outer = lax.dot_general(
            jnp.concatenate([key_high, key_high, key_low], axis=0).astype(BF16),
            jnp.concatenate([value_high, value_low, value_high], axis=0).astype(BF16),
            (((0,), (0,)), ((), ())),
            preferred_element_type=F32,
        )
        state_out[head] = shrink[head * BLK : head * BLK + 1] * state[head] + outer
    store = pltpu.make_async_copy(state_out, new_state_hbm.at[0], store_sem)
    store.start()
    gather_finish(2, heads_all, copies)

    mixed = heads_all[...].astype(F32).reshape(rows, HEADS * HEAD).astype(BF16)
    loads["out"].wait()
    half = HEADS * HEAD // 2
    first = jnp.dot(mixed[:, :half], out_w[:half], preferred_element_type=F32).astype(BF16)
    second = jnp.dot(mixed[:, half:], out_w[half:], preferred_element_type=F32).astype(BF16)
    residual = gathers[1, me].astype(F32)
    after_mix = (residual + (first.astype(F32) + second.astype(F32))).astype(BF16)
    gathers[2, me] = after_mix
    copies = gather_start(3, gathers.at[2])

    total = half_step(
        1, 3, gathers.at[2], copies, gains2_ref, ("gate2", "up2", "down2"), gate2, up2, down2
    )
    mixed_out_ref[...] = (gathers[2, me].astype(F32) + 0.5 * total).astype(BF16)
    for copy in part_copies + sent:
        copy.wait_send()
    store.wait()


def fused_call(mesh, *args):
    (
        tokens, lengths, state, gain_first, first_gate, first_up, first_down, gain_mix,
        query_weight, key_weight, value_weight, gating_weight, write_weight, forget_weight,
        forget_rate, out_weight, gain_second, second_gate, second_up, second_down,
    ) = args
    kv_size = mesh.shape["kv"]
    devices = kv_size * mesh.shape["tp"]
    rows, cols = tokens.shape
    channels = gain_first.shape[0]
    hidden_local = first_gate.shape[1]
    take = -(-hidden_local // 256) * 128
    phases = 2
    in_vmem = pl.BlockSpec(memory_space=pltpu.VMEM)
    in_smem = pl.BlockSpec(memory_space=pltpu.SMEM)
    in_any = pl.BlockSpec(memory_space=pl.ANY)
    dma = pltpu.SemaphoreType.DMA
    mixed_out, new_state = pl.pallas_call(
        functools.partial(fused_kernel, kv_size, channels),
        out_shape=(
            jax.ShapeDtypeStruct(tokens.shape, tokens.dtype),
            jax.ShapeDtypeStruct(state.shape, state.dtype),
        ),
        in_specs=[in_any, in_smem] + [in_any] * 18,
        out_specs=(in_vmem, in_any),
        scratch_shapes=[
            pltpu.VMEM((channels, take), BF16),
            pltpu.VMEM((channels, take), BF16),
            pltpu.VMEM((take, channels), BF16),
            pltpu.VMEM((channels, take), BF16),
            pltpu.VMEM((channels, take), BF16),
            pltpu.VMEM((take, channels), BF16),
            pltpu.VMEM((channels, 4 * cols), BF16),
            pltpu.VMEM(out_weight.shape, BF16),
            pltpu.VMEM((2 * HEADS, channels), BF16),
            pltpu.VMEM(state.shape[1:], F32),
            pltpu.VMEM(state.shape[1:], BF16),
            pltpu.VMEM(state.shape[1:], BF16),
            pltpu.VMEM((1, channels), F32),
            pltpu.VMEM((1, channels), F32),
            pltpu.VMEM((1, channels), F32),
            pltpu.VMEM((1, HEADS), F32),
            pltpu.VMEM(state.shape[1:], F32),
            pltpu.VMEM((rows, take), F32),
            pltpu.VMEM((rows, take), F32),
            pltpu.VMEM((rows, 4 * cols), F32),
            pltpu.VMEM((rows, 2 * HEADS), F32),
            pltpu.VMEM((3, devices, rows, cols), BF16),
            pltpu.VMEM((devices, BLK, HEADS * HEAD), BF16),
            pltpu.VMEM((phases, kv_size, rows, cols), F32),
            pltpu.VMEM((phases, kv_size, rows, cols), F32),
            pltpu.VMEM((phases, kv_size, rows, cols), BF16),
            pltpu.VMEM((phases, kv_size, rows, cols), BF16),
            pltpu.VMEM((devices, BLK, 4 * cols), BF16),
            pltpu.VMEM((devices, BLK, 4 * cols), BF16),
            dma((19,)),
            dma((4, 2 * kv_size)),
            dma((4, 2 * kv_size)),
            dma((phases, kv_size)),
            dma((phases, kv_size)),
            dma((phases, kv_size)),
            dma((phases, kv_size)),
            dma((devices,)),
            dma((devices,)),
            dma,
        ],
        compiler_params=pltpu.CompilerParams(
            collective_id=0, has_side_effects=True, vmem_limit_bytes=VMEM_LIMIT
        ),
    )(
        tokens, lengths, gain_first.reshape(1, -1), gain_mix.reshape(1, -1),
        gain_second.reshape(1, -1), forget_rate.reshape(1, -1), state,
        first_gate, first_up, first_down, query_weight, key_weight, value_weight,
        gating_weight, write_weight.T, forget_weight.T, out_weight, second_gate, second_up,
        second_down,
    )
    return hand_out(mixed_out, new_state)


def hand_out_kernel(mixed_hbm, state_hbm, mixed_out_hbm, state_out_hbm, mixed, held, in_sems, out_sems):
    heads = held.shape[0]
    count = in_sems.shape[0] - 1
    step = heads // count
    takes = [pltpu.make_async_copy(mixed_hbm, mixed, in_sems.at[count])]
    puts = [pltpu.make_async_copy(mixed, mixed_out_hbm, out_sems.at[count])]
    for i in range(count):
        at = pl.ds(i * step, step)
        takes.append(pltpu.make_async_copy(state_hbm.at[0, at], held.at[at], in_sems.at[i]))
        puts.append(pltpu.make_async_copy(held.at[at], state_out_hbm.at[0, at], out_sems.at[i]))
    for take in takes:
        take.start()
    for take, put in zip(takes, puts):
        take.wait()
        put.start()
    for put in puts:
        put.wait()


def hand_out(mixed_out, new_state):
    in_any = pl.BlockSpec(memory_space=pl.ANY)
    return pl.pallas_call(
        hand_out_kernel,
        out_shape=(
            jax.ShapeDtypeStruct(mixed_out.shape, mixed_out.dtype),
            jax.ShapeDtypeStruct(new_state.shape, new_state.dtype),
        ),
        in_specs=[in_any, in_any],
        out_specs=(in_any, in_any),
        scratch_shapes=[
            pltpu.VMEM(mixed_out.shape, mixed_out.dtype),
            pltpu.VMEM(new_state.shape[1:], new_state.dtype),
            pltpu.SemaphoreType.DMA((5,)),
            pltpu.SemaphoreType.DMA((5,)),
        ],
        compiler_params=pltpu.CompilerParams(vmem_limit_bytes=VMEM_LIMIT),
    )(mixed_out, new_state)


def fits_fused(mesh, args):
    tokens, lengths, state, first_gate = args[0], args[1], args[2], args[4]
    rows, cols = tokens.shape
    devices = mesh.shape["kv"] * mesh.shape["tp"]
    return (
        mesh.shape["tp"] == 2
        and mesh.shape["kv"] & (mesh.shape["kv"] - 1) == 0
        and lengths.shape[0] == 1
        and rows == devices * BLK
        and cols % 256 == 0
        and first_gate.shape[1] % 128 == 0
        and state.shape[1:] == (HEADS, HEAD, HEAD)
    )


def solution(mesh):
    in_specs = (
        P("dp", ("kv", "tp")),
        P(("dp", "kv", "tp")),
        P(("dp", "kv", "tp"), None, None, None),
        P(),
        P(None, "kv"),
        P(None, "kv"),
        P("kv", None),
        P(),
        P(None, ("kv", "tp")),
        P(None, ("kv", "tp")),
        P(None, ("kv", "tp")),
        P(None, ("kv", "tp")),
        P(),
        P(),
        P(),
        P(None, ("kv", "tp")),
        P(),
        P(None, "kv"),
        P(None, "kv"),
        P("kv", None),
    )
    out_specs = (P("dp", ("kv", "tp")), P(("dp", "kv", "tp"), None, None, None))

    def body(*args):
        if fits_fused(mesh, args):
            return fused_call(mesh, *args)
        return per_device(*args)

    return jax.shard_map(
        body, mesh=mesh, in_specs=in_specs, out_specs=out_specs, check_vma=False
    )
```

profile of v0, /device:TPU:0, one launch (start us, length us, event | category | flops | bytes accessed | tf_op | source)
XLA Modules:
  0.0 51.4 jit_solution(8648459061355471020)
XLA Ops:
  1.3 48.1 %shard_map.203 = (bf16[64,256]{1,0:T(8,128)(2,1)}, f32[1,16,128,128]{3,2,1,0:T(8,128)}) custom-call(bf16[64,256]{1,0:T(8,128)(2,1)} %tokens_hbm.1, s32[1]{0:T(128)S(6)} %copy.22.lengths_ref, f32[1,2048]{1,0:T(1,128)} %bitcast.8, f32[1,2048]{1,0:T(1,128)} %bitcast.9, f32[1,2048]{1,0:T(1,128)} %bitcast.10, f32[1,16]{1,0:T(1,128)} %bitcast.11, ...), custom_call_target="tpu_custom_call" | custom-call | tf_op jit(solution)/shard_map/pallas_call | solution.py:629
  49.4 2.0 %shard_map.204 = (bf16[64,256]{1,0:T(8,128)(2,1)}, f32[1,16,128,128]{3,2,1,0:T(8,128)}) custom-call(bf16[64,256]{1,0:T(8,128)(2,1)} %get-tuple-element.4.mixed_hbm, f32[1,16,128,128]{3,2,1,0:T(8,128)} %get-tuple-element.5.state_hbm), custom_call_target="tpu_custom_call" | custom-call | tf_op jit(solution)/shard_map/pallas_call | solution.py:712
where the time goes:
time: 51.6 us; the launch traced here: 51.4 us
  Pallas kernels  50.1 us (97%)
  between operations  1.29 us (2%)
    pallas_call x1, Pallas kernels, fused_call(): pl.pallas_call(functools.partial(fused_kernel, kv_size, channels), out_sh...  48.1 us
    pallas_call x1, Pallas kernels, hand_out(): pl.pallas_call(hand_out_kernel, out_shape=(jax.ShapeDtypeStruct(mixed_out...  2.02 us

commit v1 on v0

v1 whole, which is shorter than its diff:
```python
import functools
import math

import jax
import jax.numpy as jnp
from jax import lax
from jax.experimental import pallas as pl
from jax.experimental.pallas import tpu as pltpu
from jax.sharding import PartitionSpec as P

HEADS = 16
HEAD = 128
BLK = 8


EPSILON = 1e-06


def fold_step(gain, gate_cols, up_cols, portion):
    values = portion.astype(jnp.float32)
    scaled = (values * gain).astype(jnp.bfloat16)
    gate_acc = jnp.dot(scaled, gate_cols, preferred_element_type=jnp.float32)
    up_acc = jnp.dot(scaled, up_cols, preferred_element_type=jnp.float32)
    squares = jnp.sum(values * values, axis=1)
    return (gate_acc, up_acc, squares)


def finish_units(gate_acc, up_acc, squares, channels, down_rows):
    row_scale = lax.rsqrt(squares / channels + EPSILON)[:, None]
    hidden = (jax.nn.silu(gate_acc * row_scale) * (up_acc * row_scale)).astype(jnp.bfloat16)
    return jnp.dot(hidden, down_rows, preferred_element_type=jnp.float32)


def feed_forward(hidden_in, gain, w_gate, w_up, w_down):
    channels = gain.shape[0]
    paired = lax.all_to_all(hidden_in, "tp", split_axis=0, concat_axis=1, tiled=True)
    gate_acc, up_acc, squares = fold_step(
        gain, w_gate, w_up, lax.all_gather(paired, "kv", axis=1, tiled=True)
    )
    ffn_term = finish_units(gate_acc, up_acc, squares, channels, w_down)
    partial_value = lax.psum_scatter(ffn_term, "kv", scatter_dimension=1, tiled=True)
    summed = lax.all_to_all(partial_value, "tp", split_axis=1, concat_axis=0, tiled=True)
    return (hidden_in.astype(jnp.float32) + 0.5 * summed).astype(jnp.bfloat16)


def delta_block(query, key_in, value, gating, write_pre, forget_pre, rates, live, state):
    seq_count, block_len, head_count, head_size = query.shape
    precise = lax.Precision.HIGHEST
    query_unit = (
        query
        * lax.rsqrt(jnp.sum(query * query, axis=-1, keepdims=True) + EPSILON)
        / math.sqrt(head_size)
    )
    key_unit = key_in * lax.rsqrt(jnp.sum(key_in * key_in, axis=-1, keepdims=True) + EPSILON)
    live_rows = live[:, :, None]
    write_gate = jax.nn.sigmoid(write_pre) * live_rows
    forget = -jnp.exp(rates)[None, None, :] * jax.nn.softplus(forget_pre) * live_rows
    cumulative = jnp.cumsum(forget, axis=1)
    cum_heads = jnp.transpose(cumulative, (0, 2, 1))
    positions = jnp.arange(block_len)
    causal = positions[:, None] >= positions[None, :]
    strict = positions[:, None] > positions[None, :]
    differ = jnp.minimum(cum_heads[:, :, :, None] - cum_heads[:, :, None, :], 0.0)
    decay_mat = jnp.where(causal, jnp.exp(differ), 0.0)
    key_dots = jnp.einsum("sthd,suhd->shtu", key_unit, key_unit, precision=precise)
    write_heads = jnp.transpose(write_gate, (0, 2, 1))
    strict_part = jnp.where(strict, write_heads[:, :, :, None] * decay_mat * key_dots, 0.0)
    identity = jnp.eye(block_len, dtype=jnp.float32)
    squared = jnp.einsum("shtu,shuv->shtv", strict_part, strict_part, precision=precise)
    fourth = jnp.einsum("shtu,shuv->shtv", squared, squared, precision=precise)
    inverse = jnp.einsum(
        "shtu,shuv->shtv", identity - strict_part, identity + squared, precision=precise
    )
    inverse = jnp.einsum("shtu,shuv->shtv", inverse, identity + fourth, precision=precise)
    growth = jnp.exp(cumulative)
    target = jnp.einsum(
        "shtu,suhv->sthv", inverse, write_gate[..., None] * value, precision=precise
    )
    key_mix = jnp.einsum(
        "shtu,suhk->sthk", inverse, (write_gate * growth)[..., None] * key_unit, precision=precise
    )
    update = target - jnp.einsum("sthk,shkv->sthv", key_mix, state, precision=precise)
    scores = jnp.einsum("sthd,suhd->shtu", query_unit, key_unit, precision=precise) * decay_mat
    attend = jnp.einsum("sthk,shkv->sthv", query_unit * growth[..., None], state, precision=precise)
    attend = attend + jnp.einsum("shtu,suhv->sthv", scores, update, precision=precise)
    final_cum = cumulative[:, -1:, :]
    fading = jnp.exp(final_cum - cumulative)
    new_state = jnp.exp(final_cum[:, 0, :])[:, :, None, None] * state
    new_state = new_state + jnp.einsum(
        "sthk,sthv->shkv", key_unit * fading[..., None], update, precision=precise
    )
    normed = attend * lax.rsqrt(jnp.mean(attend * attend, axis=-1, keepdims=True) + EPSILON)
    normed = normed * jax.nn.silu(gating) * live[:, :, None, None]
    mixed_heads = normed.reshape(seq_count * block_len, head_count * head_size).astype(jnp.bfloat16)
    return (mixed_heads, new_state)


def per_device(
    tokens,
    lengths,
    state,
    gain_first,
    first_gate,
    first_up,
    first_down,
    gain_mix,
    query_weight,
    key_weight,
    value_weight,
    gating_weight,
    write_weight,
    forget_weight,
    forget_rate,
    out_weight,
    gain_second,
    second_gate,
    second_up,
    second_down,
):
    after_first = feed_forward(tokens, gain_first, first_gate, first_up, first_down)
    seq_count = lengths.shape[0]
    own_count = seq_count * BLK
    whole_rows = lax.all_gather(after_first, ("kv", "tp"), axis=1, tiled=True)
    scaled_all = (whole_rows.astype(jnp.float32) * gain_mix).astype(jnp.bfloat16)
    stacked = jnp.stack(
        [
            jnp.dot(scaled_all, matrix, preferred_element_type=jnp.float32)
            for matrix in (query_weight, key_weight, value_weight, gating_weight)
        ]
    )
    owned = lax.all_to_all(
        stacked.astype(jnp.bfloat16), ("kv", "tp"), split_axis=1, concat_axis=2, tiled=True
    ).astype(stacked.dtype)
    row_start = lax.axis_index(("kv", "tp")) * own_count
    own_values = lax.dynamic_slice_in_dim(whole_rows, row_start, own_count, 0).astype(jnp.float32)
    own_scaled = lax.dynamic_slice_in_dim(scaled_all, row_start, own_count, 0)
    mix_scale = lax.rsqrt(jnp.mean(own_values * own_values, axis=1, keepdims=True) + EPSILON)
    query = (owned[0] * mix_scale).reshape(seq_count, BLK, HEADS, HEAD)
    key_in = (owned[1] * mix_scale).reshape(seq_count, BLK, HEADS, HEAD)
    value = (owned[2] * mix_scale).reshape(seq_count, BLK, HEADS, HEAD)
    gating = (owned[3] * mix_scale).reshape(seq_count, BLK, HEADS, HEAD)
    write_pre = (
        jnp.dot(own_scaled, write_weight, preferred_element_type=jnp.float32) * mix_scale
    ).reshape(seq_count, BLK, HEADS)
    forget_pre = (
        jnp.dot(own_scaled, forget_weight, preferred_element_type=jnp.float32) * mix_scale
    ).reshape(seq_count, BLK, HEADS)
    positions = jnp.arange(BLK, dtype=jnp.int32)
    live = (positions[None, :] < lengths[:, None]).astype(jnp.float32)
    mixed_heads, new_state = delta_block(
        query, key_in, value, gating, write_pre, forget_pre, forget_rate, live, state
    )
    half_cols = mixed_heads.shape[1] // 2
    portion = lax.all_gather(mixed_heads, ("kv", "tp"), axis=0, tiled=True)
    first_half = jnp.dot(
        portion[:, :half_cols], out_weight[:half_cols], preferred_element_type=jnp.float32
    ).astype(jnp.bfloat16)
    second_half = jnp.dot(
        portion[:, half_cols:], out_weight[half_cols:], preferred_element_type=jnp.float32
    ).astype(jnp.bfloat16)
    first_half, second_half = lax.optimization_barrier((first_half, second_half))
    mixed_sum = first_half.astype(jnp.float32) + second_half.astype(jnp.float32)
    after_mix = (after_first.astype(jnp.float32) + mixed_sum).astype(jnp.bfloat16)
    mixed_out = feed_forward(after_mix, gain_second, second_gate, second_up, second_down)
    return (mixed_out, new_state)


F32 = jnp.float32
BF16 = jnp.bfloat16
MESH = pl.DeviceIdType.MESH
VMEM_LIMIT = 58 * 1024 * 1024


def fused_kernel(
    kv_size,
    channels,
    tokens_hbm,
    lengths_hbm,
    gains1_hbm,
    gains_mix_hbm,
    gains2_hbm,
    rates_hbm,
    state_hbm,
    gate1_hbm,
    up1_hbm,
    down1_hbm,
    query_hbm,
    key_hbm,
    value_hbm,
    gating_hbm,
    write_hbm,
    forget_hbm,
    out_hbm,
    gate2_hbm,
    up2_hbm,
    down2_hbm,
    mixed_out_ref,
    state_out,
    units1,
    down1,
    units2,
    down2,
    proj,
    out_w,
    small_w,
    state,
    state_high,
    state_low,
    gains1_ref,
    gains_mix_ref,
    gains2_ref,
    rates_ref,
    tokens_ref,
    length_ref,
    lens_all,
    picked,
    entered,
    unit_acc,
    live_acc,
    dead_acc,
    proj_acc,
    small_acc,
    middle,
    second_in,
    heads_send,
    heads_recv,
    red_send,
    red_recv,
    part_send,
    part_recv,
    small_recv,
    fin_send,
    fin_recv,
    own_send,
    own_recv,
    load_sems,
    send_sems,
    recv_sems,
):
    kv = lax.axis_index("kv")
    tp = lax.axis_index("tp")
    devices = 2 * kv_size
    me = kv * 2 + tp
    cls = lax.rem(kv + tp, 2)
    rows, cols = tokens_ref.shape
    wide = 2 * cols
    slots = BLK // 2
    half = rows // 2
    pack = rows // 4
    hidden_local = gate1_hbm.shape[1]
    own_cols = pl.ds(pl.multiple_of(tp * cols, cols), cols)
    far_first = list(range(kv_size - 1, 0, -1))

    loads = {}

    def load(name, src, dst):
        loads[name] = pltpu.make_async_copy(src, dst, load_sems.at[len(loads)])

    def swapped(off):
        chip, bit = kv, 1
        while bit < kv_size:
            if off & bit:
                chip = chip + bit - 2 * bit * lax.rem(kv // bit, 2)
            bit *= 2
        return chip

    def core_of(chip, other):
        return lax.rem(chip + cls + other, 2)

    def chip_rows(chip):
        return pl.ds(pl.multiple_of(chip * wide, wide), wide)

    load("length", lengths_hbm, length_ref)
    load("tokens", tokens_hbm, tokens_ref)
    load("gains1", gains1_hbm, gains1_ref)
    for off in range(kv_size):
        at = chip_rows(swapped(off))
        load(f"gate1{off}", gate1_hbm.at[at, :], units1.at[at, 0:hidden_local])
        load(f"up1{off}", up1_hbm.at[at, :], units1.at[at, hidden_local : 2 * hidden_local])
    early = list(loads)
    load("down1", down1_hbm, down1)
    for kind, ref in enumerate((query_hbm, key_hbm, value_hbm, gating_hbm)):
        at = pl.ds(pl.multiple_of(kind * wide + tp * cols, cols), cols)
        load(f"proj{kind}", ref, proj.at[:, at])
    load("write", write_hbm, small_w.at[0:HEADS])
    load("forget", forget_hbm, small_w.at[HEADS : 2 * HEADS])
    load("gains_mix", gains_mix_hbm, gains_mix_ref)
    load("rates", rates_hbm, rates_ref)
    load("out", out_hbm, out_w.at[:, own_cols])
    load("state", state_hbm.at[0], state)
    load("gains2", gains2_hbm, gains2_ref)
    load("gate2", gate2_hbm, units2.at[:, 0:hidden_local])
    load("up2", up2_hbm, units2.at[:, hidden_local : 2 * hidden_local])
    load("down2", down2_hbm, down2)
    late = [name for name in loads if name not in early]
    for name in early[:2]:
        loads[name].start()

    barrier = pltpu.get_barrier_semaphore()
    for off in range(1, devices):
        peer = lax.rem(me + off, devices)
        pl.semaphore_signal(
            barrier,
            inc=1,
            device_id={"kv": peer // 2, "tp": lax.rem(peer, 2)},
            device_id_type=MESH,
        )
    for name in early[2:]:
        loads[name].start()

    sent = []
    used = [0]

    def remote(src, dst, chip, core):
        copy = pltpu.make_async_remote_copy(
            src_ref=src,
            dst_ref=dst,
            send_sem=send_sems.at[used[0]],
            recv_sem=recv_sems.at[used[0]],
            device_id={"kv": chip, "tp": core},
            device_id_type=MESH,
        )
        used[0] += 1
        copy.start()
        sent.append(copy)
        return copy

    def to_class(src, dst):
        copies = {}
        for off in far_first:
            chip = swapped(off)
            copies[off] = remote(src(off), dst(off), chip, core_of(chip, 0))
        return copies

    def to_all(src, dst):
        copies = {}
        for off in far_first + [0]:
            chip = swapped(off)
            for other in (0, 1):
                if off or other:
                    core = core_of(chip, other)
                    copies[off, other] = remote(
                        src(off, other, chip * 2 + core), dst(off, other), chip, core
                    )
        return copies

    def to_partner(src, dst):
        return remote(src, dst, kv, 1 - tp)

    def iota(shape, axis):
        return lax.broadcasted_iota(jnp.int32, shape, axis)

    def dot(a, b):
        return jnp.dot(a, b, preferred_element_type=F32)

    def one_hot(mask):
        return jnp.where(mask, 1.0, 0.0).astype(BF16)

    row = iota((rows, rows), 0)
    col = iota((rows, rows), 1)
    at_class = lax.rem(row, half)
    at_seq = at_class // slots
    which = lax.rem(cls + row // half + at_seq, 2)
    picks = one_hot(col == at_seq * BLK + 2 * lax.rem(at_class, slots) + which)
    small_w[2 * HEADS :] = jnp.zeros((HEAD - 2 * HEADS, channels), BF16)
    with jax.named_scope("small_wait"):
        loads["length"].wait()
        loads["tokens"].wait()
    lens_all[me] = jnp.broadcast_to(length_ref[...], (1, HEAD))
    chosen = dot(picks, tokens_ref[...]).astype(BF16)
    picked[...] = chosen.reshape(2, half, cols)
    entered[me] = chosen[:half]
    with jax.named_scope("barrier"):
        pl.semaphore_wait(barrier, devices - 1)
    len_copies = to_all(lambda off, other, peer: lens_all.at[me], lambda off, other: lens_all.at[me])
    copies = to_all(lambda off, other, peer: picked.at[other], lambda off, other: entered.at[me])
    for name in late:
        loads[name].start()

    def ffn_slot(acc, units, gain_ref, chip, portion, first):
        at = chip_rows(chip)
        values = portion.astype(F32)
        scaled = (values * gain_ref[:, at]).astype(BF16)
        term = dot(scaled, units[at, :])
        if first:
            acc[...] = term
        else:
            acc[...] += term
        return jnp.sum(values * values, axis=1, keepdims=True)

    def finish(acc, squares):
        row_scale = lax.rsqrt(squares / channels + EPSILON)
        gate = acc[:, 0:hidden_local] * row_scale
        up = acc[:, hidden_local : 2 * hidden_local] * row_scale
        return (jax.nn.silu(gate) * up).astype(BF16)

    def lengths_by(seq):
        found = jnp.zeros(seq.shape, jnp.int32)
        for index in range(devices):
            found = jnp.where(seq == index, lens_all[index], found)
        return found

    def is_live(seq, slot, klass):
        return 2 * slot + lax.rem(klass + seq, 2) < lengths_by(seq)

    def live_column(klass):
        at = iota((half, HEAD), 0)
        return jnp.where(is_live(at // slots, lax.rem(at, slots), klass), 1.0, 0.0)

    def live_row(klass):
        at = iota((1, HEAD), 1)
        live = is_live(at // slots, lax.rem(at, slots), klass) & (at < half)
        return jnp.where(live, 1.0, 0.0)

    def place_lanes(seq, slot, column):
        target = seq * slots + slot
        before = jnp.sum(
            jnp.where(iota((half, HEAD), 0) < target, column, 0.0), axis=0, keepdims=True
        )
        count = jnp.sum(column, axis=0, keepdims=True)
        rest = count + target.astype(F32) - before
        return jnp.where(is_live(seq, slot, cls), before, rest).astype(jnp.int32)

    def place_rows(seq, slot, klass, flags):
        target = seq * slots + slot
        before = jnp.sum(
            jnp.where(iota(seq.shape, 1) < target, flags, 0.0), axis=1, keepdims=True
        )
        count = jnp.sum(flags, axis=1, keepdims=True)
        rest = count + target.astype(F32) - before
        return jnp.where(is_live(seq, slot, klass), before, rest).astype(jnp.int32)

    def chip_tokens(chip):
        return jnp.concatenate([entered[chip * 2], entered[chip * 2 + 1]], axis=1)

    loads["gains1"].wait()
    squares = jnp.zeros((half, 1), F32)
    with jax.named_scope("gather0"):
        for off in range(kv_size):
            for other in (0, 1):
                if off or other:
                    copies[off, other].wait_recv()
            loads[f"gate1{off}"].wait()
            loads[f"up1{off}"].wait()
            chip = swapped(off)
            if off == kv_size - 1:
                with jax.named_scope("order"):
                    for copy in len_copies.values():
                        copy.wait_recv()
                    column = live_column(cls)
                    lane = iota((1, HEAD), 1)
                    place = place_lanes(
                        jnp.minimum(lane // slots, devices - 1), lax.rem(lane, slots), column
                    )
                    reorder = one_hot(iota((half, HEAD), 0) == place)[:, :half]
            squares = squares + ffn_slot(
                unit_acc, units1, gains1_ref, chip, chip_tokens(chip), off == 0
            )
    with jax.named_scope("finish0"):
        hidden = dot(reorder, finish(unit_acc, squares)).astype(BF16)
    with jax.named_scope("down_wait"):
        loads["down1"].wait()
    with jax.named_scope("down0"):
        copies = {}
        for off in far_first + [0]:
            chip = swapped(off)
            own_term = dot(hidden, down1[:, chip_rows(chip)])
            if off:
                red_send[0, off] = own_term[:pack].astype(BF16)
                red_send[1, off] = own_term[pack:].astype(BF16)
                copies[0, off] = remote(
                    red_send.at[0, off], red_recv.at[0, off], chip, core_of(chip, 0)
                )
        for off in far_first:
            chip = swapped(off)
            copies[1, off] = remote(
                red_send.at[1, off], red_recv.at[1, off], chip, core_of(chip, 0)
            )
    with jax.named_scope("exchange"):
        proj_copies = []
        for kind in range(4):
            loads[f"proj{kind}"].wait()
            at = pl.ds(pl.multiple_of(kind * wide + tp * cols, cols), cols)
            proj_copies.append(to_partner(proj.at[:, at], proj.at[:, at]))
        loads["out"].wait()
        out_copy = to_partner(out_w.at[:, own_cols], out_w.at[:, own_cols])
    with jax.named_scope("tables"):
        residual = dot(reorder, chip_tokens(kv))
        flags = live_row(cls)
        other_flags = live_row(1 - cls)
        at = iota((devices * 2 * BLK, HEAD), 0)
        slot = lax.rem(at, slots)
        place = place_rows(at // (2 * BLK), slot, cls, flags)
        kind = lax.rem(at // slots, 4)
        kind = kind + cls * (1 - 2 * lax.rem(kind, 2))
        lane = iota((devices * 2 * BLK, HEAD), 1)
        spread = one_hot(
            (lane // pack == kind) & (lax.rem(lane, pack) == place) & (lane < 4 * pack)
        )[:, : 4 * pack]
        lane = iota((1, devices * 2 * BLK), 1)
        place = place_lanes(lane // (2 * BLK), lax.rem(lane, slots), column)
        at = iota((kv_size * pack, devices * 2 * BLK), 0)
        chip_at = lax.rem(iota((kv_size * pack, devices * 2 * BLK), 1) // slots, kv_size)
        gather_heads = one_hot((at // pack == chip_at) & (lax.rem(at, pack) == place))
        at = iota((BLK, HEAD), 0)
        klass = at // slots
        place = place_rows(
            jnp.zeros((BLK, HEAD), jnp.int32) + me,
            lax.rem(at, slots),
            klass,
            jnp.where(klass == cls, flags, other_flags),
        )
        lane = iota((BLK, HEAD), 1)
        pick_small = jnp.where(
            (lax.rem(lane // pack + cls, 2) == klass)
            & (lax.rem(lane, pack) == place)
            & (lane < 2 * pack),
            1.0,
            0.0,
        )[:, : 2 * pack]
        at = iota((rows, HEAD), 0)
        seq, token = at // BLK, lax.rem(at, BLK)
        klass = lax.rem(seq + token, 2)
        place = place_rows(seq, token // 2, klass, jnp.where(klass == cls, flags, other_flags))
        lane = iota((rows, HEAD), 1)
        restore = one_hot(
            (lax.rem(lane // half + cls, 2) == klass)
            & (lax.rem(lane, half) == place)
            & (lane < rows)
        )[:, :rows]
    with jax.named_scope("statecut"):
        loads["state"].wait()
        for head in range(HEADS):
            high = state[head].astype(BF16)
            state_high[head] = high
            state_low[head] = (state[head] - high.astype(F32)).astype(BF16)
    gathered = []
    for group in range(2):
        with jax.named_scope(f"red0_{group}"):
            at = slice(group * pack, (group + 1) * pack)
            for off in far_first:
                copies[group, off].wait_recv()
            total = own_term[at]
            for off in far_first:
                total = total + red_recv[group, off].astype(F32)
            middle[group, kv] = (residual[at] + 0.5 * total).astype(BF16)
            gathered.append(
                to_class(
                    lambda off: middle.at[group, kv], lambda off: middle.at[group, kv]
                )
            )

    with jax.named_scope("proj_wait"):
        for copy in proj_copies:
            copy.wait_recv()
        for name in ("write", "forget", "gains_mix", "rates"):
            loads[name].wait()
    squares = jnp.zeros((pack, 1), F32)
    with jax.named_scope("gather1"):
        for off in range(kv_size):
            if off:
                gathered[0][off].wait_recv()
            chip = swapped(off)
            at = chip_rows(chip)
            values = middle[0, chip].astype(F32)
            squares = squares + jnp.sum(values * values, axis=1, keepdims=True)
            scaled = (values * gains_mix_ref[:, at]).astype(BF16)
            term = dot(scaled, proj[at, :])
            small_term = lax.dot_general(
                scaled, small_w[:, at], (((1,), (1,)), ((), ())), preferred_element_type=F32
            )
            if off == 0:
                proj_acc[...] = term
                small_acc[0] = small_term
            else:
                proj_acc[...] += term
                small_acc[0] += small_term
    with jax.named_scope("partsend"):
        mix_scale = lax.rsqrt(squares / channels + EPSILON)
        small_acc[0] = small_acc[0] * mix_scale
        small_copy = to_partner(small_acc.at[0], small_recv.at[0])
        projected = (proj_acc[...] * mix_scale).astype(BF16)
        stacked = jnp.concatenate(
            [projected[:, kind * wide : (kind + 1) * wide] for kind in range(4)], axis=0
        )
        part_send[...] = dot(spread, stacked).astype(BF16).reshape(devices, 2 * BLK, wide)
        part_copies = to_all(
            lambda off, other, peer: part_send.at[peer],
            lambda off, other: part_recv.at[kv, cls],
        )
        part_recv[kv, cls] = part_send[me]

    with jax.named_scope("dead_units"):
        loads["gains2"].wait()
        loads["gate2"].wait()
        loads["up2"].wait()
        squares = jnp.zeros((pack, 1), F32)
        for off in range(kv_size):
            if off:
                gathered[1][off].wait_recv()
            chip = swapped(off)
            squares = squares + ffn_slot(
                dead_acc, units2, gains2_ref, chip, middle[1, chip], off == 0
            )
        dead_hidden = finish(dead_acc, squares)

    def cut_terms(a):
        high = a.astype(BF16).astype(F32)
        return high, a - high

    def dot_fine(a, b, across=False):
        high_a, low_a = cut_terms(a)
        high_b, low_b = cut_terms(b)
        axis = 1 if across else 0
        left = jnp.concatenate([high_a, high_a, low_a], axis=1).astype(BF16)
        right = jnp.concatenate([high_b, low_b, high_b], axis=axis).astype(BF16)
        return lax.dot_general(
            left, right, (((1,), (axis,)), ((), ())), preferred_element_type=F32
        )

    with jax.named_scope("premix"):
        small_copy.wait_recv()
        small_all = jnp.concatenate([small_acc[0], small_recv[0]], axis=0)
        high, low = cut_terms(small_all)
        picked_small = dot(pick_small.astype(BF16), high.astype(BF16)) + dot(
            pick_small.astype(BF16), low.astype(BF16)
        )
        write_pre = picked_small[:, 0:HEADS]
        forget_pre = picked_small[:, HEADS : 2 * HEADS]

        size = HEADS * BLK

        def token_of(at):
            at = lax.rem(at, BLK)
            return 2 * lax.rem(at, slots) + lax.rem(at // slots + me, 2)

        row = iota((size, size), 0)
        col = iota((size, size), 1)
        same = (row // BLK) == (col // BLK)
        causal = same & (token_of(row) >= token_of(col))
        strict = same & (token_of(row) > token_of(col))
        diagonal = row == col
        identity = jnp.where(diagonal, 1.0, 0.0)
        pick = iota((size, HEADS), 0) // BLK == iota((size, HEADS), 1)

        def as_column(block):
            return jnp.sum(jnp.where(pick, block, 0.0), axis=1, keepdims=True)

        def to_row(column):
            return jnp.sum(jnp.where(diagonal, column, 0.0), axis=0, keepdims=True)

        live = jnp.where(token_of(iota((size, 1), 0)) < length_ref[...], 1.0, 0.0)
        write_col = as_column(jnp.concatenate([write_pre] * HEADS, axis=0))
        forget_col = as_column(jnp.concatenate([forget_pre] * HEADS, axis=0))
        rate_col = as_column(jnp.broadcast_to(rates_ref[...], (size, HEADS)))
        write_gate = jax.nn.sigmoid(write_col) * live
        softplus = jnp.maximum(forget_col, 0.0) + jnp.log1p(jnp.exp(-jnp.abs(forget_col)))
        forget = -jnp.exp(rate_col) * softplus * live
        forget_row = to_row(forget)
        cumulative = jnp.sum(jnp.where(causal, forget_row, 0.0), axis=1, keepdims=True)
        final = jnp.sum(jnp.where(same, forget_row, 0.0), axis=1, keepdims=True)
        decay = jnp.where(
            causal, jnp.exp(jnp.minimum(cumulative - to_row(cumulative), 0.0)), 0.0
        )
        growth = jnp.exp(cumulative)
        fading = jnp.exp(final - cumulative)
        shrink = jnp.exp(final)

    with jax.named_scope("partwait"):
        for copy in part_copies.values():
            copy.wait_recv()
    scope = jax.named_scope("mix")
    scope.__enter__()
    upper = iota((BLK, wide), 0) < slots

    def by_head(pair):
        ahead, behind = [], []
        for chip in range(kv_size):
            at = slice(pair * BLK, (pair + 1) * BLK)
            mine = part_recv[chip, 0, at].astype(F32)
            theirs = part_recv[chip, 1, at].astype(F32)
            front = jnp.where(upper, mine, theirs)
            back = pltpu.roll(jnp.where(upper, theirs, mine), slots, 0)
            for start in range(0, wide, HEAD):
                ahead.append(front[:, start : start + HEAD])
                behind.append(back[:, start : start + HEAD])
        return jnp.concatenate(ahead, axis=0), jnp.concatenate(behind, axis=0)

    query, key_in = by_head(0)
    value, gating = by_head(1)
    query_unit = (
        query
        * lax.rsqrt(jnp.sum(query * query, axis=1, keepdims=True) + EPSILON)
        * (1.0 / math.sqrt(HEAD))
    )
    key_unit = key_in * lax.rsqrt(jnp.sum(key_in * key_in, axis=1, keepdims=True) + EPSILON)
    products = dot_fine(jnp.concatenate([key_unit, query_unit], axis=0), key_unit, True)
    lower = products[:size]
    lower = jnp.where(strict, write_gate * decay * lower, 0.0)
    squared = dot_fine(lower, lower)
    fourth = dot_fine(squared, squared)
    inverse = dot_fine(identity - lower, identity + squared)
    inverse = dot_fine(inverse, identity + fourth)
    key_grown = (write_gate * growth) * key_unit
    query_grown = query_unit * growth
    scores = products[size:] * decay

    key_terms, query_terms = [], []
    for head in range(HEADS):
        at = slice(head * BLK, (head + 1) * BLK)
        high, low = cut_terms(jnp.concatenate([key_grown[at], query_grown[at]], axis=0))
        both = jnp.concatenate([high, low], axis=0).astype(BF16)
        result = dot(both, state_high[head])
        result = result[: 2 * BLK] + result[2 * BLK :]
        result = result + dot(both[: 2 * BLK], state_low[head])
        key_terms.append(result[:BLK])
        query_terms.append(result[BLK:])
    update = dot_fine(inverse, write_gate * value - jnp.concatenate(key_terms, axis=0))
    attend = jnp.concatenate(query_terms, axis=0) + dot_fine(scores, update)
    normed = attend * lax.rsqrt(jnp.mean(attend * attend, axis=1, keepdims=True) + EPSILON)
    normed = normed * jax.nn.silu(gating) * live

    per_chip = wide // HEAD

    def lanes_of(chip):
        first = chip * per_chip
        return jnp.concatenate(
            [normed[(first + at) * BLK : (first + at + 1) * BLK] for at in range(per_chip)], axis=1
        )

    fronts, backs = [], []
    for chip in range(0, kv_size, 2):
        even, odd = lanes_of(chip), lanes_of(chip + 1)
        fronts.append(jnp.where(upper, even, pltpu.roll(odd, slots, 0)))
        backs.append(jnp.where(upper, pltpu.roll(even, slots, 0), odd))
    heads_send[0] = jnp.concatenate(fronts, axis=0).astype(BF16)
    heads_send[1] = jnp.concatenate(backs, axis=0).astype(BF16)
    copies = to_all(
        lambda off, other, peer: heads_send.at[lax.rem(cls + other, 2)],
        lambda off, other: heads_recv.at[me],
    )
    heads_recv[me] = heads_send[cls]
    scope.__exit__(None, None, None)

    with jax.named_scope("newstate"):
        faded = key_unit * fading
        for head in range(HEADS):
            at = slice(head * BLK, (head + 1) * BLK)
            key_high, key_low = cut_terms(faded[at])
            value_high, value_low = cut_terms(update[at])
            outer = lax.dot_general(
                jnp.concatenate([key_high, key_high, key_low], axis=0).astype(BF16),
                jnp.concatenate([value_high, value_low, value_high], axis=0).astype(BF16),
                (((0,), (0,)), ((), ())),
                preferred_element_type=F32,
            )
            state_out[0, head] = shrink[head * BLK : head * BLK + 1] * state[head] + outer

    def hand_over(group, hidden, source):
        outgoing = {}

        def term_of(chip, core):
            at = pl.ds(pl.multiple_of((chip * 2 + core) * cols, cols), cols)
            return dot(hidden, down2[:, at])

        for off in far_first:
            chip = swapped(off)
            for other in (0, 1):
                core = core_of(chip, other)
                fin_send[group, off, other] = term_of(chip, core).astype(BF16)
                outgoing[off, other] = remote(
                    fin_send.at[group, off, other], fin_recv.at[group, off, other], chip, core
                )
        theirs = pl.ds(pl.multiple_of((1 - tp) * cols, cols), cols)
        own_send[group] = source[:, theirs].astype(F32) + 0.5 * term_of(kv, 1 - tp)
        outgoing[0, 1] = to_partner(own_send.at[group], own_recv.at[group])
        own = source[:, own_cols].astype(F32) + 0.5 * term_of(kv, tp)
        return own, outgoing

    def take_in(group, own, outgoing):
        outgoing[0, 1].wait_recv()
        sums = [own, own_recv[group]]
        for other in (0, 1):
            total = None
            for off in far_first[::-1]:
                outgoing[off, other].wait_recv()
                term = fin_recv[group, off, other].astype(F32)
                total = term if total is None else total + term
            sums[other] = sums[other] + 0.5 * total
        return [total.astype(BF16) for total in sums]

    with jax.named_scope("dead_down"):
        loads["down2"].wait()
        dead_own, dead_out = hand_over(1, dead_hidden, middle.at[1, kv])

    with jax.named_scope("gather2"):
        for copy in copies.values():
            copy.wait_recv()
        out_copy.wait_recv()
    with jax.named_scope("outproj"):
        blocks = heads_recv[...].reshape(devices * 2 * BLK, wide)
        mixed = dot(gather_heads, blocks).astype(BF16)
        terms = []
        for part in range(2):
            chips = range(part * kv_size // 2, (part + 1) * kv_size // 2)
            left = jnp.concatenate([mixed[chip * pack : (chip + 1) * pack] for chip in chips], axis=1)
            right = out_w[chips[0] * wide : (chips[-1] + 1) * wide, :]
            terms.append(dot(left, right).astype(BF16).astype(F32))
        second_in[kv] = (middle[0, kv].astype(F32) + (terms[0] + terms[1])).astype(BF16)
        copies = to_class(lambda off: second_in.at[kv], lambda off: second_in.at[kv])

    squares = jnp.zeros((pack, 1), F32)
    with jax.named_scope("gather3"):
        for off in range(kv_size):
            if off:
                copies[off].wait_recv()
            chip = swapped(off)
            squares = squares + ffn_slot(
                live_acc, units2, gains2_ref, chip, second_in[chip], off == 0
            )
    with jax.named_scope("finish1"):
        hidden = finish(live_acc, squares)
    with jax.named_scope("down1"):
        live_own, live_out = hand_over(0, hidden, second_in.at[kv])
    with jax.named_scope("dead_in"):
        dead_sums = take_in(1, dead_own, dead_out)
    with jax.named_scope("live_in"):
        live_sums = take_in(0, live_own, live_out)
    with jax.named_scope("last"):
        packed = jnp.concatenate(
            [live_sums[0], dead_sums[0], live_sums[1], dead_sums[1]], axis=0
        )
        mixed_out_ref[...] = dot(restore, packed).astype(BF16)
    with jax.named_scope("tail"):
        for copy in sent:
            copy.wait_send()


def fused_call(mesh, *args):
    (
        tokens, lengths, state, gain_first, first_gate, first_up, first_down, gain_mix,
        query_weight, key_weight, value_weight, gating_weight, write_weight, forget_weight,
        forget_rate, out_weight, gain_second, second_gate, second_up, second_down,
    ) = args
    kv_size = mesh.shape["kv"]
    devices = kv_size * mesh.shape["tp"]
    rows, cols = tokens.shape
    wide = 2 * cols
    channels = gain_first.shape[0]
    hidden_local = first_gate.shape[1]
    half, pack = rows // 2, rows // 4
    in_hbm = pl.BlockSpec(memory_space=pltpu.HBM)
    in_vmem = pl.BlockSpec(memory_space=pltpu.VMEM)
    dma = pltpu.SemaphoreType.DMA
    remotes = 7 * (devices - 1) + 6 * (kv_size - 1) + 10
    operands = (
        tokens, lengths.reshape(1, 1), gain_first.reshape(1, -1), gain_mix.reshape(1, -1),
        gain_second.reshape(1, -1), forget_rate.reshape(1, -1), state,
        first_gate, first_up, first_down, query_weight, key_weight, value_weight,
        gating_weight, write_weight.T, forget_weight.T, out_weight, second_gate, second_up,
        second_down,
    )
    operands = [
        array if array.dtype == jnp.int32 else pltpu.with_memory_space_constraint(array, pltpu.HBM)
        for array in operands
    ]
    mixed_out, new_state = pl.pallas_call(
        functools.partial(fused_kernel, kv_size, channels),
        out_shape=(
            pltpu.VMEM(tokens.shape, tokens.dtype),
            pltpu.VMEM(state.shape, state.dtype),
        ),
        in_specs=[in_hbm] * len(operands),
        out_specs=(in_vmem, in_vmem),
        scratch_shapes=[
            pltpu.VMEM((channels, 2 * hidden_local), BF16),
            pltpu.VMEM((hidden_local, channels), BF16),
            pltpu.VMEM((channels, 2 * hidden_local), BF16),
            pltpu.VMEM((hidden_local, channels), BF16),
            pltpu.VMEM((channels, 4 * wide), BF16),
            pltpu.VMEM((channels, wide), BF16),
            pltpu.VMEM((HEAD, channels), BF16),
            pltpu.VMEM(state.shape[1:], F32),
            pltpu.VMEM(state.shape[1:], BF16),
            pltpu.VMEM(state.shape[1:], BF16),
            pltpu.VMEM((1, channels), F32),
            pltpu.VMEM((1, channels), F32),
            pltpu.VMEM((1, channels), F32),
            pltpu.VMEM((1, HEADS), F32),
            pltpu.VMEM((rows, cols), BF16),
            pltpu.VMEM((1, 1), jnp.int32),
            pltpu.VMEM((devices, 1, HEAD), jnp.int32),
            pltpu.VMEM((2, half, cols), BF16),
            pltpu.VMEM((devices, half, cols), BF16),
            pltpu.VMEM((half, 2 * hidden_local), F32),
            pltpu.VMEM((pack, 2 * hidden_local), F32),
            pltpu.VMEM((pack, 2 * hidden_local), F32),
            pltpu.VMEM((pack, 4 * wide), F32),
            pltpu.VMEM((1, pack, HEAD), F32),
            pltpu.VMEM((2, kv_size, pack, wide), BF16),
            pltpu.VMEM((kv_size, pack, wide), BF16),
            pltpu.VMEM((2, 2 * BLK, wide), BF16),
            pltpu.VMEM((devices, 2 * BLK, wide), BF16),
            pltpu.VMEM((2, kv_size, pack, wide), BF16),
            pltpu.VMEM((2, kv_size, pack, wide), BF16),
            pltpu.VMEM((devices, 2 * BLK, wide), BF16),
            pltpu.VMEM((kv_size, 2, 2 * BLK, wide), BF16),
            pltpu.VMEM((1, pack, HEAD), F32),
            pltpu.VMEM((2, kv_size, 2, pack, cols), BF16),
            pltpu.VMEM((2, kv_size, 2, pack, cols), BF16),
            pltpu.VMEM((2, pack, cols), F32),
            pltpu.VMEM((2, pack, cols), F32),
            dma((3 + 2 * kv_size + 15,)),
            dma((remotes,)),
            dma((remotes,)),
        ],
        compiler_params=pltpu.CompilerParams(
            collective_id=0, has_side_effects=True, vmem_limit_bytes=VMEM_LIMIT
        ),
    )(*operands)
    return hand_out(mixed_out, new_state)


def hand_out_kernel(mixed, state, mixed_out_hbm, state_out_hbm, sems):
    puts = [
        pltpu.make_async_copy(mixed, mixed_out_hbm, sems.at[0]),
        pltpu.make_async_copy(state, state_out_hbm, sems.at[1]),
    ]
    for put in puts:
        put.start()
    for put in puts:
        put.wait()


def hand_out(mixed_out, new_state):
    in_hbm = pl.BlockSpec(memory_space=pltpu.HBM)
    in_vmem = pl.BlockSpec(memory_space=pltpu.VMEM)
    arrays = [
        pltpu.with_memory_space_constraint(array, pltpu.VMEM) for array in (mixed_out, new_state)
    ]
    return pl.pallas_call(
        hand_out_kernel,
        out_shape=tuple(jax.ShapeDtypeStruct(array.shape, array.dtype) for array in arrays),
        in_specs=[in_vmem, in_vmem],
        out_specs=(in_hbm, in_hbm),
        scratch_shapes=[pltpu.SemaphoreType.DMA((2,))],
        compiler_params=pltpu.CompilerParams(vmem_limit_bytes=8 * 1024 * 1024),
    )(*arrays)


def fits_fused(mesh, args):
    tokens, lengths, state, first_gate = args[0], args[1], args[2], args[4]
    rows, cols = tokens.shape
    kv_size = mesh.shape["kv"]
    devices = kv_size * mesh.shape["tp"]
    return (
        mesh.shape["tp"] == 2
        and mesh.shape["kv"] & (mesh.shape["kv"] - 1) == 0
        and lengths.shape[0] == 1
        and rows == devices * BLK
        and devices * 2 * BLK == HEAD
        and kv_size * BLK // 2 == 2 * BLK
        and devices * cols == HEADS * HEAD
        and cols % 256 == 0
        and first_gate.shape[1] % 128 == 0
        and state.shape[1:] == (HEADS, HEAD, HEAD)
    )


def solution(mesh):
    in_specs = (
        P("dp", ("kv", "tp")),
        P(("dp", "kv", "tp")),
        P(("dp", "kv", "tp"), None, None, None),
        P(),
        P(None, "kv"),
        P(None, "kv"),
        P("kv", None),
        P(),
        P(None, ("kv", "tp")),
        P(None, ("kv", "tp")),
        P(None, ("kv", "tp")),
        P(None, ("kv", "tp")),
        P(),
        P(),
        P(),
        P(None, ("kv", "tp")),
        P(),
        P(None, "kv"),
        P(None, "kv"),
        P("kv", None),
    )
    out_specs = (P("dp", ("kv", "tp")), P(("dp", "kv", "tp"), None, None, None))

    def body(*args):
        if fits_fused(mesh, args):
            return fused_call(mesh, *args)
        return per_device(*args)

    return jax.shard_map(
        body, mesh=mesh, in_specs=in_specs, out_specs=out_specs, check_vma=False
    )
```

time: 51.6 us -> 46.9 us (0.909)
  Pallas kernels: 50.1 us -> 45.5 us
    pallas_call x1, Pallas kernels: 48.1 us -> 44.5 us  [fused_call(): pl.pallas_call(functools.partial(fused_kernel, kv_size, channels), out_sh...]
    pallas_call x1, Pallas kernels: 2.02 us -> 1 us  [hand_out(): pl.pallas_call(hand_out_kernel, out_shape=tuple((jax.ShapeDtypeStruct(arr...]
where the time goes in v1:
time: 46.9 us; the launch traced here: 46.7 us
  Pallas kernels  45.5 us (97%)
  between operations  1.29 us (3%)
    pallas_call x1, Pallas kernels, fused_call(): pl.pallas_call(functools.partial(fused_kernel, kv_size, channels), out_sh...  44.5 us
    pallas_call x1, Pallas kernels, hand_out(): pl.pallas_call(hand_out_kernel, out_shape=tuple((jax.ShapeDtypeStruct(arr...  1 us

profile of v1, /device:TPU:0, one launch (start us, length us, event | category | flops | bytes accessed | tf_op | source)
XLA Modules:
  0.0 46.7 jit_solution(14962736191264649631)
XLA Ops:
  1.3 44.5 %shard_map.203 = (bf16[64,256]{1,0:T(8,128)(2,1)S(1)}, f32[1,16,128,128]{3,2,1,0:T(8,128)S(1)}) custom-call(bf16[64,256]{1,0:T(8,128)(2,1)} %tokens_hbm.1, s32[1,1]{1,0:T(1,128)} %bitcast.7.lengths_hbm, f32[1,2048]{1,0:T(1,128)} %bitcast.10, f32[1,2048]{1,0:T(1,128)} %bitcast.11, f32[1,2048]{1,0:T(1,128)} %bitcast.12, f32[1,16]{1,0:T(1,128)} %bitcast.13, ...), custom_call_target="tpu_custom_call" | custom-call | tf_op jit(solution)/shard_map/pallas_call | solution.py:867
  45.7 1.0 %shard_map.204 = (bf16[64,256]{1,0:T(8,128)(2,1)}, f32[1,16,128,128]{3,2,1,0:T(8,128)}) custom-call(bf16[64,256]{1,0:T(8,128)(2,1)S(1)} %get-tuple-element.4.mixed, f32[1,16,128,128]{3,2,1,0:T(8,128)S(1)} %get-tuple-element.5.state), custom_call_target="tpu_custom_call" | custom-call | tf_op jit(solution)/shard_map/pallas_call | solution.py:941

commit v2 on v1

--- a/solution.py
+++ b/solution.py
@@ -249,18 +249,31 @@
     pack = rows // 4
     hidden_local = gate1_hbm.shape[1]
     own_cols = pl.ds(pl.multiple_of(tp * cols, cols), cols)
-    far_first = list(range(kv_size - 1, 0, -1))
+    inner = lax.rem((kv + 1) // 2, 2)
+    near_first = [1, 2 + inner, 3 - inner]
+    far_first = near_first[::-1]
 
     loads = {}
 
-    def load(name, src, dst):
-        loads[name] = pltpu.make_async_copy(src, dst, load_sems.at[len(loads)])
+    def load(name, *pairs):
+        sem = load_sems.at[len(loads)]
+        loads[name] = [pltpu.make_async_copy(src, dst, sem) for src, dst in pairs]
+
+    def start(name):
+        for copy in loads[name]:
+            copy.start()
+
+    def loaded(name, ref=None):
+        if ref is None:
+            loads[name][0].wait()
+        else:
+            sem = load_sems.at[list(loads).index(name)]
+            pltpu.make_async_copy(ref, ref, sem).wait()
 
     def swapped(off):
-        chip, bit = kv, 1
+        chip, bit = 0, 1
         while bit < kv_size:
-            if off & bit:
-                chip = chip + bit - 2 * bit * lax.rem(kv // bit, 2)
+            chip = chip + bit * lax.rem(kv // bit + off // bit, 2)
             bit *= 2
         return chip
 
@@ -270,31 +283,42 @@
     def chip_rows(chip):
         return pl.ds(pl.multiple_of(chip * wide, wide), wide)
 
-    load("length", lengths_hbm, length_ref)
-    load("tokens", tokens_hbm, tokens_ref)
-    load("gains1", gains1_hbm, gains1_ref)
-    for off in range(kv_size):
+    def kind_cols(kind):
+        return pl.ds(pl.multiple_of(kind * wide + tp * cols, cols), cols)
+
+    load("length", (lengths_hbm, length_ref))
+    load("tokens", (tokens_hbm, tokens_ref))
+    load("gains1", (gains1_hbm, gains1_ref))
+    for index, off in enumerate([0] + near_first):
         at = chip_rows(swapped(off))
-        load(f"gate1{off}", gate1_hbm.at[at, :], units1.at[at, 0:hidden_local])
-        load(f"up1{off}", up1_hbm.at[at, :], units1.at[at, hidden_local : 2 * hidden_local])
+        load(
+            f"units1{index}",
+            (gate1_hbm.at[at, :], units1.at[at, 0:hidden_local]),
+            (up1_hbm.at[at, :], units1.at[at, hidden_local : 2 * hidden_local]),
+        )
     early = list(loads)
-    load("down1", down1_hbm, down1)
-    for kind, ref in enumerate((query_hbm, key_hbm, value_hbm, gating_hbm)):
-        at = pl.ds(pl.multiple_of(kind * wide + tp * cols, cols), cols)
-        load(f"proj{kind}", ref, proj.at[:, at])
-    load("write", write_hbm, small_w.at[0:HEADS])
-    load("forget", forget_hbm, small_w.at[HEADS : 2 * HEADS])
-    load("gains_mix", gains_mix_hbm, gains_mix_ref)
-    load("rates", rates_hbm, rates_ref)
-    load("out", out_hbm, out_w.at[:, own_cols])
-    load("state", state_hbm.at[0], state)
-    load("gains2", gains2_hbm, gains2_ref)
-    load("gate2", gate2_hbm, units2.at[:, 0:hidden_local])
-    load("up2", up2_hbm, units2.at[:, hidden_local : 2 * hidden_local])
-    load("down2", down2_hbm, down2)
+    load("down1", (down1_hbm, down1))
+    kinds = (query_hbm, key_hbm, value_hbm, gating_hbm)
+    load("proj", *[(ref, proj.at[:, kind_cols(kind)]) for kind, ref in enumerate(kinds)])
+    load(
+        "small",
+        (write_hbm, small_w.at[0:HEADS]),
+        (forget_hbm, small_w.at[HEADS : 2 * HEADS]),
+    )
+    load("gains_mix", (gains_mix_hbm, gains_mix_ref))
+    load("rates", (rates_hbm, rates_ref))
+    load("out", (out_hbm, out_w.at[:, own_cols]))
+    load("state", (state_hbm.at[0], state))
+    load("gains2", (gains2_hbm, gains2_ref))
+    load(
+        "units2",
+        (gate2_hbm, units2.at[:, 0:hidden_local]),
+        (up2_hbm, units2.at[:, hidden_local : 2 * hidden_local]),
+    )
+    load("down2", (down2_hbm, down2))
     late = [name for name in loads if name not in early]
     for name in early[:2]:
-        loads[name].start()
+        start(name)
 
     barrier = pltpu.get_barrier_semaphore()
     for off in range(1, devices):
@@ -306,46 +330,57 @@
             device_id_type=MESH,
         )
     for name in early[2:]:
-        loads[name].start()
-
-    sent = []
-    used = [0]
-
-    def remote(src, dst, chip, core):
+        start(name)
+
+    sends, receives, width = {}, {}, [0]
+
+    def remote(name, src, dst, chip, core, at=0, spread=1):
+        if name not in sends:
+            sends[name] = len(sends)
+            receives[name] = width[0]
+            width[0] += spread
         copy = pltpu.make_async_remote_copy(
             src_ref=src,
             dst_ref=dst,
-            send_sem=send_sems.at[used[0]],
-            recv_sem=recv_sems.at[used[0]],
+            send_sem=send_sems.at[sends[name]],
+            recv_sem=recv_sems.at[receives[name] + at],
             device_id={"kv": chip, "tp": core},
             device_id_type=MESH,
         )
-        used[0] += 1
         copy.start()
-        sent.append(copy)
-        return copy
-
-    def to_class(src, dst):
-        copies = {}
+
+    def of_phase(name, ref, at=0):
+        return pltpu.make_async_remote_copy(
+            src_ref=ref,
+            dst_ref=ref,
+            send_sem=send_sems.at[sends[name]],
+            recv_sem=recv_sems.at[receives[name] + at],
+            device_id={"kv": kv, "tp": 1 - tp},
+            device_id_type=MESH,
+        )
+
+    def arrived(name, ref, at=0):
+        of_phase(name, ref, at).wait_recv()
+
+    def to_class(name, src, dst, spread=1):
         for off in far_first:
             chip = swapped(off)
-            copies[off] = remote(src(off), dst(off), chip, core_of(chip, 0))
-        return copies
-
-    def to_all(src, dst):
-        copies = {}
+            remote(name, src(off), dst(off), chip, core_of(chip, 0), off if spread > 1 else 0, spread)
+
+    def to_all(name, src, dst, spread=1):
         for off in far_first + [0]:
             chip = swapped(off)
             for other in (0, 1):
-                if off or other:
-                    core = core_of(chip, other)
-                    copies[off, other] = remote(
-                        src(off, other, chip * 2 + core), dst(off, other), chip, core
-                    )
-        return copies
-
-    def to_partner(src, dst):
-        return remote(src, dst, kv, 1 - tp)
+                if other == 0 and isinstance(off, int) and off == 0:
+                    continue
+                core = core_of(chip, other)
+                remote(
+                    name, src(other, chip * 2 + core), dst(other), chip, core,
+                    off if spread > 1 else 0, spread,
+                )
+
+    def to_partner(name, src, dst):
+        remote(name, src, dst, kv, 1 - tp)
 
     def iota(shape, axis):
         return lax.broadcasted_iota(jnp.int32, shape, axis)
@@ -362,20 +397,20 @@
     at_seq = at_class // slots
     which = lax.rem(cls + row // half + at_seq, 2)
     picks = one_hot(col == at_seq * BLK + 2 * lax.rem(at_class, slots) + which)
-    small_w[2 * HEADS :] = jnp.zeros((HEAD - 2 * HEADS, channels), BF16)
     with jax.named_scope("small_wait"):
-        loads["length"].wait()
-        loads["tokens"].wait()
+        loaded("length")
+        loaded("tokens")
     lens_all[me] = jnp.broadcast_to(length_ref[...], (1, HEAD))
     chosen = dot(picks, tokens_ref[...]).astype(BF16)
     picked[...] = chosen.reshape(2, half, cols)
     entered[me] = chosen[:half]
     with jax.named_scope("barrier"):
         pl.semaphore_wait(barrier, devices - 1)
-    len_copies = to_all(lambda off, other, peer: lens_all.at[me], lambda off, other: lens_all.at[me])
-    copies = to_all(lambda off, other, peer: picked.at[other], lambda off, other: entered.at[me])
+    to_all("tokens", lambda other, peer: picked.at[other], lambda other: entered.at[me], kv_size)
+    to_all("lens", lambda other, peer: lens_all.at[me], lambda other: lens_all.at[me])
     for name in late:
-        loads[name].start()
+        start(name)
+    small_w[2 * HEADS :] = jnp.zeros((HEAD - 2 * HEADS, channels), BF16)
 
     def ffn_slot(acc, units, gain_ref, chip, portion, first):
         at = chip_rows(chip)
@@ -433,70 +468,65 @@
     def chip_tokens(chip):
         return jnp.concatenate([entered[chip * 2], entered[chip * 2 + 1]], axis=1)
 
-    loads["gains1"].wait()
+    loaded("gains1")
     squares = jnp.zeros((half, 1), F32)
-    with jax.named_scope("gather0"):
-        for off in range(kv_size):
-            for other in (0, 1):
-                if off or other:
-                    copies[off, other].wait_recv()
-            loads[f"gate1{off}"].wait()
-            loads[f"up1{off}"].wait()
-            chip = swapped(off)
-            if off == kv_size - 1:
-                with jax.named_scope("order"):
-                    for copy in len_copies.values():
-                        copy.wait_recv()
-                    column = live_column(cls)
-                    lane = iota((1, HEAD), 1)
-                    place = place_lanes(
-                        jnp.minimum(lane // slots, devices - 1), lax.rem(lane, slots), column
-                    )
-                    reorder = one_hot(iota((half, HEAD), 0) == place)[:, :half]
+    for index, off in enumerate([0] + near_first):
+        chip = swapped(off)
+        with jax.named_scope(f"tokens_wait{index}"):
+            if index:
+                arrived("tokens", entered.at[pl.ds(chip * 2, 2)], off)
+            else:
+                arrived("tokens", entered.at[kv * 2 + 1 - tp], off)
+            loaded(f"units1{index}", units1.at[chip_rows(chip), :])
+            if index == kv_size - 1:
+                arrived("lens", lens_all.at[pl.ds(0, devices - 1)])
+        with jax.named_scope(f"units_slot{index}"):
+            if index == kv_size - 1:
+                column = live_column(cls)
+                lane = iota((1, HEAD), 1)
+                place = place_lanes(
+                    jnp.minimum(lane // slots, devices - 1), lax.rem(lane, slots), column
+                )
+                reorder = one_hot(iota((half, HEAD), 0) == place)[:, :half]
             squares = squares + ffn_slot(
-                unit_acc, units1, gains1_ref, chip, chip_tokens(chip), off == 0
+                unit_acc, units1, gains1_ref, chip, chip_tokens(chip), index == 0
             )
+        if index == kv_size - 2:
+            with jax.named_scope("exchange"):
+                loaded("proj", proj.at[:, 0 : 4 * cols])
+                for kind in range(4):
+                    at = kind_cols(kind)
+                    to_partner("proj", proj.at[:, at], proj.at[:, at])
     with jax.named_scope("finish0"):
         hidden = dot(reorder, finish(unit_acc, squares)).astype(BF16)
     with jax.named_scope("down_wait"):
-        loads["down1"].wait()
+        loaded("down1")
     with jax.named_scope("down0"):
-        copies = {}
-        for off in far_first + [0]:
-            chip = swapped(off)
-            own_term = dot(hidden, down1[:, chip_rows(chip)])
-            if off:
-                red_send[0, off] = own_term[:pack].astype(BF16)
-                red_send[1, off] = own_term[pack:].astype(BF16)
-                copies[0, off] = remote(
-                    red_send.at[0, off], red_recv.at[0, off], chip, core_of(chip, 0)
-                )
         for off in far_first:
             chip = swapped(off)
-            copies[1, off] = remote(
-                red_send.at[1, off], red_recv.at[1, off], chip, core_of(chip, 0)
-            )
-    with jax.named_scope("exchange"):
-        proj_copies = []
-        for kind in range(4):
-            loads[f"proj{kind}"].wait()
-            at = pl.ds(pl.multiple_of(kind * wide + tp * cols, cols), cols)
-            proj_copies.append(to_partner(proj.at[:, at], proj.at[:, at]))
-        loads["out"].wait()
-        out_copy = to_partner(out_w.at[:, own_cols], out_w.at[:, own_cols])
+            term = dot(hidden, down1[:, chip_rows(chip)])
+            red_send[0, off] = term[:pack].astype(BF16)
+            red_send[1, off] = term[pack:].astype(BF16)
+            remote("red0", red_send.at[0, off], red_recv.at[0, off], chip, core_of(chip, 0))
+        own_term = dot(hidden, down1[:, chip_rows(kv)])
+        for off in far_first:
+            chip = swapped(off)
+            remote("red1", red_send.at[1, off], red_recv.at[1, off], chip, core_of(chip, 0))
+    with jax.named_scope("exchange_out"):
+        loaded("out")
+        to_partner("out", out_w.at[:, own_cols], out_w.at[:, own_cols])
     with jax.named_scope("tables"):
         residual = dot(reorder, chip_tokens(kv))
         flags = live_row(cls)
         other_flags = live_row(1 - cls)
-        at = iota((devices * 2 * BLK, HEAD), 0)
+        at = iota((rows, HEAD), 0)
         slot = lax.rem(at, slots)
-        place = place_rows(at // (2 * BLK), slot, cls, flags)
-        kind = lax.rem(at // slots, 4)
-        kind = kind + cls * (1 - 2 * lax.rem(kind, 2))
-        lane = iota((devices * 2 * BLK, HEAD), 1)
+        place = place_rows(at // BLK, slot, cls, flags)
+        kind = lax.rem(at // slots + cls, 2)
+        lane = iota((rows, HEAD), 1)
         spread = one_hot(
-            (lane // pack == kind) & (lax.rem(lane, pack) == place) & (lane < 4 * pack)
-        )[:, : 4 * pack]
+            (lane // pack == kind) & (lax.rem(lane, pack) == place) & (lane < 2 * pack)
+        )[:, : 2 * pack]
         lane = iota((1, devices * 2 * BLK), 1)
         place = place_lanes(lane // (2 * BLK), lax.rem(lane, slots), column)
         at = iota((kv_size * pack, devices * 2 * BLK), 0)
@@ -529,79 +559,78 @@
             & (lane < rows)
         )[:, :rows]
     with jax.named_scope("statecut"):
-        loads["state"].wait()
+        loaded("state")
         for head in range(HEADS):
             high = state[head].astype(BF16)
             state_high[head] = high
             state_low[head] = (state[head] - high.astype(F32)).astype(BF16)
-    gathered = []
     for group in range(2):
         with jax.named_scope(f"red0_{group}"):
             at = slice(group * pack, (group + 1) * pack)
-            for off in far_first:
-                copies[group, off].wait_recv()
+            arrived(f"red{group}", red_recv.at[group, pl.ds(1, kv_size - 1)])
             total = own_term[at]
-            for off in far_first:
+            for off in range(1, kv_size):
                 total = total + red_recv[group, off].astype(F32)
             middle[group, kv] = (residual[at] + 0.5 * total).astype(BF16)
-            gathered.append(
-                to_class(
-                    lambda off: middle.at[group, kv], lambda off: middle.at[group, kv]
-                )
+            to_class(
+                f"middle{group}",
+                lambda off: middle.at[group, kv],
+                lambda off: middle.at[group, kv],
+                1 if group else kv_size,
             )
 
     with jax.named_scope("proj_wait"):
-        for copy in proj_copies:
-            copy.wait_recv()
-        for name in ("write", "forget", "gains_mix", "rates"):
-            loads[name].wait()
+        arrived("proj", proj.at[:, 0 : 4 * cols])
+        loaded("small", small_w.at[0 : 2 * HEADS])
+        loaded("gains_mix")
+        loaded("rates")
     squares = jnp.zeros((pack, 1), F32)
-    with jax.named_scope("gather1"):
-        for off in range(kv_size):
-            if off:
-                gathered[0][off].wait_recv()
-            chip = swapped(off)
-            at = chip_rows(chip)
+    for index, off in enumerate([0] + near_first):
+        chip = swapped(off)
+        at = chip_rows(chip)
+        with jax.named_scope(f"middle_wait{index}"):
+            if index:
+                arrived("middle0", middle.at[0, chip], off)
+        with jax.named_scope(f"proj_slot{index}"):
             values = middle[0, chip].astype(F32)
             squares = squares + jnp.sum(values * values, axis=1, keepdims=True)
             scaled = (values * gains_mix_ref[:, at]).astype(BF16)
-            term = dot(scaled, proj[at, :])
             small_term = lax.dot_general(
                 scaled, small_w[:, at], (((1,), (1,)), ((), ())), preferred_element_type=F32
             )
-            if off == 0:
-                proj_acc[...] = term
+            if index == 0:
+                proj_acc[...] = dot(scaled, proj[at, :])
                 small_acc[0] = small_term
-            else:
-                proj_acc[...] += term
+            elif index < kv_size - 1:
+                proj_acc[...] += dot(scaled, proj[at, :])
                 small_acc[0] += small_term
     with jax.named_scope("partsend"):
         mix_scale = lax.rsqrt(squares / channels + EPSILON)
-        small_acc[0] = small_acc[0] * mix_scale
-        small_copy = to_partner(small_acc.at[0], small_recv.at[0])
-        projected = (proj_acc[...] * mix_scale).astype(BF16)
-        stacked = jnp.concatenate(
-            [projected[:, kind * wide : (kind + 1) * wide] for kind in range(4)], axis=0
-        )
-        part_send[...] = dot(spread, stacked).astype(BF16).reshape(devices, 2 * BLK, wide)
-        part_copies = to_all(
-            lambda off, other, peer: part_send.at[peer],
-            lambda off, other: part_recv.at[kv, cls],
-        )
-        part_recv[kv, cls] = part_send[me]
+        for pair in range(2):
+            lanes = slice(pair * 2 * wide, (pair + 1) * 2 * wide)
+            projected = proj_acc[:, lanes] + dot(scaled, proj[at, lanes])
+            projected = (projected * mix_scale).astype(BF16)
+            stacked = jnp.concatenate([projected[:, :wide], projected[:, wide:]], axis=0)
+            part = dot(spread, stacked).astype(BF16)
+            part_send[pair] = part.reshape(devices, BLK, wide)
+            to_all(
+                f"part{pair}",
+                lambda other, peer: part_send.at[pair, peer],
+                lambda other: part_recv.at[pair, kv, cls],
+            )
+            if pair == 0:
+                small_acc[0] = (small_acc[0] + small_term) * mix_scale
+                to_partner("small", small_acc.at[0], small_recv.at[0])
+        for pair in range(2):
+            part_recv[pair, kv, cls] = part_send[pair, me]
 
     with jax.named_scope("dead_units"):
-        loads["gains2"].wait()
-        loads["gate2"].wait()
-        loads["up2"].wait()
-        squares = jnp.zeros((pack, 1), F32)
-        for off in range(kv_size):
-            if off:
-                gathered[1][off].wait_recv()
-            chip = swapped(off)
-            squares = squares + ffn_slot(
-                dead_acc, units2, gains2_ref, chip, middle[1, chip], off == 0
-            )
+        loaded("gains2")
+        loaded("units2", units2)
+        arrived("middle1", middle.at[1, pl.ds(0, kv_size - 1)])
+        values = jnp.concatenate([middle[1, chip] for chip in range(kv_size)], axis=1).astype(F32)
+        squares = jnp.sum(values * values, axis=1, keepdims=True)
+        dead_acc[...] = dot((values * gains2_ref[...]).astype(BF16), units2[...])
         dead_hidden = finish(dead_acc, squares)
 
     def cut_terms(a):
@@ -619,7 +648,7 @@
         )
 
     with jax.named_scope("premix"):
-        small_copy.wait_recv()
+        arrived("small", small_recv.at[0])
         small_all = jnp.concatenate([small_acc[0], small_recv[0]], axis=0)
         high, low = cut_terms(small_all)
         picked_small = dot(pick_small.astype(BF16), high.astype(BF16)) + dot(
@@ -666,19 +695,17 @@
         fading = jnp.exp(final - cumulative)
         shrink = jnp.exp(final)
 
-    with jax.named_scope("partwait"):
-        for copy in part_copies.values():
-            copy.wait_recv()
-    scope = jax.named_scope("mix")
+    with jax.named_scope("partwait0"):
+        arrived("part0", part_send.at[0, pl.ds(0, devices - 1)])
+    scope = jax.named_scope("mix0")
     scope.__enter__()
     upper = iota((BLK, wide), 0) < slots
 
     def by_head(pair):
         ahead, behind = [], []
         for chip in range(kv_size):
-            at = slice(pair * BLK, (pair + 1) * BLK)
-            mine = part_recv[chip, 0, at].astype(F32)
-            theirs = part_recv[chip, 1, at].astype(F32)
+            mine = part_recv[pair, chip, 0].astype(F32)
+            theirs = part_recv[pair, chip, 1].astype(F32)
             front = jnp.where(upper, mine, theirs)
             back = pltpu.roll(jnp.where(upper, theirs, mine), slots, 0)
             for start in range(0, wide, HEAD):
@@ -687,7 +714,6 @@
         return jnp.concatenate(ahead, axis=0), jnp.concatenate(behind, axis=0)
 
     query, key_in = by_head(0)
-    value, gating = by_head(1)
     query_unit = (
         query
         * lax.rsqrt(jnp.sum(query * query, axis=1, keepdims=True) + EPSILON)
@@ -715,6 +741,12 @@
         result = result + dot(both[: 2 * BLK], state_low[head])
         key_terms.append(result[:BLK])
         query_terms.append(result[BLK:])
+    scope.__exit__(None, None, None)
+    with jax.named_scope("partwait1"):
+        arrived("part1", part_send.at[1, pl.ds(0, devices - 1)])
+    scope = jax.named_scope("mix1")
+    scope.__enter__()
+    value, gating = by_head(1)
     update = dot_fine(inverse, write_gate * value - jnp.concatenate(key_terms, axis=0))
     attend = jnp.concatenate(query_terms, axis=0) + dot_fine(scores, update)
     normed = attend * lax.rsqrt(jnp.mean(attend * attend, axis=1, keepdims=True) + EPSILON)
@@ -735,9 +767,10 @@
         backs.append(jnp.where(upper, pltpu.roll(even, slots, 0), odd))
     heads_send[0] = jnp.concatenate(fronts, axis=0).astype(BF16)
     heads_send[1] = jnp.concatenate(backs, axis=0).astype(BF16)
-    copies = to_all(
-        lambda off, other, peer: heads_send.at[lax.rem(cls + other, 2)],
-        lambda off, other: heads_recv.at[me],
+    to_all(
+        "heads",
+        lambda other, peer: heads_send.at[lax.rem(cls + other, 2)],
+        lambda other: heads_recv.at[me],
     )
     heads_recv[me] = heads_send[cls]
     scope.__exit__(None, None, None)
@@ -757,46 +790,40 @@
             state_out[0, head] = shrink[head * BLK : head * BLK + 1] * state[head] + outer
 
     def hand_over(group, hidden, source):
-        outgoing = {}
-
-        def term_of(chip, core):
-            at = pl.ds(pl.multiple_of((chip * 2 + core) * cols, cols), cols)
-            return dot(hidden, down2[:, at])
-
         for off in far_first:
             chip = swapped(off)
+            term = dot(hidden, down2[:, chip_rows(chip)]).astype(BF16)
+            fin_send[group, off, 0] = term[:, :cols]
+            fin_send[group, off, 1] = term[:, cols:]
             for other in (0, 1):
                 core = core_of(chip, other)
-                fin_send[group, off, other] = term_of(chip, core).astype(BF16)
-                outgoing[off, other] = remote(
-                    fin_send.at[group, off, other], fin_recv.at[group, off, other], chip, core
+                remote(
+                    f"fin{group}", fin_send.at[group, off, core],
+                    fin_recv.at[group, off, other], chip, core,
                 )
-        theirs = pl.ds(pl.multiple_of((1 - tp) * cols, cols), cols)
-        own_send[group] = source[:, theirs].astype(F32) + 0.5 * term_of(kv, 1 - tp)
-        outgoing[0, 1] = to_partner(own_send.at[group], own_recv.at[group])
-        own = source[:, own_cols].astype(F32) + 0.5 * term_of(kv, tp)
-        return own, outgoing
-
-    def take_in(group, own, outgoing):
-        outgoing[0, 1].wait_recv()
-        sums = [own, own_recv[group]]
+        term = source.astype(F32) + 0.5 * dot(hidden, down2[:, chip_rows(kv)])
+        own_send[group, 0] = term[:, :cols]
+        own_send[group, 1] = term[:, cols:]
+        to_partner(f"own{group}", own_send.at[group, 1 - tp], own_recv.at[group])
+
+    def take_in(group):
+        arrived(f"own{group}", own_recv.at[group])
+        arrived(f"fin{group}", fin_recv.at[group, pl.ds(1, kv_size - 1)])
+        sums = [own_send[group, tp], own_recv[group]]
         for other in (0, 1):
-            total = None
-            for off in far_first[::-1]:
-                outgoing[off, other].wait_recv()
-                term = fin_recv[group, off, other].astype(F32)
-                total = term if total is None else total + term
+            total = fin_recv[group, 1, other].astype(F32)
+            for off in range(2, kv_size):
+                total = total + fin_recv[group, off, other].astype(F32)
             sums[other] = sums[other] + 0.5 * total
         return [total.astype(BF16) for total in sums]
 
     with jax.named_scope("dead_down"):
-        loads["down2"].wait()
-        dead_own, dead_out = hand_over(1, dead_hidden, middle.at[1, kv])
+        loaded("down2")
+        hand_over(1, dead_hidden, middle[1, kv])
 
     with jax.named_scope("gather2"):
-        for copy in copies.values():
-            copy.wait_recv()
-        out_copy.wait_recv()
+        arrived("heads", heads_recv.at[pl.ds(0, devices - 1)])
+        arrived("out", out_w.at[:, own_cols])
     with jax.named_scope("outproj"):
         blocks = heads_recv[...].reshape(devices * 2 * BLK, wide)
         mixed = dot(gather_heads, blocks).astype(BF16)
@@ -807,33 +834,49 @@
             right = out_w[chips[0] * wide : (chips[-1] + 1) * wide, :]
             terms.append(dot(left, right).astype(BF16).astype(F32))
         second_in[kv] = (middle[0, kv].astype(F32) + (terms[0] + terms[1])).astype(BF16)
-        copies = to_class(lambda off: second_in.at[kv], lambda off: second_in.at[kv])
+        to_class("second", lambda off: second_in.at[kv], lambda off: second_in.at[kv], kv_size)
 
     squares = jnp.zeros((pack, 1), F32)
-    with jax.named_scope("gather3"):
-        for off in range(kv_size):
-            if off:
-                copies[off].wait_recv()
-            chip = swapped(off)
+    for index, off in enumerate([0] + near_first):
+        chip = swapped(off)
+        with jax.named_scope(f"second_wait{index}"):
+            if index:
+                arrived("second", second_in.at[chip], off)
+        with jax.named_scope(f"live_slot{index}"):
             squares = squares + ffn_slot(
-                live_acc, units2, gains2_ref, chip, second_in[chip], off == 0
+                live_acc, units2, gains2_ref, chip, second_in[chip], index == 0
             )
     with jax.named_scope("finish1"):
         hidden = finish(live_acc, squares)
     with jax.named_scope("down1"):
-        live_own, live_out = hand_over(0, hidden, second_in.at[kv])
+        hand_over(0, hidden, second_in[kv])
     with jax.named_scope("dead_in"):
-        dead_sums = take_in(1, dead_own, dead_out)
+        dead_sums = take_in(1)
     with jax.named_scope("live_in"):
-        live_sums = take_in(0, live_own, live_out)
+        live_sums = take_in(0)
     with jax.named_scope("last"):
         packed = jnp.concatenate(
             [live_sums[0], dead_sums[0], live_sums[1], dead_sums[1]], axis=0
         )
         mixed_out_ref[...] = dot(restore, packed).astype(BF16)
     with jax.named_scope("tail"):
-        for copy in sent:
-            copy.wait_send()
+        totals = {
+            "tokens": entered.at[pl.ds(0, devices - 1)],
+            "lens": lens_all.at[pl.ds(0, devices - 1)],
+            "proj": proj.at[:, 0 : 4 * cols],
+            "out": out_w.at[:, own_cols],
+            "small": small_acc.at[0],
+            "heads": heads_recv.at[pl.ds(0, devices - 1)],
+            "second": second_in.at[pl.ds(0, kv_size - 1)],
+        }
+        for index in range(2):
+            totals[f"red{index}"] = red_send.at[index, pl.ds(1, kv_size - 1)]
+            totals[f"middle{index}"] = middle.at[index, pl.ds(0, kv_size - 1)]
+            totals[f"part{index}"] = part_send.at[index, pl.ds(0, devices - 1)]
+            totals[f"fin{index}"] = fin_send.at[index, pl.ds(1, kv_size - 1)]
+            totals[f"own{index}"] = own_send.at[index, 0]
+        for name in sends:
+            of_phase(name, totals[name]).wait_send()
 
 
 def fused_call(mesh, *args):
@@ -852,7 +895,6 @@
     in_hbm = pl.BlockSpec(memory_space=pltpu.HBM)
     in_vmem = pl.BlockSpec(memory_space=pltpu.VMEM)
     dma = pltpu.SemaphoreType.DMA
-    remotes = 7 * (devices - 1) + 6 * (kv_size - 1) + 10
     operands = (
         tokens, lengths.reshape(1, 1), gain_first.reshape(1, -1), gain_mix.reshape(1, -1),
         gain_second.reshape(1, -1), forget_rate.reshape(1, -1), state,
@@ -903,16 +945,16 @@
             pltpu.VMEM((devices, 2 * BLK, wide), BF16),
             pltpu.VMEM((2, kv_size, pack, wide), BF16),
             pltpu.VMEM((2, kv_size, pack, wide), BF16),
-            pltpu.VMEM((devices, 2 * BLK, wide), BF16),
-            pltpu.VMEM((kv_size, 2, 2 * BLK, wide), BF16),
+            pltpu.VMEM((2, devices, BLK, wide), BF16),
+            pltpu.VMEM((2, kv_size, 2, BLK, wide), BF16),
             pltpu.VMEM((1, pack, HEAD), F32),
             pltpu.VMEM((2, kv_size, 2, pack, cols), BF16),
             pltpu.VMEM((2, kv_size, 2, pack, cols), BF16),
+            pltpu.VMEM((2, 2, pack, cols), F32),
             pltpu.VMEM((2, pack, cols), F32),
-            pltpu.VMEM((2, pack, cols), F32),
-            dma((3 + 2 * kv_size + 15,)),
-            dma((remotes,)),
-            dma((remotes,)),
+            dma((kv_size + 13,)),
+            dma((17,)),
+            dma((3 * kv_size + 14,)),
         ],
         compiler_params=pltpu.CompilerParams(
             collective_id=0, has_side_effects=True, vmem_limit_bytes=VMEM_LIMIT

time: 46.9 us -> 43.2 us (0.921)
  Pallas kernels: 45.5 us -> 41.7 us
    pallas_call x1, Pallas kernels: 44.5 us -> 40.7 us  [fused_call(): pl.pallas_call(functools.partial(fused_kernel, kv_size, channels), out_sh...]
where the time goes in v2:
time: 43.2 us; the launch traced here: 43 us
  Pallas kernels  41.7 us (97%)
  between operations  1.29 us (3%)
    pallas_call x1, Pallas kernels, fused_call(): pl.pallas_call(functools.partial(fused_kernel, kv_size, channels), out_sh...  40.7 us
    pallas_call x1, Pallas kernels, hand_out(): pl.pallas_call(hand_out_kernel, out_shape=tuple((jax.ShapeDtypeStruct(arr...  1 us

profile of v2, /device:TPU:0, one launch (start us, length us, event | category | flops | bytes accessed | tf_op | source)
XLA Modules:
  0.0 43.0 jit_solution(10403573510216955202)
XLA Ops:
  1.3 40.7 %shard_map.203 = (bf16[64,256]{1,0:T(8,128)(2,1)S(1)}, f32[1,16,128,128]{3,2,1,0:T(8,128)S(1)}) custom-call(bf16[64,256]{1,0:T(8,128)(2,1)} %tokens_hbm.1, s32[1,1]{1,0:T(1,128)} %bitcast.7.lengths_hbm, f32[1,2048]{1,0:T(1,128)} %bitcast.10, f32[1,2048]{1,0:T(1,128)} %bitcast.11, f32[1,2048]{1,0:T(1,128)} %bitcast.12, f32[1,16]{1,0:T(1,128)} %bitcast.13, ...), custom_call_target="tpu_custom_call" | custom-call | tf_op jit(solution)/shard_map/pallas_call | solution.py:909
  42.0 1.0 %shard_map.204 = (bf16[64,256]{1,0:T(8,128)(2,1)}, f32[1,16,128,128]{3,2,1,0:T(8,128)}) custom-call(bf16[64,256]{1,0:T(8,128)(2,1)S(1)} %get-tuple-element.4.mixed, f32[1,16,128,128]{3,2,1,0:T(8,128)S(1)} %get-tuple-element.5.state), custom_call_target="tpu_custom_call" | custom-call | tf_op jit(solution)/shard_map/pallas_call | solution.py:983

commit v3 on v2

--- a/solution.py
+++ b/solution.py
@@ -194,7 +194,8 @@
     gate2_hbm,
     up2_hbm,
     down2_hbm,
-    mixed_out_ref,
+    packed_out,
+    order_out,
     state_out,
     units1,
     down1,
@@ -297,9 +298,9 @@
             (up1_hbm.at[at, :], units1.at[at, hidden_local : 2 * hidden_local]),
         )
     early = list(loads)
-    load("down1", (down1_hbm, down1))
     kinds = (query_hbm, key_hbm, value_hbm, gating_hbm)
     load("proj", *[(ref, proj.at[:, kind_cols(kind)]) for kind, ref in enumerate(kinds)])
+    load("down1", (down1_hbm, down1))
     load(
         "small",
         (write_hbm, small_w.at[0:HEADS]),
@@ -319,48 +320,43 @@
     late = [name for name in loads if name not in early]
     for name in early[:2]:
         start(name)
-
     barrier = pltpu.get_barrier_semaphore()
-    for off in range(1, devices):
-        peer = lax.rem(me + off, devices)
-        pl.semaphore_signal(
-            barrier,
-            inc=1,
-            device_id={"kv": peer // 2, "tp": lax.rem(peer, 2)},
-            device_id_type=MESH,
-        )
+    here = 0
+    for off in far_first + [here]:
+        for core in (tp, 1 - tp) if off is not here else (1 - tp,):
+            pl.semaphore_signal(
+                barrier, inc=1, device_id={"kv": swapped(off), "tp": core}, device_id_type=MESH
+            )
     for name in early[2:]:
         start(name)
 
     sends, receives, width = {}, {}, [0]
 
     def remote(name, src, dst, chip, core, at=0, spread=1):
-        if name not in sends:
-            sends[name] = len(sends)
+        sends.setdefault(name.rstrip("01"), len(sends))
+        if name not in receives:
             receives[name] = width[0]
             width[0] += spread
         copy = pltpu.make_async_remote_copy(
             src_ref=src,
             dst_ref=dst,
-            send_sem=send_sems.at[sends[name]],
+            send_sem=send_sems.at[sends[name.rstrip("01")]],
             recv_sem=recv_sems.at[receives[name] + at],
             device_id={"kv": chip, "tp": core},
             device_id_type=MESH,
         )
         copy.start()
 
-    def of_phase(name, ref, at=0):
-        return pltpu.make_async_remote_copy(
+    def arrived(name, ref, at=0):
+        sem = recv_sems.at[receives[name] + at]
+        pltpu.make_async_remote_copy(
             src_ref=ref,
             dst_ref=ref,
-            send_sem=send_sems.at[sends[name]],
-            recv_sem=recv_sems.at[receives[name] + at],
+            send_sem=sem,
+            recv_sem=sem,
             device_id={"kv": kv, "tp": 1 - tp},
             device_id_type=MESH,
-        )
-
-    def arrived(name, ref, at=0):
-        of_phase(name, ref, at).wait_recv()
+        ).wait_recv()
 
     def to_class(name, src, dst, spread=1):
         for off in far_first:
@@ -368,19 +364,26 @@
             remote(name, src(off), dst(off), chip, core_of(chip, 0), off if spread > 1 else 0, spread)
 
     def to_all(name, src, dst, spread=1):
-        for off in far_first + [0]:
+        for off in far_first:
             chip = swapped(off)
-            for other in (0, 1):
-                if other == 0 and isinstance(off, int) and off == 0:
-                    continue
+            same = lax.rem(off, 2)
+            for other in (same, 1 - same):
                 core = core_of(chip, other)
                 remote(
                     name, src(other, chip * 2 + core), dst(other), chip, core,
                     off if spread > 1 else 0, spread,
                 )
+        to_partner(name, src(1, kv * 2 + 1 - tp), dst(1))
 
     def to_partner(name, src, dst):
         remote(name, src, dst, kv, 1 - tp)
+
+    def columns_of(hidden, down, chips):
+        right = jnp.concatenate([down[:, chip_rows(chip)] for chip in chips], axis=1)
+        both = jnp.dot(hidden, right, preferred_element_type=F32)
+        return [both[:, at * wide : (at + 1) * wide] for at in range(len(chips))]
+
+    pairs = [(far_first[0], far_first[1]), (far_first[2], 0)]
 
     def iota(shape, axis):
         return lax.broadcasted_iota(jnp.int32, shape, axis)
@@ -502,16 +505,15 @@
     with jax.named_scope("down_wait"):
         loaded("down1")
     with jax.named_scope("down0"):
-        for off in far_first:
-            chip = swapped(off)
-            term = dot(hidden, down1[:, chip_rows(chip)])
-            red_send[0, off] = term[:pack].astype(BF16)
-            red_send[1, off] = term[pack:].astype(BF16)
-            remote("red0", red_send.at[0, off], red_recv.at[0, off], chip, core_of(chip, 0))
-        own_term = dot(hidden, down1[:, chip_rows(kv)])
-        for off in far_first:
-            chip = swapped(off)
-            remote("red1", red_send.at[1, off], red_recv.at[1, off], chip, core_of(chip, 0))
+        for pair in pairs:
+            chips = [swapped(off) for off in pair]
+            for off, chip, term in zip(pair, chips, columns_of(hidden, down1, chips)):
+                if off is pairs[1][1]:
+                    own_term = term
+                    continue
+                red_send[0, off] = term[:pack].astype(BF16)
+                red_send[1, off] = term[pack:].astype(BF16)
+                remote("red0", red_send.at[0, off], red_recv.at[0, off], chip, core_of(chip, 0))
     with jax.named_scope("exchange_out"):
         loaded("out")
         to_partner("out", out_w.at[:, own_cols], out_w.at[:, own_cols])
@@ -553,7 +555,7 @@
         klass = lax.rem(seq + token, 2)
         place = place_rows(seq, token // 2, klass, jnp.where(klass == cls, flags, other_flags))
         lane = iota((rows, HEAD), 1)
-        restore = one_hot(
+        order_out[...] = one_hot(
             (lax.rem(lane // half + cls, 2) == klass)
             & (lax.rem(lane, half) == place)
             & (lane < rows)
@@ -564,21 +566,26 @@
             high = state[head].astype(BF16)
             state_high[head] = high
             state_low[head] = (state[head] - high.astype(F32)).astype(BF16)
-    for group in range(2):
-        with jax.named_scope(f"red0_{group}"):
-            at = slice(group * pack, (group + 1) * pack)
-            arrived(f"red{group}", red_recv.at[group, pl.ds(1, kv_size - 1)])
-            total = own_term[at]
-            for off in range(1, kv_size):
-                total = total + red_recv[group, off].astype(F32)
-            middle[group, kv] = (residual[at] + 0.5 * total).astype(BF16)
-            to_class(
-                f"middle{group}",
-                lambda off: middle.at[group, kv],
-                lambda off: middle.at[group, kv],
-                1 if group else kv_size,
-            )
-
+    for off in far_first:
+        chip = swapped(off)
+        remote("red1", red_send.at[1, off], red_recv.at[1, off], chip, core_of(chip, 0))
+
+    def first_done(group):
+        at = slice(group * pack, (group + 1) * pack)
+        arrived(f"red{group}", red_recv.at[group, pl.ds(1, kv_size - 1)])
+        total = own_term[at]
+        for off in range(1, kv_size):
+            total = total + red_recv[group, off].astype(F32)
+        middle[group, kv] = (residual[at] + 0.5 * total).astype(BF16)
+        to_class(
+            f"middle{group}",
+            lambda off: middle.at[group, kv],
+            lambda off: middle.at[group, kv],
+            1 if group else kv_size,
+        )
+
+    with jax.named_scope("red0"):
+        first_done(0)
     with jax.named_scope("proj_wait"):
         arrived("proj", proj.at[:, 0 : 4 * cols])
         loaded("small", small_w.at[0 : 2 * HEADS])
@@ -601,6 +608,8 @@
             if index == 0:
                 proj_acc[...] = dot(scaled, proj[at, :])
                 small_acc[0] = small_term
+                with jax.named_scope("red1"):
+                    first_done(1)
             elif index < kv_size - 1:
                 proj_acc[...] += dot(scaled, proj[at, :])
                 small_acc[0] += small_term
@@ -624,15 +633,6 @@
         for pair in range(2):
             part_recv[pair, kv, cls] = part_send[pair, me]
 
-    with jax.named_scope("dead_units"):
-        loaded("gains2")
-        loaded("units2", units2)
-        arrived("middle1", middle.at[1, pl.ds(0, kv_size - 1)])
-        values = jnp.concatenate([middle[1, chip] for chip in range(kv_size)], axis=1).astype(F32)
-        squares = jnp.sum(values * values, axis=1, keepdims=True)
-        dead_acc[...] = dot((values * gains2_ref[...]).astype(BF16), units2[...])
-        dead_hidden = finish(dead_acc, squares)
-
     def cut_terms(a):
         high = a.astype(BF16).astype(F32)
         return high, a - high
@@ -694,6 +694,15 @@
         growth = jnp.exp(cumulative)
         fading = jnp.exp(final - cumulative)
         shrink = jnp.exp(final)
+
+    with jax.named_scope("dead_units"):
+        loaded("gains2")
+        loaded("units2", units2)
+        arrived("middle1", middle.at[1, pl.ds(0, kv_size - 1)])
+        values = jnp.concatenate([middle[1, chip] for chip in range(kv_size)], axis=1).astype(F32)
+        squares = jnp.sum(values * values, axis=1, keepdims=True)
+        dead_acc[...] = dot((values * gains2_ref[...]).astype(BF16), units2[...])
+        dead_hidden = finish(dead_acc, squares)
 
     with jax.named_scope("partwait0"):
         arrived("part0", part_send.at[0, pl.ds(0, devices - 1)])
@@ -789,22 +798,33 @@
             )
             state_out[0, head] = shrink[head * BLK : head * BLK + 1] * state[head] + outer
 
-    def hand_over(group, hidden, source):
-        for off in far_first:
-            chip = swapped(off)
-            term = dot(hidden, down2[:, chip_rows(chip)]).astype(BF16)
-            fin_send[group, off, 0] = term[:, :cols]
-            fin_send[group, off, 1] = term[:, cols:]
-            for other in (0, 1):
-                core = core_of(chip, other)
-                remote(
-                    f"fin{group}", fin_send.at[group, off, core],
-                    fin_recv.at[group, off, other], chip, core,
-                )
-        term = source.astype(F32) + 0.5 * dot(hidden, down2[:, chip_rows(kv)])
-        own_send[group, 0] = term[:, :cols]
-        own_send[group, 1] = term[:, cols:]
+    def hand_off(group, off):
+        chip = swapped(off)
+        for other in (0, 1):
+            core = core_of(chip, other)
+            remote(
+                f"fin{group}", fin_send.at[group, off, core],
+                fin_recv.at[group, off, other], chip, core,
+            )
+
+    def hand_own(group):
         to_partner(f"own{group}", own_send.at[group, 1 - tp], own_recv.at[group])
+
+    def second_down(group, hidden, source, at_once):
+        for pair in pairs:
+            chips = [swapped(off) for off in pair]
+            for off, chip, term in zip(pair, chips, columns_of(hidden, down2, chips)):
+                if off is pairs[1][1]:
+                    term = source.astype(F32) + 0.5 * term
+                    own_send[group, 0] = term[:, :cols]
+                    own_send[group, 1] = term[:, cols:]
+                    continue
+                fin_send[group, off, 0] = term[:, :cols].astype(BF16)
+                fin_send[group, off, 1] = term[:, cols:].astype(BF16)
+                if at_once:
+                    hand_off(group, off)
+        if at_once:
+            hand_own(group)
 
     def take_in(group):
         arrived(f"own{group}", own_recv.at[group])
@@ -819,8 +839,7 @@
 
     with jax.named_scope("dead_down"):
         loaded("down2")
-        hand_over(1, dead_hidden, middle[1, kv])
-
+        second_down(1, dead_hidden, middle[1, kv], False)
     with jax.named_scope("gather2"):
         arrived("heads", heads_recv.at[pl.ds(0, devices - 1)])
         arrived("out", out_w.at[:, own_cols])
@@ -846,19 +865,23 @@
             squares = squares + ffn_slot(
                 live_acc, units2, gains2_ref, chip, second_in[chip], index == 0
             )
+        if index == 1:
+            with jax.named_scope("dead_off"):
+                for off in far_first:
+                    hand_off(1, off)
+                hand_own(1)
     with jax.named_scope("finish1"):
         hidden = finish(live_acc, squares)
     with jax.named_scope("down1"):
-        hand_over(0, hidden, second_in[kv])
+        second_down(0, hidden, second_in[kv], True)
     with jax.named_scope("dead_in"):
         dead_sums = take_in(1)
     with jax.named_scope("live_in"):
         live_sums = take_in(0)
     with jax.named_scope("last"):
-        packed = jnp.concatenate(
+        packed_out[...] = jnp.concatenate(
             [live_sums[0], dead_sums[0], live_sums[1], dead_sums[1]], axis=0
         )
-        mixed_out_ref[...] = dot(restore, packed).astype(BF16)
     with jax.named_scope("tail"):
         totals = {
             "tokens": entered.at[pl.ds(0, devices - 1)],
@@ -868,15 +891,22 @@
             "small": small_acc.at[0],
             "heads": heads_recv.at[pl.ds(0, devices - 1)],
             "second": second_in.at[pl.ds(0, kv_size - 1)],
+            "red": red_send.at[:, pl.ds(1, kv_size - 1)],
+            "middle": middle.at[:, pl.ds(0, kv_size - 1)],
+            "part": part_send.at[:, pl.ds(0, devices - 1)],
+            "fin": fin_send.at[:, pl.ds(1, kv_size - 1)],
+            "own": own_send.at[0],
         }
-        for index in range(2):
-            totals[f"red{index}"] = red_send.at[index, pl.ds(1, kv_size - 1)]
-            totals[f"middle{index}"] = middle.at[index, pl.ds(0, kv_size - 1)]
-            totals[f"part{index}"] = part_send.at[index, pl.ds(0, devices - 1)]
-            totals[f"fin{index}"] = fin_send.at[index, pl.ds(1, kv_size - 1)]
-            totals[f"own{index}"] = own_send.at[index, 0]
-        for name in sends:
-            of_phase(name, totals[name]).wait_send()
+        for name, ref in totals.items():
+            sem = send_sems.at[sends[name]]
+            pltpu.make_async_remote_copy(
+                src_ref=ref,
+                dst_ref=ref,
+                send_sem=sem,
+                recv_sem=sem,
+                device_id={"kv": kv, "tp": 1 - tp},
+                device_id_type=MESH,
+            ).wait_send()
 
 
 def fused_call(mesh, *args):
@@ -906,14 +936,15 @@
         array if array.dtype == jnp.int32 else pltpu.with_memory_space_constraint(array, pltpu.HBM)
         for array in operands
     ]
-    mixed_out, new_state = pl.pallas_call(
+    results = pl.pallas_call(
         functools.partial(fused_kernel, kv_size, channels),
         out_shape=(
             pltpu.VMEM(tokens.shape, tokens.dtype),
+            pltpu.VMEM((rows, rows), BF16),
             pltpu.VMEM(state.shape, state.dtype),
         ),
         in_specs=[in_hbm] * len(operands),
-        out_specs=(in_vmem, in_vmem),
+        out_specs=(in_vmem, in_vmem, in_vmem),
         scratch_shapes=[
             pltpu.VMEM((channels, 2 * hidden_local), BF16),
             pltpu.VMEM((hidden_local, channels), BF16),
@@ -953,39 +984,46 @@
             pltpu.VMEM((2, 2, pack, cols), F32),
             pltpu.VMEM((2, pack, cols), F32),
             dma((kv_size + 13,)),
-            dma((17,)),
+            dma((12,)),
             dma((3 * kv_size + 14,)),
         ],
         compiler_params=pltpu.CompilerParams(
             collective_id=0, has_side_effects=True, vmem_limit_bytes=VMEM_LIMIT
         ),
     )(*operands)
-    return hand_out(mixed_out, new_state)
-
-
-def hand_out_kernel(mixed, state, mixed_out_hbm, state_out_hbm, sems):
-    puts = [
-        pltpu.make_async_copy(mixed, mixed_out_hbm, sems.at[0]),
-        pltpu.make_async_copy(state, state_out_hbm, sems.at[1]),
-    ]
-    for put in puts:
-        put.start()
-    for put in puts:
-        put.wait()
-
-
-def hand_out(mixed_out, new_state):
+    return hand_out(*results)
+
+
+def hand_out_kernel(packed, order, state, mixed_hbm, state_hbm, mixed, sems):
+    put_state = pltpu.make_async_copy(state, state_hbm, sems.at[0])
+    put_state.start()
+    restored = jnp.dot(order[...], packed[...], preferred_element_type=F32)
+    mixed[...] = restored.astype(BF16)
+    put_mixed = pltpu.make_async_copy(mixed, mixed_hbm, sems.at[1])
+    put_mixed.start()
+    put_mixed.wait()
+    put_state.wait()
+
+
+def hand_out(packed, order, new_state):
     in_hbm = pl.BlockSpec(memory_space=pltpu.HBM)
     in_vmem = pl.BlockSpec(memory_space=pltpu.VMEM)
     arrays = [
-        pltpu.with_memory_space_constraint(array, pltpu.VMEM) for array in (mixed_out, new_state)
+        pltpu.with_memory_space_constraint(array, pltpu.VMEM)
+        for array in (packed, order, new_state)
     ]
     return pl.pallas_call(
         hand_out_kernel,
-        out_shape=tuple(jax.ShapeDtypeStruct(array.shape, array.dtype) for array in arrays),
-        in_specs=[in_vmem, in_vmem],
+        out_shape=(
+            jax.ShapeDtypeStruct(packed.shape, packed.dtype),
+            jax.ShapeDtypeStruct(new_state.shape, new_state.dtype),
+        ),
+        in_specs=[in_vmem] * 3,
         out_specs=(in_hbm, in_hbm),
-        scratch_shapes=[pltpu.SemaphoreType.DMA((2,))],
+        scratch_shapes=[
+            pltpu.VMEM(packed.shape, packed.dtype),
+            pltpu.SemaphoreType.DMA((2,)),
+        ],
         compiler_params=pltpu.CompilerParams(vmem_limit_bytes=8 * 1024 * 1024),
     )(*arrays)
 

time: 43.2 us -> 41.6 us (0.963)
  Pallas kernels: 41.7 us -> 40.2 us
    pallas_call x1, Pallas kernels: 40.7 us -> 39.2 us  [fused_call(): pl.pallas_call(functools.partial(fused_kernel, kv_size, channels), out_sh...]
where the time goes in v3:
time: 41.6 us; the launch traced here: 41.5 us
  Pallas kernels  40.2 us (97%)
  between operations  1.29 us (3%)
    pallas_call x1, Pallas kernels, fused_call(): pl.pallas_call(functools.partial(fused_kernel, kv_size, channels), out_sh...  39.2 us
    pallas_call x1, Pallas kernels, hand_out(): pl.pallas_call(hand_out_kernel, out_shape=(jax.ShapeDtypeStruct(packed.sh...  0.99 us

profile of v3, /device:TPU:0, one launch (start us, length us, event | category | flops | bytes accessed | tf_op | source)
XLA Modules:
  0.0 41.5 jit_solution(3423357868476056674)
XLA Ops:
  1.3 39.2 %shard_map.203 = (bf16[64,256]{1,0:T(8,128)(2,1)S(1)}, bf16[64,64]{1,0:T(8,128)(2,1)S(1)}, f32[1,16,128,128]{3,2,1,0:T(8,128)S(1)}) custom-call(bf16[64,256]{1,0:T(8,128)(2,1)} %tokens_hbm.1, s32[1,1]{1,0:T(1,128)} %bitcast.7.lengths_hbm, f32[1,2048]{1,0:T(1,128)} %bitcast.10, f32[1,2048]{1,0:T(1,128)} %bitcast.11, f32[1,2048]{1,0:T(1,128)} %bitcast.12, ...), custom_call_target="tpu_custom_call" | custom-call | tf_op jit(solution)/shard_map/pallas_call | solution.py:939
  40.5 1.0 %shard_map.204 = (bf16[64,256]{1,0:T(8,128)(2,1)}, f32[1,16,128,128]{3,2,1,0:T(8,128)}) custom-call(bf16[64,256]{1,0:T(8,128)(2,1)S(1)} %get-tuple-element.5.packed, bf16[64,64]{1,0:T(8,128)(2,1)S(1)} %get-tuple-element.6.order, f32[1,16,128,128]{3,2,1,0:T(8,128)S(1)} %get-tuple-element.7.state), custom_call_target="tpu_custom_call" | custom-call | tf_op jit(solution)/shard_map/pallas_call | solution.py:1015

commit v4 on v3

--- a/solution.py
+++ b/solution.py
@@ -218,7 +218,6 @@
     entered,
     unit_acc,
     live_acc,
-    dead_acc,
     proj_acc,
     small_acc,
     middle,
@@ -234,6 +233,7 @@
     fin_recv,
     own_send,
     own_recv,
+    spread_cols,
     load_sems,
     send_sems,
     recv_sems,
@@ -254,10 +254,11 @@
     near_first = [1, 2 + inner, 3 - inner]
     far_first = near_first[::-1]
 
-    loads = {}
-
-    def load(name, *pairs):
-        sem = load_sems.at[len(loads)]
+    loads, load_at = {}, {}
+
+    def load(name, *pairs, after=None):
+        load_at[name] = load_at[after] if after else len(set(load_at.values()))
+        sem = load_sems.at[load_at[name]]
         loads[name] = [pltpu.make_async_copy(src, dst, sem) for src, dst in pairs]
 
     def start(name):
@@ -268,7 +269,7 @@
         if ref is None:
             loads[name][0].wait()
         else:
-            sem = load_sems.at[list(loads).index(name)]
+            sem = load_sems.at[load_at[name]]
             pltpu.make_async_copy(ref, ref, sem).wait()
 
     def swapped(off):
@@ -306,18 +307,20 @@
         (write_hbm, small_w.at[0:HEADS]),
         (forget_hbm, small_w.at[HEADS : 2 * HEADS]),
     )
-    load("gains_mix", (gains_mix_hbm, gains_mix_ref))
-    load("rates", (rates_hbm, rates_ref))
+    load("gains_mix", (gains_mix_hbm, gains_mix_ref), after="length")
+    load("rates", (rates_hbm, rates_ref), after="tokens")
     load("out", (out_hbm, out_w.at[:, own_cols]))
-    load("state", (state_hbm.at[0], state))
-    load("gains2", (gains2_hbm, gains2_ref))
+    load("state", (state_hbm.at[0], state), after="units10")
+    load("gains2", (gains2_hbm, gains2_ref), after="gains1")
     load(
         "units2",
         (gate2_hbm, units2.at[:, 0:hidden_local]),
         (up2_hbm, units2.at[:, hidden_local : 2 * hidden_local]),
-    )
-    load("down2", (down2_hbm, down2))
-    late = [name for name in loads if name not in early]
+        after="units11",
+    )
+    load("down2", (down2_hbm, down2), after="units12")
+    last = ("state", "gains2", "units2", "down2")
+    late = [name for name in loads if name not in early and name not in last]
     for name in early[:2]:
         start(name)
     barrier = pltpu.get_barrier_semaphore()
@@ -331,12 +334,26 @@
         start(name)
 
     sends, receives, width = {}, {}, [0]
+    send_after = {"heads": "tokens", "second": "lens", "fin": "red", "own": "out"}
+    receive_after = {
+        "heads": "tokens",
+        "second": "tokens",
+        "fin0": "red0",
+        "fin1": "red1",
+        "own0": "small",
+        "own1": "proj",
+    }
 
     def remote(name, src, dst, chip, core, at=0, spread=1):
-        sends.setdefault(name.rstrip("01"), len(sends))
+        base = name.rstrip("01")
+        if base not in sends:
+            sends[base] = sends[send_after[base]] if base in send_after else len(set(sends.values()))
         if name not in receives:
-            receives[name] = width[0]
-            width[0] += spread
+            if name in receive_after:
+                receives[name] = receives[receive_after[name]]
+            else:
+                receives[name] = width[0]
+                width[0] += spread
         copy = pltpu.make_async_remote_copy(
             src_ref=src,
             dst_ref=dst,
@@ -358,6 +375,17 @@
             device_id_type=MESH,
         ).wait_recv()
 
+    def all_sent(name, ref):
+        sem = send_sems.at[sends[name]]
+        pltpu.make_async_remote_copy(
+            src_ref=ref,
+            dst_ref=ref,
+            send_sem=sem,
+            recv_sem=sem,
+            device_id={"kv": kv, "tp": 1 - tp},
+            device_id_type=MESH,
+        ).wait_send()
+
     def to_class(name, src, dst, spread=1):
         for off in far_first:
             chip = swapped(off)
@@ -366,8 +394,8 @@
     def to_all(name, src, dst, spread=1):
         for off in far_first:
             chip = swapped(off)
-            same = lax.rem(off, 2)
-            for other in (same, 1 - same):
+            first = lax.rem(chip + cls, 2)
+            for other in (first, 1 - first):
                 core = core_of(chip, other)
                 remote(
                     name, src(other, chip * 2 + core), dst(other), chip, core,
@@ -415,16 +443,18 @@
         start(name)
     small_w[2 * HEADS :] = jnp.zeros((HEAD - 2 * HEADS, channels), BF16)
 
-    def ffn_slot(acc, units, gain_ref, chip, portion, first):
+    def ffn_slot(acc, units, gain_ref, chip, portion, index):
         at = chip_rows(chip)
         values = portion.astype(F32)
         scaled = (values * gain_ref[:, at]).astype(BF16)
         term = dot(scaled, units[at, :])
-        if first:
+        if index == 0:
             acc[...] = term
+        elif index < kv_size - 1:
+            acc[...] += term
         else:
-            acc[...] += term
-        return jnp.sum(values * values, axis=1, keepdims=True)
+            term = acc[...] + term
+        return jnp.sum(values * values, axis=1, keepdims=True), term
 
     def finish(acc, squares):
         row_scale = lax.rsqrt(squares / channels + EPSILON)
@@ -491,9 +521,10 @@
                     jnp.minimum(lane // slots, devices - 1), lax.rem(lane, slots), column
                 )
                 reorder = one_hot(iota((half, HEAD), 0) == place)[:, :half]
-            squares = squares + ffn_slot(
-                unit_acc, units1, gains1_ref, chip, chip_tokens(chip), index == 0
+            square, total = ffn_slot(
+                unit_acc, units1, gains1_ref, chip, chip_tokens(chip), index
             )
+            squares = squares + square
         if index == kv_size - 2:
             with jax.named_scope("exchange"):
                 loaded("proj", proj.at[:, 0 : 4 * cols])
@@ -501,7 +532,7 @@
                     at = kind_cols(kind)
                     to_partner("proj", proj.at[:, at], proj.at[:, at])
     with jax.named_scope("finish0"):
-        hidden = dot(reorder, finish(unit_acc, squares)).astype(BF16)
+        hidden = dot(reorder, finish(total, squares)).astype(BF16)
     with jax.named_scope("down_wait"):
         loaded("down1")
     with jax.named_scope("down0"):
@@ -517,6 +548,8 @@
     with jax.named_scope("exchange_out"):
         loaded("out")
         to_partner("out", out_w.at[:, own_cols], out_w.at[:, own_cols])
+        for name in last:
+            start(name)
     with jax.named_scope("tables"):
         residual = dot(reorder, chip_tokens(kv))
         flags = live_row(cls)
@@ -524,7 +557,7 @@
         at = iota((rows, HEAD), 0)
         slot = lax.rem(at, slots)
         place = place_rows(at // BLK, slot, cls, flags)
-        kind = lax.rem(at // slots + cls, 2)
+        kind = lax.rem(at // slots + at // BLK + cls, 2)
         lane = iota((rows, HEAD), 1)
         spread = one_hot(
             (lane // pack == kind) & (lax.rem(lane, pack) == place) & (lane < 2 * pack)
@@ -535,7 +568,7 @@
         chip_at = lax.rem(iota((kv_size * pack, devices * 2 * BLK), 1) // slots, kv_size)
         gather_heads = one_hot((at // pack == chip_at) & (lax.rem(at, pack) == place))
         at = iota((BLK, HEAD), 0)
-        klass = at // slots
+        klass = lax.rem(at // slots + me, 2)
         place = place_rows(
             jnp.zeros((BLK, HEAD), jnp.int32) + me,
             lax.rem(at, slots),
@@ -560,12 +593,6 @@
             & (lax.rem(lane, half) == place)
             & (lane < rows)
         )[:, :rows]
-    with jax.named_scope("statecut"):
-        loaded("state")
-        for head in range(HEADS):
-            high = state[head].astype(BF16)
-            state_high[head] = high
-            state_low[head] = (state[head] - high.astype(F32)).astype(BF16)
     for off in far_first:
         chip = swapped(off)
         remote("red1", red_send.at[1, off], red_recv.at[1, off], chip, core_of(chip, 0))
@@ -586,6 +613,12 @@
 
     with jax.named_scope("red0"):
         first_done(0)
+    with jax.named_scope("statecut"):
+        loaded("state")
+        for head in range(HEADS):
+            high = state[head].astype(BF16)
+            state_high[head] = high
+            state_low[head] = (state[head] - high.astype(F32)).astype(BF16)
     with jax.named_scope("proj_wait"):
         arrived("proj", proj.at[:, 0 : 4 * cols])
         loaded("small", small_w.at[0 : 2 * HEADS])
@@ -647,6 +680,39 @@
             left, right, (((1,), (axis,)), ((), ())), preferred_element_type=F32
         )
 
+    with jax.named_scope("premix_a"):
+        size = HEADS * BLK
+
+        def token_of(at):
+            at = lax.rem(at, BLK)
+            return 2 * lax.rem(at, slots) + at // slots
+
+        row = iota((size, size), 0)
+        col = iota((size, size), 1)
+        same = (row // BLK) == (col // BLK)
+        causal = same & (token_of(row) >= token_of(col))
+        strict = same & (token_of(row) > token_of(col))
+        diagonal = row == col
+        pick = iota((size, HEADS), 0) // BLK == iota((size, HEADS), 1)
+
+        def as_column(block):
+            return jnp.sum(jnp.where(pick, block, 0.0), axis=1, keepdims=True)
+
+        def to_row(column):
+            return jnp.sum(jnp.where(diagonal, column, 0.0), axis=0, keepdims=True)
+
+    with jax.named_scope("dead_units"):
+        all_sent("tokens", entered.at[pl.ds(0, devices - 1)])
+        all_sent("lens", lens_all.at[pl.ds(0, devices - 1)])
+        all_sent("red", red_send.at[:, pl.ds(1, kv_size - 1)])
+        all_sent("out", out_w.at[:, own_cols])
+        loaded("gains2")
+        loaded("units2", units2)
+        arrived("middle1", middle.at[1, pl.ds(0, kv_size - 1)])
+        values = jnp.concatenate([middle[1, chip] for chip in range(kv_size)], axis=1).astype(F32)
+        squares = jnp.sum(values * values, axis=1, keepdims=True)
+        dead_hidden = finish(dot((values * gains2_ref[...]).astype(BF16), units2[...]), squares)
+
     with jax.named_scope("premix"):
         arrived("small", small_recv.at[0])
         small_all = jnp.concatenate([small_acc[0], small_recv[0]], axis=0)
@@ -656,27 +722,6 @@
         )
         write_pre = picked_small[:, 0:HEADS]
         forget_pre = picked_small[:, HEADS : 2 * HEADS]
-
-        size = HEADS * BLK
-
-        def token_of(at):
-            at = lax.rem(at, BLK)
-            return 2 * lax.rem(at, slots) + lax.rem(at // slots + me, 2)
-
-        row = iota((size, size), 0)
-        col = iota((size, size), 1)
-        same = (row // BLK) == (col // BLK)
-        causal = same & (token_of(row) >= token_of(col))
-        strict = same & (token_of(row) > token_of(col))
-        diagonal = row == col
-        identity = jnp.where(diagonal, 1.0, 0.0)
-        pick = iota((size, HEADS), 0) // BLK == iota((size, HEADS), 1)
-
-        def as_column(block):
-            return jnp.sum(jnp.where(pick, block, 0.0), axis=1, keepdims=True)
-
-        def to_row(column):
-            return jnp.sum(jnp.where(diagonal, column, 0.0), axis=0, keepdims=True)
 
         live = jnp.where(token_of(iota((size, 1), 0)) < length_ref[...], 1.0, 0.0)
         write_col = as_column(jnp.concatenate([write_pre] * HEADS, axis=0))
@@ -695,15 +740,6 @@
         fading = jnp.exp(final - cumulative)
         shrink = jnp.exp(final)
 
-    with jax.named_scope("dead_units"):
-        loaded("gains2")
-        loaded("units2", units2)
-        arrived("middle1", middle.at[1, pl.ds(0, kv_size - 1)])
-        values = jnp.concatenate([middle[1, chip] for chip in range(kv_size)], axis=1).astype(F32)
-        squares = jnp.sum(values * values, axis=1, keepdims=True)
-        dead_acc[...] = dot((values * gains2_ref[...]).astype(BF16), units2[...])
-        dead_hidden = finish(dead_acc, squares)
-
     with jax.named_scope("partwait0"):
         arrived("part0", part_send.at[0, pl.ds(0, devices - 1)])
     scope = jax.named_scope("mix0")
@@ -713,10 +749,10 @@
     def by_head(pair):
         ahead, behind = [], []
         for chip in range(kv_size):
-            mine = part_recv[pair, chip, 0].astype(F32)
-            theirs = part_recv[pair, chip, 1].astype(F32)
-            front = jnp.where(upper, mine, theirs)
-            back = pltpu.roll(jnp.where(upper, theirs, mine), slots, 0)
+            even = part_recv[pair, chip, lax.rem(me, 2)].astype(F32)
+            odd = part_recv[pair, chip, lax.rem(me + 1, 2)].astype(F32)
+            front = jnp.where(upper, even, odd)
+            back = pltpu.roll(jnp.where(upper, odd, even), slots, 0)
             for start in range(0, wide, HEAD):
                 ahead.append(front[:, start : start + HEAD])
                 behind.append(back[:, start : start + HEAD])
@@ -730,15 +766,10 @@
     )
     key_unit = key_in * lax.rsqrt(jnp.sum(key_in * key_in, axis=1, keepdims=True) + EPSILON)
     products = dot_fine(jnp.concatenate([key_unit, query_unit], axis=0), key_unit, True)
-    lower = products[:size]
-    lower = jnp.where(strict, write_gate * decay * lower, 0.0)
-    squared = dot_fine(lower, lower)
-    fourth = dot_fine(squared, squared)
-    inverse = dot_fine(identity - lower, identity + squared)
-    inverse = dot_fine(inverse, identity + fourth)
+    lower = jnp.where(strict, write_gate * decay * products[:size], 0.0)
+    scores = products[size:] * decay
     key_grown = (write_gate * growth) * key_unit
     query_grown = query_unit * growth
-    scores = products[size:] * decay
 
     key_terms, query_terms = [], []
     for head in range(HEADS):
@@ -750,14 +781,36 @@
         result = result + dot(both[: 2 * BLK], state_low[head])
         key_terms.append(result[:BLK])
         query_terms.append(result[BLK:])
+    for head in range(HEADS):
+        at = slice(head * BLK, (head + 1) * BLK)
+        for token in range(BLK):
+            place = head * BLK + slots * (token % 2) + token // 2
+            spread_cols[1, head, token] = jnp.broadcast_to(scores[at, place : place + 1], (BLK, HEAD))
+            if token < BLK - 1:
+                spread_cols[0, head, token] = jnp.broadcast_to(
+                    lower[at, place : place + 1], (BLK, HEAD)
+                )
     scope.__exit__(None, None, None)
     with jax.named_scope("partwait1"):
         arrived("part1", part_send.at[1, pl.ds(0, devices - 1)])
     scope = jax.named_scope("mix1")
     scope.__enter__()
     value, gating = by_head(1)
-    update = dot_fine(inverse, write_gate * value - jnp.concatenate(key_terms, axis=0))
-    attend = jnp.concatenate(query_terms, axis=0) + dot_fine(scores, update)
+    updates, attends = [], []
+    for head in range(HEADS):
+        at = slice(head * BLK, (head + 1) * BLK)
+        solved = (write_gate * value)[at] - key_terms[head]
+        attend = query_terms[head]
+        for token in range(BLK):
+            place = slots * (token % 2) + token // 2
+            known = jnp.broadcast_to(solved[place : place + 1], (BLK, HEAD))
+            attend = attend + spread_cols[1, head, token] * known
+            if token < BLK - 1:
+                solved = solved - spread_cols[0, head, token] * known
+        updates.append(solved)
+        attends.append(attend)
+    update = jnp.concatenate(updates, axis=0)
+    attend = jnp.concatenate(attends, axis=0)
     normed = attend * lax.rsqrt(jnp.mean(attend * attend, axis=1, keepdims=True) + EPSILON)
     normed = normed * jax.nn.silu(gating) * live
 
@@ -778,10 +831,10 @@
     heads_send[1] = jnp.concatenate(backs, axis=0).astype(BF16)
     to_all(
         "heads",
-        lambda other, peer: heads_send.at[lax.rem(cls + other, 2)],
+        lambda other, peer: heads_send.at[lax.rem(cls + other + me, 2)],
         lambda other: heads_recv.at[me],
     )
-    heads_recv[me] = heads_send[cls]
+    heads_recv[me] = heads_send[lax.rem(cls + me, 2)]
     scope.__exit__(None, None, None)
 
     with jax.named_scope("newstate"):
@@ -862,16 +915,17 @@
             if index:
                 arrived("second", second_in.at[chip], off)
         with jax.named_scope(f"live_slot{index}"):
-            squares = squares + ffn_slot(
-                live_acc, units2, gains2_ref, chip, second_in[chip], index == 0
+            square, total = ffn_slot(
+                live_acc, units2, gains2_ref, chip, second_in[chip], index
             )
+            squares = squares + square
         if index == 1:
             with jax.named_scope("dead_off"):
                 for off in far_first:
                     hand_off(1, off)
                 hand_own(1)
     with jax.named_scope("finish1"):
-        hidden = finish(live_acc, squares)
+        hidden = finish(total, squares)
     with jax.named_scope("down1"):
         second_down(0, hidden, second_in[kv], True)
     with jax.named_scope("dead_in"):
@@ -883,30 +937,14 @@
             [live_sums[0], dead_sums[0], live_sums[1], dead_sums[1]], axis=0
         )
     with jax.named_scope("tail"):
-        totals = {
-            "tokens": entered.at[pl.ds(0, devices - 1)],
-            "lens": lens_all.at[pl.ds(0, devices - 1)],
-            "proj": proj.at[:, 0 : 4 * cols],
-            "out": out_w.at[:, own_cols],
-            "small": small_acc.at[0],
-            "heads": heads_recv.at[pl.ds(0, devices - 1)],
-            "second": second_in.at[pl.ds(0, kv_size - 1)],
-            "red": red_send.at[:, pl.ds(1, kv_size - 1)],
-            "middle": middle.at[:, pl.ds(0, kv_size - 1)],
-            "part": part_send.at[:, pl.ds(0, devices - 1)],
-            "fin": fin_send.at[:, pl.ds(1, kv_size - 1)],
-            "own": own_send.at[0],
-        }
-        for name, ref in totals.items():
-            sem = send_sems.at[sends[name]]
-            pltpu.make_async_remote_copy(
-                src_ref=ref,
-                dst_ref=ref,
-                send_sem=sem,
-                recv_sem=sem,
-                device_id={"kv": kv, "tp": 1 - tp},
-                device_id_type=MESH,
-            ).wait_send()
+        all_sent("proj", proj.at[:, 0 : 4 * cols])
+        all_sent("small", small_acc.at[0])
+        all_sent("heads", heads_recv.at[pl.ds(0, devices - 1)])
+        all_sent("second", second_in.at[pl.ds(0, kv_size - 1)])
+        all_sent("middle", middle.at[:, pl.ds(0, kv_size - 1)])
+        all_sent("part", part_send.at[:, pl.ds(0, devices - 1)])
+        all_sent("fin", fin_send.at[:, pl.ds(1, kv_size - 1)])
+        all_sent("own", own_send.at[0])
 
 
 def fused_call(mesh, *args):
@@ -967,7 +1005,6 @@
             pltpu.VMEM((devices, half, cols), BF16),
             pltpu.VMEM((half, 2 * hidden_local), F32),
             pltpu.VMEM((pack, 2 * hidden_local), F32),
-            pltpu.VMEM((pack, 2 * hidden_local), F32),
             pltpu.VMEM((pack, 4 * wide), F32),
             pltpu.VMEM((1, pack, HEAD), F32),
             pltpu.VMEM((2, kv_size, pack, wide), BF16),
@@ -983,9 +1020,10 @@
             pltpu.VMEM((2, kv_size, 2, pack, cols), BF16),
             pltpu.VMEM((2, 2, pack, cols), F32),
             pltpu.VMEM((2, pack, cols), F32),
-            dma((kv_size + 13,)),
-            dma((12,)),
-            dma((3 * kv_size + 14,)),
+            pltpu.VMEM((2, HEADS, BLK, BLK, HEAD), F32),
+            dma((kv_size + 7,)),
+            dma((8,)),
+            dma((2 * kv_size + 9,)),
         ],
         compiler_params=pltpu.CompilerParams(
             collective_id=0, has_side_effects=True, vmem_limit_bytes=VMEM_LIMIT
@@ -995,14 +1033,14 @@
 
 
 def hand_out_kernel(packed, order, state, mixed_hbm, state_hbm, mixed, sems):
-    put_state = pltpu.make_async_copy(state, state_hbm, sems.at[0])
-    put_state.start()
+    puts = [pltpu.make_async_copy(state, state_hbm, sems.at[0])]
+    puts[0].start()
     restored = jnp.dot(order[...], packed[...], preferred_element_type=F32)
     mixed[...] = restored.astype(BF16)
-    put_mixed = pltpu.make_async_copy(mixed, mixed_hbm, sems.at[1])
-    put_mixed.start()
-    put_mixed.wait()
-    put_state.wait()
+    puts.append(pltpu.make_async_copy(mixed, mixed_hbm, sems.at[1]))
+    puts[-1].start()
+    for put in puts:
+        put.wait()
 
 
 def hand_out(packed, order, new_state):

time: 41.6 us -> 41.1 us (0.988)
  Pallas kernels: 40.2 us -> 39.7 us
    pallas_call x1, Pallas kernels: 39.2 us -> 38.7 us  [fused_call(): pl.pallas_call(functools.partial(fused_kernel, kv_size, channels), out_sh...]
where the time goes in v4:
time: 41.1 us; the launch traced here: 41 us
  Pallas kernels  39.7 us (97%)
  between operations  1.29 us (3%)
    pallas_call x1, Pallas kernels, fused_call(): pl.pallas_call(functools.partial(fused_kernel, kv_size, channels), out_sh...  38.7 us
    pallas_call x1, Pallas kernels, hand_out(): pl.pallas_call(hand_out_kernel, out_shape=(jax.ShapeDtypeStruct(packed.sh...  0.99 us

profile of v4, /device:TPU:0, one launch (start us, length us, event | category | flops | bytes accessed | tf_op | source)
XLA Modules:
  0.0 41.0 jit_solution(8391957949436674263)
XLA Ops:
  1.3 38.7 %shard_map.203 = (bf16[64,256]{1,0:T(8,128)(2,1)S(1)}, bf16[64,64]{1,0:T(8,128)(2,1)S(1)}, f32[1,16,128,128]{3,2,1,0:T(8,128)S(1)}) custom-call(bf16[64,256]{1,0:T(8,128)(2,1)} %tokens_hbm.1, s32[1,1]{1,0:T(1,128)} %bitcast.7.lengths_hbm, f32[1,2048]{1,0:T(1,128)} %bitcast.10, f32[1,2048]{1,0:T(1,128)} %bitcast.11, f32[1,2048]{1,0:T(1,128)} %bitcast.12, ...), custom_call_target="tpu_custom_call" | custom-call | tf_op jit(solution)/shard_map/pallas_call | solution.py:977
  40.0 1.0 %shard_map.204 = (bf16[64,256]{1,0:T(8,128)(2,1)}, f32[1,16,128,128]{3,2,1,0:T(8,128)}) custom-call(bf16[64,256]{1,0:T(8,128)(2,1)S(1)} %get-tuple-element.5.packed, bf16[64,64]{1,0:T(8,128)(2,1)S(1)} %get-tuple-element.6.order, f32[1,16,128,128]{3,2,1,0:T(8,128)S(1)} %get-tuple-element.7.state), custom_call_target="tpu_custom_call" | custom-call | tf_op jit(solution)/shard_map/pallas_call | solution.py:1053

commit v5 on v4

--- a/solution.py
+++ b/solution.py
@@ -336,7 +336,8 @@
     sends, receives, width = {}, {}, [0]
     send_after = {"heads": "tokens", "second": "lens", "fin": "red", "own": "out"}
     receive_after = {
-        "heads": "tokens",
+        "heads0": "tokens",
+        "heads1": "lens",
         "second": "tokens",
         "fin0": "red0",
         "fin1": "red1",
@@ -391,17 +392,18 @@
             chip = swapped(off)
             remote(name, src(off), dst(off), chip, core_of(chip, 0), off if spread > 1 else 0, spread)
 
-    def to_all(name, src, dst, spread=1):
-        for off in far_first:
+    def to_all(name, src, dst, spread=1, near="", far="", order=far_first):
+        for off in order:
             chip = swapped(off)
             first = lax.rem(chip + cls, 2)
             for other in (first, 1 - first):
                 core = core_of(chip, other)
                 remote(
-                    name, src(other, chip * 2 + core), dst(other), chip, core,
+                    name + (near if off is far_first[2] else far),
+                    src(other, chip * 2 + core), dst(other), chip, core,
                     off if spread > 1 else 0, spread,
                 )
-        to_partner(name, src(1, kv * 2 + 1 - tp), dst(1))
+        to_partner(name + near, src(1, kv * 2 + 1 - tp), dst(1))
 
     def to_partner(name, src, dst):
         remote(name, src, dst, kv, 1 - tp)
@@ -428,15 +430,13 @@
     at_seq = at_class // slots
     which = lax.rem(cls + row // half + at_seq, 2)
     picks = one_hot(col == at_seq * BLK + 2 * lax.rem(at_class, slots) + which)
-    with jax.named_scope("small_wait"):
-        loaded("length")
-        loaded("tokens")
+    loaded("length")
+    loaded("tokens")
     lens_all[me] = jnp.broadcast_to(length_ref[...], (1, HEAD))
     chosen = dot(picks, tokens_ref[...]).astype(BF16)
     picked[...] = chosen.reshape(2, half, cols)
     entered[me] = chosen[:half]
-    with jax.named_scope("barrier"):
-        pl.semaphore_wait(barrier, devices - 1)
+    pl.semaphore_wait(barrier, devices - 1)
     to_all("tokens", lambda other, peer: picked.at[other], lambda other: entered.at[me], kv_size)
     to_all("lens", lambda other, peer: lens_all.at[me], lambda other: lens_all.at[me])
     for name in late:
@@ -505,94 +505,87 @@
     squares = jnp.zeros((half, 1), F32)
     for index, off in enumerate([0] + near_first):
         chip = swapped(off)
-        with jax.named_scope(f"tokens_wait{index}"):
-            if index:
-                arrived("tokens", entered.at[pl.ds(chip * 2, 2)], off)
-            else:
-                arrived("tokens", entered.at[kv * 2 + 1 - tp], off)
-            loaded(f"units1{index}", units1.at[chip_rows(chip), :])
-            if index == kv_size - 1:
-                arrived("lens", lens_all.at[pl.ds(0, devices - 1)])
-        with jax.named_scope(f"units_slot{index}"):
-            if index == kv_size - 1:
-                column = live_column(cls)
-                lane = iota((1, HEAD), 1)
-                place = place_lanes(
-                    jnp.minimum(lane // slots, devices - 1), lax.rem(lane, slots), column
-                )
-                reorder = one_hot(iota((half, HEAD), 0) == place)[:, :half]
-            square, total = ffn_slot(
-                unit_acc, units1, gains1_ref, chip, chip_tokens(chip), index
+        if index:
+            arrived("tokens", entered.at[pl.ds(chip * 2, 2)], off)
+        else:
+            arrived("tokens", entered.at[kv * 2 + 1 - tp], off)
+        loaded(f"units1{index}", units1.at[chip_rows(chip), :])
+        if index == kv_size - 1:
+            arrived("lens", lens_all.at[pl.ds(0, devices - 1)])
+        if index == kv_size - 1:
+            column = live_column(cls)
+            lane = iota((1, HEAD), 1)
+            place = place_lanes(
+                jnp.minimum(lane // slots, devices - 1), lax.rem(lane, slots), column
             )
-            squares = squares + square
+            reorder = one_hot(iota((half, HEAD), 0) == place)[:, :half]
+        square, total = ffn_slot(
+            unit_acc, units1, gains1_ref, chip, chip_tokens(chip), index
+        )
+        squares = squares + square
         if index == kv_size - 2:
-            with jax.named_scope("exchange"):
-                loaded("proj", proj.at[:, 0 : 4 * cols])
-                for kind in range(4):
-                    at = kind_cols(kind)
-                    to_partner("proj", proj.at[:, at], proj.at[:, at])
-    with jax.named_scope("finish0"):
-        hidden = dot(reorder, finish(total, squares)).astype(BF16)
-    with jax.named_scope("down_wait"):
-        loaded("down1")
-    with jax.named_scope("down0"):
-        for pair in pairs:
-            chips = [swapped(off) for off in pair]
-            for off, chip, term in zip(pair, chips, columns_of(hidden, down1, chips)):
-                if off is pairs[1][1]:
-                    own_term = term
-                    continue
-                red_send[0, off] = term[:pack].astype(BF16)
-                red_send[1, off] = term[pack:].astype(BF16)
-                remote("red0", red_send.at[0, off], red_recv.at[0, off], chip, core_of(chip, 0))
-    with jax.named_scope("exchange_out"):
-        loaded("out")
-        to_partner("out", out_w.at[:, own_cols], out_w.at[:, own_cols])
-        for name in last:
-            start(name)
-    with jax.named_scope("tables"):
-        residual = dot(reorder, chip_tokens(kv))
-        flags = live_row(cls)
-        other_flags = live_row(1 - cls)
-        at = iota((rows, HEAD), 0)
-        slot = lax.rem(at, slots)
-        place = place_rows(at // BLK, slot, cls, flags)
-        kind = lax.rem(at // slots + at // BLK + cls, 2)
-        lane = iota((rows, HEAD), 1)
-        spread = one_hot(
-            (lane // pack == kind) & (lax.rem(lane, pack) == place) & (lane < 2 * pack)
-        )[:, : 2 * pack]
-        lane = iota((1, devices * 2 * BLK), 1)
-        place = place_lanes(lane // (2 * BLK), lax.rem(lane, slots), column)
-        at = iota((kv_size * pack, devices * 2 * BLK), 0)
-        chip_at = lax.rem(iota((kv_size * pack, devices * 2 * BLK), 1) // slots, kv_size)
-        gather_heads = one_hot((at // pack == chip_at) & (lax.rem(at, pack) == place))
-        at = iota((BLK, HEAD), 0)
-        klass = lax.rem(at // slots + me, 2)
-        place = place_rows(
-            jnp.zeros((BLK, HEAD), jnp.int32) + me,
-            lax.rem(at, slots),
-            klass,
-            jnp.where(klass == cls, flags, other_flags),
-        )
-        lane = iota((BLK, HEAD), 1)
-        pick_small = jnp.where(
-            (lax.rem(lane // pack + cls, 2) == klass)
-            & (lax.rem(lane, pack) == place)
-            & (lane < 2 * pack),
-            1.0,
-            0.0,
-        )[:, : 2 * pack]
-        at = iota((rows, HEAD), 0)
-        seq, token = at // BLK, lax.rem(at, BLK)
-        klass = lax.rem(seq + token, 2)
-        place = place_rows(seq, token // 2, klass, jnp.where(klass == cls, flags, other_flags))
-        lane = iota((rows, HEAD), 1)
-        order_out[...] = one_hot(
-            (lax.rem(lane // half + cls, 2) == klass)
-            & (lax.rem(lane, half) == place)
-            & (lane < rows)
-        )[:, :rows]
+            loaded("proj", proj.at[:, 0 : 4 * cols])
+            for kind in range(4):
+                at = kind_cols(kind)
+                to_partner("proj", proj.at[:, at], proj.at[:, at])
+    hidden = dot(reorder, finish(total, squares)).astype(BF16)
+    loaded("down1")
+    for pair in pairs:
+        chips = [swapped(off) for off in pair]
+        for off, chip, term in zip(pair, chips, columns_of(hidden, down1, chips)):
+            if off is pairs[1][1]:
+                own_term = term
+                continue
+            red_send[0, off] = term[:pack].astype(BF16)
+            red_send[1, off] = term[pack:].astype(BF16)
+            remote("red0", red_send.at[0, off], red_recv.at[0, off], chip, core_of(chip, 0))
+    loaded("out")
+    to_partner("out", out_w.at[:, own_cols], out_w.at[:, own_cols])
+    for name in last:
+        start(name)
+    residual = dot(reorder, chip_tokens(kv))
+    flags = live_row(cls)
+    other_flags = live_row(1 - cls)
+    at = iota((rows, HEAD), 0)
+    slot = lax.rem(at, slots)
+    place = place_rows(at // BLK, slot, cls, flags)
+    kind = lax.rem(at // slots + at // BLK + cls, 2)
+    lane = iota((rows, HEAD), 1)
+    spread = one_hot(
+        (lane // pack == kind) & (lax.rem(lane, pack) == place) & (lane < 2 * pack)
+    )[:, : 2 * pack]
+    lane = iota((1, devices * 2 * BLK), 1)
+    place = place_lanes(lax.rem(lane, rows) // BLK, lax.rem(lane, slots), column)
+    at = iota((kv_size * pack, devices * 2 * BLK), 0)
+    lane = iota((kv_size * pack, devices * 2 * BLK), 1)
+    chip_at = 2 * (lane // rows) + lax.rem(lane // slots, 2)
+    gather_heads = one_hot((at // pack == chip_at) & (lax.rem(at, pack) == place))
+    at = iota((BLK, HEAD), 0)
+    klass = lax.rem(at // slots + me, 2)
+    place = place_rows(
+        jnp.zeros((BLK, HEAD), jnp.int32) + me,
+        lax.rem(at, slots),
+        klass,
+        jnp.where(klass == cls, flags, other_flags),
+    )
+    lane = iota((BLK, HEAD), 1)
+    pick_small = jnp.where(
+        (lax.rem(lane // pack + cls, 2) == klass)
+        & (lax.rem(lane, pack) == place)
+        & (lane < 2 * pack),
+        1.0,
+        0.0,
+    )[:, : 2 * pack]
+    at = iota((rows, HEAD), 0)
+    seq, token = at // BLK, lax.rem(at, BLK)
+    klass = lax.rem(seq + token, 2)
+    place = place_rows(seq, token // 2, klass, jnp.where(klass == cls, flags, other_flags))
+    lane = iota((rows, HEAD), 1)
+    order_out[...] = one_hot(
+        (lax.rem(lane // half + cls, 2) == klass)
+        & (lax.rem(lane, half) == place)
+        & (lane < rows)
+    )[:, :rows]
     for off in far_first:
         chip = swapped(off)
         remote("red1", red_send.at[1, off], red_recv.at[1, off], chip, core_of(chip, 0))
@@ -611,60 +604,56 @@
             1 if group else kv_size,
         )
 
-    with jax.named_scope("red0"):
-        first_done(0)
-    with jax.named_scope("statecut"):
-        loaded("state")
-        for head in range(HEADS):
-            high = state[head].astype(BF16)
-            state_high[head] = high
-            state_low[head] = (state[head] - high.astype(F32)).astype(BF16)
-    with jax.named_scope("proj_wait"):
-        arrived("proj", proj.at[:, 0 : 4 * cols])
-        loaded("small", small_w.at[0 : 2 * HEADS])
-        loaded("gains_mix")
-        loaded("rates")
+    first_done(0)
+    loaded("state")
+    for head in range(HEADS):
+        high = state[head].astype(BF16)
+        state_high[head] = high
+        state_low[head] = (state[head] - high.astype(F32)).astype(BF16)
+    arrived("proj", proj.at[:, 0 : 4 * cols])
+    loaded("small", small_w.at[0 : 2 * HEADS])
+    loaded("gains_mix")
+    loaded("rates")
     squares = jnp.zeros((pack, 1), F32)
     for index, off in enumerate([0] + near_first):
         chip = swapped(off)
         at = chip_rows(chip)
-        with jax.named_scope(f"middle_wait{index}"):
-            if index:
-                arrived("middle0", middle.at[0, chip], off)
-        with jax.named_scope(f"proj_slot{index}"):
-            values = middle[0, chip].astype(F32)
-            squares = squares + jnp.sum(values * values, axis=1, keepdims=True)
-            scaled = (values * gains_mix_ref[:, at]).astype(BF16)
-            small_term = lax.dot_general(
-                scaled, small_w[:, at], (((1,), (1,)), ((), ())), preferred_element_type=F32
-            )
-            if index == 0:
-                proj_acc[...] = dot(scaled, proj[at, :])
-                small_acc[0] = small_term
-                with jax.named_scope("red1"):
-                    first_done(1)
-            elif index < kv_size - 1:
-                proj_acc[...] += dot(scaled, proj[at, :])
-                small_acc[0] += small_term
-    with jax.named_scope("partsend"):
-        mix_scale = lax.rsqrt(squares / channels + EPSILON)
-        for pair in range(2):
-            lanes = slice(pair * 2 * wide, (pair + 1) * 2 * wide)
-            projected = proj_acc[:, lanes] + dot(scaled, proj[at, lanes])
-            projected = (projected * mix_scale).astype(BF16)
-            stacked = jnp.concatenate([projected[:, :wide], projected[:, wide:]], axis=0)
-            part = dot(spread, stacked).astype(BF16)
-            part_send[pair] = part.reshape(devices, BLK, wide)
-            to_all(
-                f"part{pair}",
-                lambda other, peer: part_send.at[pair, peer],
-                lambda other: part_recv.at[pair, kv, cls],
-            )
-            if pair == 0:
-                small_acc[0] = (small_acc[0] + small_term) * mix_scale
-                to_partner("small", small_acc.at[0], small_recv.at[0])
-        for pair in range(2):
-            part_recv[pair, kv, cls] = part_send[pair, me]
+        if index:
+            arrived("middle0", middle.at[0, chip], off)
+        values = middle[0, chip].astype(F32)
+        squares = squares + jnp.sum(values * values, axis=1, keepdims=True)
+        scaled = (values * gains_mix_ref[:, at]).astype(BF16)
+        small_term = lax.dot_general(
+            scaled, small_w[:, at], (((1,), (1,)), ((), ())), preferred_element_type=F32
+        )
+        if index == 0:
+            proj_acc[...] = dot(scaled, proj[at, :])
+            small_acc[0] = small_term
+            first_done(1)
+        elif index < kv_size - 1:
+            proj_acc[...] += dot(scaled, proj[at, :])
+            small_acc[0] += small_term
+    mix_scale = lax.rsqrt(squares / channels + EPSILON)
+    for pair in range(2):
+        lanes = slice(pair * 2 * wide, (pair + 1) * 2 * wide)
+        projected = proj_acc[:, lanes] + dot(scaled, proj[at, lanes])
+        projected = (projected * mix_scale).astype(BF16)
+        stacked = jnp.concatenate([projected[:, :wide], projected[:, wide:]], axis=0)
+        part = dot(spread, stacked).astype(BF16)
+        part_send[pair] = part.reshape(devices, BLK, wide)
+        to_all(
+            f"part{pair}",
+            lambda other, peer: part_send.at[pair, peer],
+            lambda other: part_recv.at[pair, kv, cls],
+            near="0",
+            far="1",
+            order=[far_first[2], far_first[0], far_first[1]],
+        )
+        if pair == 0:
+            small_acc[0] = (small_acc[0] + small_term) * mix_scale
+            to_partner("small", small_acc.at[0], small_recv.at[0])
+    for pair in range(2):
+        part_recv[pair, kv, cls] = part_send[pair, me]
 
     def cut_terms(a):
         high = a.astype(BF16).astype(F32)
@@ -680,52 +669,48 @@
             left, right, (((1,), (axis,)), ((), ())), preferred_element_type=F32
         )
 
-    with jax.named_scope("premix_a"):
-        size = HEADS * BLK
-
-        def token_of(at):
-            at = lax.rem(at, BLK)
-            return 2 * lax.rem(at, slots) + at // slots
-
-        row = iota((size, size), 0)
-        col = iota((size, size), 1)
-        same = (row // BLK) == (col // BLK)
-        causal = same & (token_of(row) >= token_of(col))
-        strict = same & (token_of(row) > token_of(col))
-        diagonal = row == col
-        pick = iota((size, HEADS), 0) // BLK == iota((size, HEADS), 1)
+    all_sent("tokens", entered.at[pl.ds(0, devices - 1)])
+    all_sent("lens", lens_all.at[pl.ds(0, devices - 1)])
+    all_sent("red", red_send.at[:, pl.ds(1, kv_size - 1)])
+    all_sent("out", out_w.at[:, own_cols])
+    arrived("small", small_recv.at[0])
+    small_all = jnp.concatenate([small_acc[0], small_recv[0]], axis=0)
+    high, low = cut_terms(small_all)
+    picked_small = dot(pick_small.astype(BF16), high.astype(BF16)) + dot(
+        pick_small.astype(BF16), low.astype(BF16)
+    )
+    write_pre = picked_small[:, 0:HEADS]
+    forget_pre = picked_small[:, HEADS : 2 * HEADS]
+
+    heads = HEADS // 2
+    size = heads * BLK
+
+    def token_of(at):
+        at = lax.rem(at, BLK)
+        return 2 * lax.rem(at, slots) + at // slots
+
+    row = iota((size, size), 0)
+    col = iota((size, size), 1)
+    same = (row // BLK) == (col // BLK)
+    causal = same & (token_of(row) >= token_of(col))
+    strict = same & (token_of(row) > token_of(col))
+    diagonal = row == col
+    live = jnp.where(token_of(iota((size, 1), 0)) < length_ref[...], 1.0, 0.0)
+    upper = iota((BLK, wide), 0) < slots
+    even_class = lax.rem(me, 2)
+    per_chip = wide // HEAD
+
+    def to_row(column):
+        return jnp.sum(jnp.where(diagonal, column, 0.0), axis=0, keepdims=True)
+
+    def gates(side):
+        pick = side * heads + iota((size, HEADS), 0) // BLK == iota((size, HEADS), 1)
 
         def as_column(block):
             return jnp.sum(jnp.where(pick, block, 0.0), axis=1, keepdims=True)
 
-        def to_row(column):
-            return jnp.sum(jnp.where(diagonal, column, 0.0), axis=0, keepdims=True)
-
-    with jax.named_scope("dead_units"):
-        all_sent("tokens", entered.at[pl.ds(0, devices - 1)])
-        all_sent("lens", lens_all.at[pl.ds(0, devices - 1)])
-        all_sent("red", red_send.at[:, pl.ds(1, kv_size - 1)])
-        all_sent("out", out_w.at[:, own_cols])
-        loaded("gains2")
-        loaded("units2", units2)
-        arrived("middle1", middle.at[1, pl.ds(0, kv_size - 1)])
-        values = jnp.concatenate([middle[1, chip] for chip in range(kv_size)], axis=1).astype(F32)
-        squares = jnp.sum(values * values, axis=1, keepdims=True)
-        dead_hidden = finish(dot((values * gains2_ref[...]).astype(BF16), units2[...]), squares)
-
-    with jax.named_scope("premix"):
-        arrived("small", small_recv.at[0])
-        small_all = jnp.concatenate([small_acc[0], small_recv[0]], axis=0)
-        high, low = cut_terms(small_all)
-        picked_small = dot(pick_small.astype(BF16), high.astype(BF16)) + dot(
-            pick_small.astype(BF16), low.astype(BF16)
-        )
-        write_pre = picked_small[:, 0:HEADS]
-        forget_pre = picked_small[:, HEADS : 2 * HEADS]
-
-        live = jnp.where(token_of(iota((size, 1), 0)) < length_ref[...], 1.0, 0.0)
-        write_col = as_column(jnp.concatenate([write_pre] * HEADS, axis=0))
-        forget_col = as_column(jnp.concatenate([forget_pre] * HEADS, axis=0))
+        write_col = as_column(jnp.concatenate([write_pre] * heads, axis=0))
+        forget_col = as_column(jnp.concatenate([forget_pre] * heads, axis=0))
         rate_col = as_column(jnp.broadcast_to(rates_ref[...], (size, HEADS)))
         write_gate = jax.nn.sigmoid(write_col) * live
         softplus = jnp.maximum(forget_col, 0.0) + jnp.log1p(jnp.exp(-jnp.abs(forget_col)))
@@ -736,120 +721,111 @@
         decay = jnp.where(
             causal, jnp.exp(jnp.minimum(cumulative - to_row(cumulative), 0.0)), 0.0
         )
-        growth = jnp.exp(cumulative)
-        fading = jnp.exp(final - cumulative)
-        shrink = jnp.exp(final)
-
-    with jax.named_scope("partwait0"):
-        arrived("part0", part_send.at[0, pl.ds(0, devices - 1)])
-    scope = jax.named_scope("mix0")
-    scope.__enter__()
-    upper = iota((BLK, wide), 0) < slots
-
-    def by_head(pair):
+        return write_gate, decay, jnp.exp(cumulative), jnp.exp(final - cumulative), jnp.exp(final)
+
+    def by_head(pair, side):
         ahead, behind = [], []
-        for chip in range(kv_size):
-            even = part_recv[pair, chip, lax.rem(me, 2)].astype(F32)
-            odd = part_recv[pair, chip, lax.rem(me + 1, 2)].astype(F32)
+        for at in range(2):
+            chip = 2 * side + at
+            even = part_recv[pair, chip, even_class].astype(F32)
+            odd = part_recv[pair, chip, 1 - even_class].astype(F32)
             front = jnp.where(upper, even, odd)
             back = pltpu.roll(jnp.where(upper, odd, even), slots, 0)
-            for start in range(0, wide, HEAD):
-                ahead.append(front[:, start : start + HEAD])
-                behind.append(back[:, start : start + HEAD])
+            for start_at in range(0, wide, HEAD):
+                ahead.append(front[:, start_at : start_at + HEAD])
+                behind.append(back[:, start_at : start_at + HEAD])
         return jnp.concatenate(ahead, axis=0), jnp.concatenate(behind, axis=0)
 
-    query, key_in = by_head(0)
-    query_unit = (
-        query
-        * lax.rsqrt(jnp.sum(query * query, axis=1, keepdims=True) + EPSILON)
-        * (1.0 / math.sqrt(HEAD))
-    )
-    key_unit = key_in * lax.rsqrt(jnp.sum(key_in * key_in, axis=1, keepdims=True) + EPSILON)
-    products = dot_fine(jnp.concatenate([key_unit, query_unit], axis=0), key_unit, True)
-    lower = jnp.where(strict, write_gate * decay * products[:size], 0.0)
-    scores = products[size:] * decay
-    key_grown = (write_gate * growth) * key_unit
-    query_grown = query_unit * growth
-
-    key_terms, query_terms = [], []
-    for head in range(HEADS):
-        at = slice(head * BLK, (head + 1) * BLK)
-        high, low = cut_terms(jnp.concatenate([key_grown[at], query_grown[at]], axis=0))
-        both = jnp.concatenate([high, low], axis=0).astype(BF16)
-        result = dot(both, state_high[head])
-        result = result[: 2 * BLK] + result[2 * BLK :]
-        result = result + dot(both[: 2 * BLK], state_low[head])
-        key_terms.append(result[:BLK])
-        query_terms.append(result[BLK:])
-    for head in range(HEADS):
-        at = slice(head * BLK, (head + 1) * BLK)
-        for token in range(BLK):
-            place = head * BLK + slots * (token % 2) + token // 2
-            spread_cols[1, head, token] = jnp.broadcast_to(scores[at, place : place + 1], (BLK, HEAD))
-            if token < BLK - 1:
-                spread_cols[0, head, token] = jnp.broadcast_to(
-                    lower[at, place : place + 1], (BLK, HEAD)
+    kept = []
+    sides = [kv // 2, 1 - kv // 2]
+    all_gates = [gates(side) for side in sides]
+    for group, side in enumerate(sides):
+        write_gate, decay, growth, fading, shrink = all_gates[group]
+        arrived(f"part0{group}", part_send.at[0, pl.ds(0, 3 + group)])
+        query, key_in = by_head(0, side)
+        query_unit = (
+            query
+            * lax.rsqrt(jnp.sum(query * query, axis=1, keepdims=True) + EPSILON)
+            * (1.0 / math.sqrt(HEAD))
+        )
+        key_unit = key_in * lax.rsqrt(
+            jnp.sum(key_in * key_in, axis=1, keepdims=True) + EPSILON
+        )
+        products = dot_fine(jnp.concatenate([key_unit, query_unit], axis=0), key_unit, True)
+        lower = jnp.where(strict, write_gate * decay * products[:size], 0.0)
+        scores = products[size:] * decay
+        key_grown = (write_gate * growth) * key_unit
+        query_grown = query_unit * growth
+        key_terms, query_terms = [], []
+        for head in range(heads):
+            at = slice(head * BLK, (head + 1) * BLK)
+            high, low = cut_terms(jnp.concatenate([key_grown[at], query_grown[at]], axis=0))
+            both = jnp.concatenate([high, low], axis=0).astype(BF16)
+            result = dot(both, state_high[side * heads + head])
+            result = result[: 2 * BLK] + result[2 * BLK :]
+            result = result + dot(both[: 2 * BLK], state_low[side * heads + head])
+            key_terms.append(result[:BLK])
+            query_terms.append(result[BLK:])
+            for token in range(BLK):
+                place = head * BLK + slots * (token % 2) + token // 2
+                spread_cols[1, head, token] = jnp.broadcast_to(
+                    scores[at, place : place + 1], (BLK, HEAD)
                 )
-    scope.__exit__(None, None, None)
-    with jax.named_scope("partwait1"):
-        arrived("part1", part_send.at[1, pl.ds(0, devices - 1)])
-    scope = jax.named_scope("mix1")
-    scope.__enter__()
-    value, gating = by_head(1)
-    updates, attends = [], []
-    for head in range(HEADS):
-        at = slice(head * BLK, (head + 1) * BLK)
-        solved = (write_gate * value)[at] - key_terms[head]
-        attend = query_terms[head]
-        for token in range(BLK):
-            place = slots * (token % 2) + token // 2
-            known = jnp.broadcast_to(solved[place : place + 1], (BLK, HEAD))
-            attend = attend + spread_cols[1, head, token] * known
-            if token < BLK - 1:
-                solved = solved - spread_cols[0, head, token] * known
-        updates.append(solved)
-        attends.append(attend)
-    update = jnp.concatenate(updates, axis=0)
-    attend = jnp.concatenate(attends, axis=0)
-    normed = attend * lax.rsqrt(jnp.mean(attend * attend, axis=1, keepdims=True) + EPSILON)
-    normed = normed * jax.nn.silu(gating) * live
-
-    per_chip = wide // HEAD
-
-    def lanes_of(chip):
-        first = chip * per_chip
-        return jnp.concatenate(
-            [normed[(first + at) * BLK : (first + at + 1) * BLK] for at in range(per_chip)], axis=1
-        )
-
-    fronts, backs = [], []
-    for chip in range(0, kv_size, 2):
-        even, odd = lanes_of(chip), lanes_of(chip + 1)
-        fronts.append(jnp.where(upper, even, pltpu.roll(odd, slots, 0)))
-        backs.append(jnp.where(upper, pltpu.roll(even, slots, 0), odd))
-    heads_send[0] = jnp.concatenate(fronts, axis=0).astype(BF16)
-    heads_send[1] = jnp.concatenate(backs, axis=0).astype(BF16)
-    to_all(
-        "heads",
-        lambda other, peer: heads_send.at[lax.rem(cls + other + me, 2)],
-        lambda other: heads_recv.at[me],
-    )
-    heads_recv[me] = heads_send[lax.rem(cls + me, 2)]
-    scope.__exit__(None, None, None)
-
-    with jax.named_scope("newstate"):
-        faded = key_unit * fading
-        for head in range(HEADS):
+                if token < BLK - 1:
+                    spread_cols[0, head, token] = jnp.broadcast_to(
+                        lower[at, place : place + 1], (BLK, HEAD)
+                    )
+        arrived(f"part1{group}", part_send.at[1, pl.ds(0, 3 + group)])
+        value, gating = by_head(1, side)
+        updates, attends = [], []
+        for head in range(heads):
+            at = slice(head * BLK, (head + 1) * BLK)
+            solved = (write_gate * value)[at] - key_terms[head]
+            attend = query_terms[head]
+            for token in range(BLK):
+                place = slots * (token % 2) + token // 2
+                known = jnp.broadcast_to(solved[place : place + 1], (BLK, HEAD))
+                attend = attend + spread_cols[1, head, token] * known
+                if token < BLK - 1:
+                    solved = solved - spread_cols[0, head, token] * known
+            updates.append(solved)
+            attends.append(attend)
+        attend = jnp.concatenate(attends, axis=0)
+        normed = attend * lax.rsqrt(jnp.mean(attend * attend, axis=1, keepdims=True) + EPSILON)
+        normed = normed * jax.nn.silu(gating) * live
+        even, odd = [
+            jnp.concatenate(
+                [
+                    normed[(first + at) * BLK : (first + at + 1) * BLK]
+                    for at in range(per_chip)
+                ],
+                axis=1,
+            )
+            for first in (0, per_chip)
+        ]
+        heads_send[group, 0] = jnp.where(upper, even, pltpu.roll(odd, slots, 0)).astype(BF16)
+        heads_send[group, 1] = jnp.where(upper, pltpu.roll(even, slots, 0), odd).astype(BF16)
+        to_all(
+            f"heads{group}",
+            lambda other, peer: heads_send.at[group, lax.rem(cls + other + me, 2)],
+            lambda other: heads_recv.at[side, me],
+        )
+        heads_recv[side, me] = heads_send[group, lax.rem(cls + me, 2)]
+        kept.append((key_unit * fading, updates, shrink))
+
+    for side, (faded, updates, shrink) in zip(sides, kept):
+        for head in range(heads):
             at = slice(head * BLK, (head + 1) * BLK)
             key_high, key_low = cut_terms(faded[at])
-            value_high, value_low = cut_terms(update[at])
+            value_high, value_low = cut_terms(updates[head])
             outer = lax.dot_general(
                 jnp.concatenate([key_high, key_high, key_low], axis=0).astype(BF16),
                 jnp.concatenate([value_high, value_low, value_high], axis=0).astype(BF16),
                 (((0,), (0,)), ((), ())),
                 preferred_element_type=F32,
             )
-            state_out[0, head] = shrink[head * BLK : head * BLK + 1] * state[head] + outer
+            index = side * heads + head
+            state_out[0, index] = shrink[head * BLK : head * BLK + 1] * state[index] + outer
 
     def hand_off(group, off):
         chip = swapped(off)
@@ -890,61 +866,57 @@
             sums[other] = sums[other] + 0.5 * total
         return [total.astype(BF16) for total in sums]
 
-    with jax.named_scope("dead_down"):
-        loaded("down2")
-        second_down(1, dead_hidden, middle[1, kv], False)
-    with jax.named_scope("gather2"):
-        arrived("heads", heads_recv.at[pl.ds(0, devices - 1)])
-        arrived("out", out_w.at[:, own_cols])
-    with jax.named_scope("outproj"):
-        blocks = heads_recv[...].reshape(devices * 2 * BLK, wide)
-        mixed = dot(gather_heads, blocks).astype(BF16)
-        terms = []
-        for part in range(2):
-            chips = range(part * kv_size // 2, (part + 1) * kv_size // 2)
-            left = jnp.concatenate([mixed[chip * pack : (chip + 1) * pack] for chip in chips], axis=1)
-            right = out_w[chips[0] * wide : (chips[-1] + 1) * wide, :]
-            terms.append(dot(left, right).astype(BF16).astype(F32))
-        second_in[kv] = (middle[0, kv].astype(F32) + (terms[0] + terms[1])).astype(BF16)
-        to_class("second", lambda off: second_in.at[kv], lambda off: second_in.at[kv], kv_size)
+    loaded("gains2")
+    loaded("units2", units2)
+    arrived("middle1", middle.at[1, pl.ds(0, kv_size - 1)])
+    values = jnp.concatenate([middle[1, chip] for chip in range(kv_size)], axis=1).astype(F32)
+    squares = jnp.sum(values * values, axis=1, keepdims=True)
+    dead_hidden = finish(dot((values * gains2_ref[...]).astype(BF16), units2[...]), squares)
+
+    loaded("down2")
+    second_down(1, dead_hidden, middle[1, kv], False)
+    for group in range(2):
+        arrived(f"heads{group}", heads_recv.at[0, pl.ds(0, devices - 1)])
+    arrived("out", out_w.at[:, own_cols])
+    blocks = heads_recv[...].astype(F32).reshape(devices * 2 * BLK, wide).astype(BF16)
+    mixed = dot(gather_heads, blocks).astype(BF16)
+    terms = []
+    for part in range(2):
+        chips = range(part * kv_size // 2, (part + 1) * kv_size // 2)
+        left = jnp.concatenate([mixed[chip * pack : (chip + 1) * pack] for chip in chips], axis=1)
+        right = out_w[chips[0] * wide : (chips[-1] + 1) * wide, :]
+        terms.append(dot(left, right).astype(BF16).astype(F32))
+    second_in[kv] = (middle[0, kv].astype(F32) + (terms[0] + terms[1])).astype(BF16)
+    to_class("second", lambda off: second_in.at[kv], lambda off: second_in.at[kv], kv_size)
 
     squares = jnp.zeros((pack, 1), F32)
     for index, off in enumerate([0] + near_first):
         chip = swapped(off)
-        with jax.named_scope(f"second_wait{index}"):
-            if index:
-                arrived("second", second_in.at[chip], off)
-        with jax.named_scope(f"live_slot{index}"):
-            square, total = ffn_slot(
-                live_acc, units2, gains2_ref, chip, second_in[chip], index
-            )
-            squares = squares + square
+        if index:
+            arrived("second", second_in.at[chip], off)
+        square, total = ffn_slot(
+            live_acc, units2, gains2_ref, chip, second_in[chip], index
+        )
+        squares = squares + square
         if index == 1:
-            with jax.named_scope("dead_off"):
-                for off in far_first:
-                    hand_off(1, off)
-                hand_own(1)
-    with jax.named_scope("finish1"):
-        hidden = finish(total, squares)
-    with jax.named_scope("down1"):
-        second_down(0, hidden, second_in[kv], True)
-    with jax.named_scope("dead_in"):
-        dead_sums = take_in(1)
-    with jax.named_scope("live_in"):
-        live_sums = take_in(0)
-    with jax.named_scope("last"):
-        packed_out[...] = jnp.concatenate(
-            [live_sums[0], dead_sums[0], live_sums[1], dead_sums[1]], axis=0
-        )
-    with jax.named_scope("tail"):
-        all_sent("proj", proj.at[:, 0 : 4 * cols])
-        all_sent("small", small_acc.at[0])
-        all_sent("heads", heads_recv.at[pl.ds(0, devices - 1)])
-        all_sent("second", second_in.at[pl.ds(0, kv_size - 1)])
-        all_sent("middle", middle.at[:, pl.ds(0, kv_size - 1)])
-        all_sent("part", part_send.at[:, pl.ds(0, devices - 1)])
-        all_sent("fin", fin_send.at[:, pl.ds(1, kv_size - 1)])
-        all_sent("own", own_send.at[0])
+            for off in far_first:
+                hand_off(1, off)
+            hand_own(1)
+    hidden = finish(total, squares)
+    second_down(0, hidden, second_in[kv], True)
+    dead_sums = take_in(1)
+    live_sums = take_in(0)
+    packed_out[...] = jnp.concatenate(
+        [live_sums[0], dead_sums[0], live_sums[1], dead_sums[1]], axis=0
+    )
+    all_sent("proj", proj.at[:, 0 : 4 * cols])
+    all_sent("small", small_acc.at[0])
+    all_sent("heads", heads_recv.at[:, pl.ds(0, devices - 1)])
+    all_sent("second", second_in.at[pl.ds(0, kv_size - 1)])
+    all_sent("middle", middle.at[:, pl.ds(0, kv_size - 1)])
+    all_sent("part", part_send.at[:, pl.ds(0, devices - 1)])
+    all_sent("fin", fin_send.at[:, pl.ds(1, kv_size - 1)])
+    all_sent("own", own_send.at[0])
 
 
 def fused_call(mesh, *args):
@@ -1009,8 +981,8 @@
             pltpu.VMEM((1, pack, HEAD), F32),
             pltpu.VMEM((2, kv_size, pack, wide), BF16),
             pltpu.VMEM((kv_size, pack, wide), BF16),
-            pltpu.VMEM((2, 2 * BLK, wide), BF16),
-            pltpu.VMEM((devices, 2 * BLK, wide), BF16),
+            pltpu.VMEM((2, 2, BLK, wide), BF16),
+            pltpu.VMEM((2, devices, BLK, wide), BF16),
             pltpu.VMEM((2, kv_size, pack, wide), BF16),
             pltpu.VMEM((2, kv_size, pack, wide), BF16),
             pltpu.VMEM((2, devices, BLK, wide), BF16),
@@ -1020,10 +992,10 @@
             pltpu.VMEM((2, kv_size, 2, pack, cols), BF16),
             pltpu.VMEM((2, 2, pack, cols), F32),
             pltpu.VMEM((2, pack, cols), F32),
-            pltpu.VMEM((2, HEADS, BLK, BLK, HEAD), F32),
+            pltpu.VMEM((2, HEADS // 2, BLK, BLK, HEAD), F32),
             dma((kv_size + 7,)),
             dma((8,)),
-            dma((2 * kv_size + 9,)),
+            dma((2 * kv_size + 11,)),
         ],
         compiler_params=pltpu.CompilerParams(
             collective_id=0, has_side_effects=True, vmem_limit_bytes=VMEM_LIMIT

time: 41.1 us -> 39.9 us (0.971)
  Pallas kernels: 39.7 us -> 38.5 us
    pallas_call x1, Pallas kernels: 38.7 us -> 37.5 us  [fused_call(): pl.pallas_call(functools.partial(fused_kernel, kv_size, channels), out_sh...]
where the time goes in v5:
time: 39.9 us; the launch traced here: 39.7 us
  Pallas kernels  38.5 us (96%)
  between operations  1.29 us (3%)
    pallas_call x1, Pallas kernels, fused_call(): pl.pallas_call(functools.partial(fused_kernel, kv_size, channels), out_sh...  37.5 us
    pallas_call x1, Pallas kernels, hand_out(): pl.pallas_call(hand_out_kernel, out_shape=(jax.ShapeDtypeStruct(packed.sh...  0.99 us

profile of v5, /device:TPU:0, one launch (start us, length us, event | category | flops | bytes accessed | tf_op | source)
XLA Modules:
  0.0 39.7 jit_solution(6221919538150600285)
XLA Ops:
  1.3 37.5 %shard_map.203 = (bf16[64,256]{1,0:T(8,128)(2,1)S(1)}, bf16[64,64]{1,0:T(8,128)(2,1)S(1)}, f32[1,16,128,128]{3,2,1,0:T(8,128)S(1)}) custom-call(bf16[64,256]{1,0:T(8,128)(2,1)} %tokens_hbm.1, s32[1,1]{1,0:T(1,128)} %bitcast.7.lengths_hbm, f32[1,2048]{1,0:T(1,128)} %bitcast.10, f32[1,2048]{1,0:T(1,128)} %bitcast.11, f32[1,2048]{1,0:T(1,128)} %bitcast.12, ...), custom_call_target="tpu_custom_call" | custom-call | tf_op jit(solution)/shard_map/pallas_call | solution.py:949
  38.8 1.0 %shard_map.204 = (bf16[64,256]{1,0:T(8,128)(2,1)}, f32[1,16,128,128]{3,2,1,0:T(8,128)}) custom-call(bf16[64,256]{1,0:T(8,128)(2,1)S(1)} %get-tuple-element.5.packed, bf16[64,64]{1,0:T(8,128)(2,1)S(1)} %get-tuple-element.6.order, f32[1,16,128,128]{3,2,1,0:T(8,128)S(1)} %get-tuple-element.7.state), custom_call_target="tpu_custom_call" | custom-call | tf_op jit(solution)/shard_map/pallas_call | solution.py:1025

commit v6 on v5

--- a/solution.py
+++ b/solution.py
@@ -321,8 +321,6 @@
     load("down2", (down2_hbm, down2), after="units12")
     last = ("state", "gains2", "units2", "down2")
     late = [name for name in loads if name not in early and name not in last]
-    for name in early[:2]:
-        start(name)
     barrier = pltpu.get_barrier_semaphore()
     here = 0
     for off in far_first + [here]:
@@ -330,7 +328,7 @@
             pl.semaphore_signal(
                 barrier, inc=1, device_id={"kv": swapped(off), "tp": core}, device_id_type=MESH
             )
-    for name in early[2:]:
+    for name in early:
         start(name)
 
     sends, receives, width = {}, {}, [0]
@@ -840,10 +838,11 @@
         to_partner(f"own{group}", own_send.at[group, 1 - tp], own_recv.at[group])
 
     def second_down(group, hidden, source, at_once):
-        for pair in pairs:
+        alone = [(far_first[0],), (far_first[1], far_first[2]), (0,)]
+        for pair in alone if at_once else pairs:
             chips = [swapped(off) for off in pair]
             for off, chip, term in zip(pair, chips, columns_of(hidden, down2, chips)):
-                if off is pairs[1][1]:
+                if off is alone[2][0]:
                     term = source.astype(F32) + 0.5 * term
                     own_send[group, 0] = term[:, :cols]
                     own_send[group, 1] = term[:, cols:]

time: 39.9 us -> 39.9 us (level)
  no operation moved by 1% of the time
where the time goes in v6:
time: 39.9 us; the launch traced here: 39.8 us
  Pallas kernels  38.5 us (96%)
  between operations  1.29 us (3%)
    pallas_call x1, Pallas kernels, fused_call(): pl.pallas_call(functools.partial(fused_kernel, kv_size, channels), out_sh...  37.5 us
    pallas_call x1, Pallas kernels, hand_out(): pl.pallas_call(hand_out_kernel, out_shape=(jax.ShapeDtypeStruct(packed.sh...  0.99 us

profile of v6, /device:TPU:0, one launch (start us, length us, event | category | flops | bytes accessed | tf_op | source)
XLA Modules:
  0.0 39.8 jit_solution(15487579950158336581)
XLA Ops:
  1.3 37.5 %shard_map.203 = (bf16[64,256]{1,0:T(8,128)(2,1)S(1)}, bf16[64,64]{1,0:T(8,128)(2,1)S(1)}, f32[1,16,128,128]{3,2,1,0:T(8,128)S(1)}) custom-call(bf16[64,256]{1,0:T(8,128)(2,1)} %tokens_hbm.1, s32[1,1]{1,0:T(1,128)} %bitcast.7.lengths_hbm, f32[1,2048]{1,0:T(1,128)} %bitcast.10, f32[1,2048]{1,0:T(1,128)} %bitcast.11, f32[1,2048]{1,0:T(1,128)} %bitcast.12, ...), custom_call_target="tpu_custom_call" | custom-call | tf_op jit(solution)/shard_map/pallas_call | solution.py:948
  38.8 1.0 %shard_map.204 = (bf16[64,256]{1,0:T(8,128)(2,1)}, f32[1,16,128,128]{3,2,1,0:T(8,128)}) custom-call(bf16[64,256]{1,0:T(8,128)(2,1)S(1)} %get-tuple-element.5.packed, bf16[64,64]{1,0:T(8,128)(2,1)S(1)} %get-tuple-element.6.order, f32[1,16,128,128]{3,2,1,0:T(8,128)S(1)} %get-tuple-element.7.state), custom_call_target="tpu_custom_call" | custom-call | tf_op jit(solution)/shard_map/pallas_call | solution.py:1024
